TPU v7x, 256 devices: a whole 4x4x8 slice. The times are simulated.
256 devices in a mesh: ep: 16 (over y, x), tp: 16 (over z, core).
Axes of the slice: x: 4, y: 4, z: 8, core: 2. Of those that a mesh axis runs over, the one named last changes fastest.
Arguments:
- tokens: bfloat16 [1024, 2048], P('ep'), may hold values from -7 to 7
- state: float32 [1024, 32, 64, 64], P('ep', 'tp'), may hold values from -6 to 6
- routes: int32 [1024, 2], P('ep'), may hold values from 0 to 15, all different within a row; in each aligned block of 64 rows (0 to 63, 64 to 127, ...) at most 12 rows name the same one
- route_logits: float32 [1024, 2], P('ep'), may hold values from -4 to 4
- mix_gain: float32 [2048], replicated, may hold values from 0.1 to 1.9
- w_recept: bfloat16 [2048, 2048], P(None, 'tp')
- w_key: bfloat16 [2048, 2048], P(None, 'tp'), may hold values from -0.125 to 0.125
- w_value: bfloat16 [2048, 2048], P(None, 'tp'), may hold values from -0.125 to 0.125
- w_decay: bfloat16 [2048, 2048], P(None, 'tp'), may hold values from -0.125 to 0.125
- w_rate: bfloat16 [2048, 2048], P(None, 'tp'), may hold values from -0.125 to 0.125
- decay_base: float32 [2048], P('tp'), may hold values from -3 to 1
- rate_base: float32 [2048], P('tp'), may hold values from -3 to 3
- key_gain: float32 [2048], P('tp'), may hold values from 0.1 to 1.9
- group_gain: float32 [2048], P('tp'), may hold values from 0.1 to 1.9
- w_output: bfloat16 [2048, 2048], P('tp'), may hold values from -0.125 to 0.125
- ffn_gain: float32 [2048], replicated, may hold values from 0.1 to 1.9
- w_gate: bfloat16 [16, 2048, 7168], P('ep', None, 'tp'), may hold values from -0.125 to 0.125
- w_up: bfloat16 [16, 2048, 7168], P('ep', None, 'tp'), may hold values from -0.125 to 0.125
- w_down: bfloat16 [16, 7168, 2048], P('ep', 'tp'), may hold values from -0.0625 to 0.0625
Outputs:
- output: bfloat16 [1024, 2048], P('ep', 'tp')
- new_state: float32 [1024, 32, 64, 64], P('ep', 'tp')
Inputs may be any that keep to these rules, and one draw needn't show every extreme that they name: `routes`: for each expert, the 64 tokens of one device group's rows name it in at most 12 of their rows; the 2 experts of a row differ.
All inputs are finite; a program needn't handle non-finite values.
Results may differ from a plain program's by a relative error of at most 0.0091.
Values may be sent and summed in bfloat16 or wider, within the bound.
No kernel may reach another device: no remote copies, remote signals or barrier semaphores. Data moves between devices by JAX's collectives and lax.ppermute only.
A program may use at most 64 MiB of HBM per device.

v0:
```python
import jax
import jax.numpy as jnp
from jax import lax
from jax.sharding import Mesh
from jax.sharding import PartitionSpec as P

TP = ("tp_0", "tp_1")


RMS_EPS = 1e-06
GROUP_EPS = 0.00064
UNIT_EPS = 6.4e-05
HIGHEST = lax.Precision.HIGHEST


def cut_along(shard, dim, devices):
    before, after = (shard.shape[:dim], shard.shape[dim + 1 :])
    return jnp.moveaxis(shard.reshape(*before, devices, -1, *after), dim, 0)


def sum_at_owner(shard, axis, dim):
    pieces = cut_along(shard, dim, lax.axis_size(axis))
    arrived = lax.all_to_all(pieces, axis, split_axis=0, concat_axis=0, tiled=True)
    return arrived.astype(jnp.float32).sum(axis=0)


def from_everyone(shard, axis):
    copies = jnp.broadcast_to(shard, (lax.axis_size(axis), *shard.shape))
    return lax.all_to_all(copies, axis, split_axis=0, concat_axis=0, tiled=True)


def of_everyone(shard, axis):
    everything = from_everyone(shard, axis)
    return jnp.sum(everything, axis=0)


def gather_axes(shard, axes, dim):
    for axis in reversed(axes):
        shard = lax.all_gather(shard, axis, axis=dim, tiled=True)
    return shard


def rounded(values):
    return lax.optimization_barrier(values.astype(jnp.bfloat16)).astype(jnp.float32)


def mix_heads(
    normed,
    state,
    w_recept,
    w_key,
    w_value,
    w_decay,
    w_rate,
    decay_base,
    rate_base,
    key_gain,
    group_gain,
):
    seq_rows = state.shape[0]
    head_count = state.shape[1]

    def project(weight):
        return rounded(jnp.dot(normed, weight, preferred_element_type=jnp.float32))

    def split_heads(values):
        return values.reshape(seq_rows, head_count, -1)

    recept = split_heads(project(w_recept))
    keys_now = split_heads(project(w_key))
    values_now = split_heads(project(w_value))
    decay_pre = project(w_decay) + decay_base
    decay_now = split_heads(jnp.exp(-jnp.exp(-jax.nn.softplus(-decay_pre) - 0.5)))
    rate_now = split_heads(jax.nn.sigmoid(project(w_rate) + rate_base))
    scaled = keys_now * key_gain.reshape(head_count, -1)[None]
    unit_key = scaled * lax.rsqrt(jnp.sum(scaled * scaled, axis=2, keepdims=True) + UNIT_EPS)
    removed = jnp.einsum("bhvk,bhk->bhv", state, unit_key, precision=HIGHEST)
    new_state = (
        state * decay_now[:, :, None, :]
        - removed[:, :, :, None] * (unit_key * rate_now)[:, :, None, :]
        + values_now[:, :, :, None] * keys_now[:, :, None, :]
    )
    readout = jnp.einsum("bhvk,bhk->bhv", new_state, recept, precision=HIGHEST)
    centred = readout - jnp.mean(readout, axis=2, keepdims=True)
    spread = jnp.mean(centred * centred, axis=2, keepdims=True)
    normed_read = centred * lax.rsqrt(spread + GROUP_EPS) * group_gain.reshape(head_count, -1)[None]
    return (normed_read.reshape(seq_rows, -1).astype(jnp.bfloat16), new_state)


def slot_numbers(route_rows, expert_count, capacity):
    flat_routes = route_rows.reshape(-1)
    one_hot = (flat_routes[:, None] == jnp.arange(expert_count, dtype=jnp.int32)[None, :]).astype(
        jnp.int32
    )
    earlier = jnp.cumsum(one_hot, axis=0) - one_hot
    placed = jnp.sum(earlier * one_hot, axis=1)
    return (flat_routes * capacity + placed).reshape(route_rows.shape)


def local(
    tokens,
    state,
    routes,
    route_logits,
    mix_gain,
    w_recept,
    w_key,
    w_value,
    w_decay,
    w_rate,
    decay_base,
    rate_base,
    key_gain,
    group_gain,
    w_output,
    ffn_gain,
    w_gate,
    w_up,
    w_down,
):
    seq_rows, full_width = tokens.shape
    top_count = routes.shape[1]
    share_cols = full_width // lax.axis_size(TP)
    tp_index = lax.axis_index(TP)
    group_count = lax.axis_size("ep")
    capacity = max(2, 3 * top_count * seq_rows // (2 * group_count))
    slot_count = group_count * capacity
    values = tokens.astype(jnp.float32)
    normed = (
        values * lax.rsqrt(jnp.mean(values * values, axis=1, keepdims=True) + RMS_EPS) * mix_gain
    ).astype(jnp.bfloat16)
    mixed_rows, new_state = mix_heads(
        normed,
        state,
        w_recept,
        w_key,
        w_value,
        w_decay,
        w_rate,
        decay_base,
        rate_base,
        key_gain,
        group_gain,
    )
    partial_out = jnp.dot(mixed_rows, w_output, preferred_element_type=jnp.float32)
    slot_ids = slot_numbers(routes, group_count, capacity)
    slot_range = jnp.arange(slot_count, dtype=jnp.int32)
    pick_rows = jnp.any(slot_ids[None, :, :] == slot_range[:, None, None], axis=2).astype(
        jnp.bfloat16
    )
    route_exp = jnp.exp(route_logits)
    route_weight = route_exp / jnp.sum(route_exp, axis=1, keepdims=True)
    combine = jnp.sum(
        jnp.where(slot_ids[:, :, None] == slot_range[None, None, :], route_weight[:, :, None], 0.0),
        axis=1,
    )
    mix_part = sum_at_owner(partial_out.astype(jnp.bfloat16), TP, 1)
    own_vals = lax.dynamic_slice_in_dim(values, tp_index * share_cols, share_cols, 1)
    resid_own = (own_vals + mix_part).astype(jnp.bfloat16)
    resid_vals = resid_own.astype(jnp.float32)
    square_sum = of_everyone(jnp.sum(resid_vals * resid_vals, axis=1), TP)
    own_gain = lax.dynamic_slice_in_dim(ffn_gain, tp_index * share_cols, share_cols, 0)
    ffn_cols = (
        resid_vals * lax.rsqrt(square_sum / full_width + RMS_EPS)[:, None] * own_gain
    ).astype(jnp.bfloat16)
    outgoing = jnp.dot(pick_rows, ffn_cols, preferred_element_type=jnp.float32).astype(jnp.bfloat16)
    arrived = lax.all_to_all(
        outgoing.reshape(group_count, capacity, share_cols),
        "ep",
        split_axis=0,
        concat_axis=0,
        tiled=True,
    )
    slot_cols = arrived.reshape(slot_count, share_cols)
    gate_local = w_gate[0]
    up_local = w_up[0]
    segment = gather_axes(slot_cols, TP, 1)
    gate_act = jnp.dot(segment, gate_local, preferred_element_type=jnp.float32)
    upward = jnp.dot(segment, up_local, preferred_element_type=jnp.float32)
    hidden = (jax.nn.silu(gate_act) * upward).astype(jnp.bfloat16)
    expert_part = jnp.dot(hidden, w_down[0], preferred_element_type=jnp.float32)
    returned = lax.all_to_all(
        expert_part.reshape(group_count, capacity, full_width).astype(jnp.bfloat16),
        "ep",
        split_axis=0,
        concat_axis=0,
        tiled=True,
    ).astype(jnp.float32)
    moe_full = jnp.dot(
        combine,
        returned.reshape(slot_count, full_width),
        precision=HIGHEST,
        preferred_element_type=jnp.float32,
    )
    moe_own = sum_at_owner(moe_full.astype(jnp.bfloat16), TP, 1)
    output = (resid_own.astype(jnp.float32) + moe_own).astype(jnp.bfloat16)
    return (output, new_state)


def solution(mesh):
    torus = Mesh(mesh.devices.reshape(mesh.shape["ep"], 8, 2), ("ep", "tp_0", "tp_1"))
    return jax.shard_map(
        local,
        mesh=torus,
        in_specs=(
            P("ep", None),
            P("ep", TP, None, None),
            P("ep", None),
            P("ep", None),
            P(),
            P(None, TP),
            P(None, TP),
            P(None, TP),
            P(None, TP),
            P(None, TP),
            P(TP),
            P(TP),
            P(TP),
            P(TP),
            P(TP, None),
            P(),
            P("ep", None, TP),
            P("ep", None, TP),
            P("ep", TP, None),
        ),
        out_specs=(P("ep", TP), P("ep", TP, None, None)),
        check_vma=False,
    )
```

profile of v0, /device:TPU:1, one launch (start us, length us, event | category | flops | bytes accessed | tf_op | source)
XLA Modules:
  0.0 147.5 jit_solution(14206047786434785173)
XLA Ops:
  0.6 1.2 multiply_reduce_fusion
  1.9 1.4 convolution_convert_fusion.7
  3.4 0.7 mul.173
  4.3 1.4 convolution_convert_fusion.6
  5.8 0.7 add_divide_fusion
  6.6 1.4 convolution_convert_fusion.8
  8.0 0.7 fusion.24
  8.8 1.4 convolution_convert_fusion.5
  10.3 1.4 convolution_convert_fusion.4
  12.0 8.5 %fusion.29 = f32[64,2,1,64]{3,2,1,0:T(1,128)S(1)} fusion(f32[64,2,64,1]{2,3,1,0:T(1,128)S(1)} %bitcast.59, f32[64,2,64,64]{3,2,1,0:T(8,128)} %param.20), kind=kOutput, calls=%fused_computation.63 | convolution fusion | flops 6291456 | bytes 2162688 | tf_op jit(solution)/shard_map/bhvk,bhk->bhv/dot_general | solution.py:77
  20.4 2.7 %multiply_add_fusion = f32[64,2,64,64]{3,2,1,0:T(8,128)S(1)} fusion(f32[64,2,64,64]{3,2,1,0:T(8,128)S(1)} %copy-done.1, f32[64,2,64]{2,1,0:T(2,128)S(1)} %reshape.117, f32[64,2,64]{2,1,0:T(2,128)S(1)} %reshape.118, f32[64,2,64]{2,1,0:T(2,128)S(1)} %get-tuple-element.4, f32[64,2,64]{2,1,0:T(2,128)S(1)} %bitcast.58, f32[64,2,64]{2,1,0:T(2,128)S(1)} %mul.170), kind=kLoop, calls=%fused_computation | loop fusion | flops 2621440 | bytes 4358144 | tf_op jit(solution)/shard_map/add | solution.py:79
  23.2 2.0 %copy-done.2 = f32[64,2,64,64]{3,2,1,0:T(8,128)} copy-done((f32[64,2,64,64]{3,2,1,0:T(8,128)}, f32[64,2,64,64]{3,2,1,0:T(8,128)S(1)}, u32[]{:S(2)}) %copy-start.2) | copy-done | bytes 2097176
  25.2 3.4 %fusion.30 = f32[64,2,1,64]{3,2,1,0:T(1,128)S(1)} fusion(f32[64,2,64,64]{3,2,1,0:T(8,128)S(1)} %multiply_add_fusion, bf16[64,2,64,1]{2,3,1,0:T(2,128)(2,1)S(1)} %reshape.125), kind=kOutput, calls=%fused_computation.64 | convolution fusion | flops 6291456 | bytes 2146304 | tf_op jit(solution)/shard_map/bhvk,bhk->bhv/dot_general | solution.py:83
  29.6 0.8 copy.102
  30.4 10.0 %all-to-all-start = ((bf16[16,64,128]{2,1,0:T(8,128)(2,1)}), bf16[16,64,128]{2,1,0:T(8,128)(2,1)S(1)}, u32[]{:S(2)}, u32[]{:S(2)}) async-start(bf16[16,64,128]{2,1,0:T(8,128)(2,1)} %bitcast.53), calls=%async_computation | async-start | bytes 524288 | tf_op jit(solution)/shard_map/all_to_all | solution.py:23
  41.3 10.6 %all-to-all-done = bf16[16,64,128]{2,1,0:T(8,128)(2,1)S(1)} async-done(((bf16[16,64,128]{2,1,0:T(8,128)(2,1)}), bf16[16,64,128]{2,1,0:T(8,128)(2,1)S(1)}, u32[]{:S(2)}, u32[]{:S(2)}) %all-to-all-start) | async-done | bytes 262176 | tf_op jit(solution)/shard_map/all_to_all | solution.py:23
  52.1 0.6 broadcast_in_dim.12
  52.7 3.4 %all-to-all-start.1 = ((f32[16,1,64]{2,1,0:T(1,128)}), f32[16,1,64]{2,1,0:T(1,128)S(1)}, u32[]{:S(2)}, u32[]{:S(2)}) async-start(f32[16,1,64]{2,1,0:T(1,128)} %broadcast_in_dim.12), calls=%async_computation.1 | async-start | bytes 16384 | tf_op jit(solution)/shard_map/all_to_all | solution.py:29
  56.2 0.8 dynamic_slice.7
  57.0 5.7 %all-to-all-done.1 = f32[16,1,64]{2,1,0:T(1,128)S(1)} async-done(((f32[16,1,64]{2,1,0:T(1,128)}), f32[16,1,64]{2,1,0:T(1,128)S(1)}, u32[]{:S(2)}, u32[]{:S(2)}) %all-to-all-start.1) | async-done | bytes 4128 | tf_op jit(solution)/shard_map/all_to_all | solution.py:29
  63.0 13.1 %all_to_all.26 = bf16[16,12,128]{2,1,0:T(8,128)(2,1)S(1)} all-to-all(bf16[16,12,128]{2,1,0:T(8,128)(2,1)S(1)} %reshape.112), channel_id=1, replica_groups=mesh['ep'=16,'tp_0'=8,'tp_1'=2] {'ep'}, dimensions={0} | all-to-all | bytes 98304 | tf_op jit(solution)/shard_map/all_to_all | solution.py:167
  76.1 3.6 %all_gather.6 = bf16[192,256]{1,0:T(8,128)(2,1)S(1)} all-gather(bf16[192,128]{1,0:T(8,128)(2,1)S(1)} %reshape.113), channel_id=1, replica_groups=mesh['ep'=16,'tp_0'=8,'tp_1'=2] {'tp_1'}, dimensions={1}, use_global_device_ids=true | all-gather | bytes 147456 | tf_op jit(solution)/shard_map/all_gather | solution.py:39
  79.7 20.6 %all_gather.7 = bf16[192,2048]{1,0:T(8,128)(2,1)S(1)} all-gather(bf16[192,256]{1,0:T(8,128)(2,1)S(1)} %all_gather.6), channel_id=1, replica_groups=mesh['ep'=16,'tp_0'=8,'tp_1'=2] {'tp_0'}, dimensions={1}, use_global_device_ids=true | all-gather | bytes 884736 | tf_op jit(solution)/shard_map/all_gather | solution.py:39
  100.4 2.2 %fusion.3 = f32[192,448]{1,0:T(8,128)S(1)} fusion(bf16[192,2048]{1,0:T(8,128)(2,1)S(1)} %all_gather.7, bf16[1,2048,448]{1,2,0:T(8,128)(2,1)} %param.35), kind=kOutput, calls=%fused_computation.7 | convolution fusion | flops 352321536 | bytes 2965504 | tf_op jit(solution)/shard_map/dot_general | solution.py:178
  102.5 2.2 %fusion.8 = bf16[192,448]{1,0:T(8,128)(2,1)S(1)} fusion(bf16[192,2048]{1,0:T(8,128)(2,1)S(1)} %all_gather.7, bf16[1,2048,448]{1,2,0:T(8,128)(2,1)} %param.36, f32[192,448]{1,0:T(8,128)S(1)} %fusion.3), kind=kOutput, calls=%fused_computation.10 | convolution fusion | flops 352837632 | bytes 3137536 | tf_op jit(solution)/shard_map/dot_general | solution.py:179
  104.8 0.6 convolution_convert_fusion
  105.5 1.4 copy.85
  106.9 3.7 %all-to-all-start.3 = ((bf16[16,12,2048]{2,1,0:T(8,128)(2,1)}), bf16[16,12,2048]{2,1,0:T(8,128)(2,1)S(1)}, u32[]{:S(2)}, u32[]{:S(2)}) async-start(bf16[16,12,2048]{2,1,0:T(8,128)(2,1)} %copy.85), calls=%async_computation.3 | async-start | bytes 2097152 | tf_op jit(solution)/shard_map/all_to_all | solution.py:182
  110.7 12.3 %all-to-all-done.3 = bf16[16,12,2048]{2,1,0:T(8,128)(2,1)S(1)} async-done(((bf16[16,12,2048]{2,1,0:T(8,128)(2,1)}), bf16[16,12,2048]{2,1,0:T(8,128)(2,1)S(1)}, u32[]{:S(2)}, u32[]{:S(2)}) %all-to-all-start.3) | async-done | bytes 786464 | tf_op jit(solution)/shard_map/all_to_all | solution.py:182
  123.0 1.1 reshape.114
  124.0 1.7 %fusion.12 = bf16[8,16,8,128]{3,2,1,0:T(8,128)(2,1)S(1)} fusion(f32[64,192]{1,0:T(8,128)S(1)} %select_reduce_fusion, bf16[192,2048]{1,0:T(8,128)(2,1)} %reshape.114), kind=kOutput, calls=%fused_computation.12 | convolution fusion | flops 302120960 | bytes 1097728 | tf_op jit(solution)/shard_map/dot_general | solution.py:189
  125.8 21.0 %all_to_all.27 = bf16[16,64,128]{2,1,0:T(8,128)(2,1)S(1)} all-to-all(bf16[16,64,128]{2,1,0:T(8,128)(2,1)S(1)} %bitcast.57), channel_id=1, replica_groups=mesh['ep'=16,'tp_0'=8,'tp_1'=2] {'tp_0','tp_1'}, dimensions={0} | all-to-all | bytes 524288 | tf_op jit(solution)/shard_map/all_to_all | solution.py:23
  (56 shorter events, 4.2 us)
Async XLA Ops:
  0.6 104.2 %copy-start = (bf16[1,448,2048]{2,1,0:T(8,128)(2,1)S(1)}, bf16[1,448,2048]{2,1,0:T(8,128)(2,1)}, u32[]{:S(2)}) copy-start(bf16[1,448,2048]{2,1,0:T(8,128)(2,1)} %param.37) | copy-start | bytes 5505028
  11.8 8.6 %copy-start.1 = (f32[64,2,64,64]{3,2,1,0:T(8,128)S(1)}, f32[64,2,64,64]{3,2,1,0:T(8,128)}, u32[]{:S(2)}) copy-start(f32[64,2,64,64]{3,2,1,0:T(8,128)} %param.20) | copy-start | bytes 6291460
  23.2 2.0 %copy-start.2 = (f32[64,2,64,64]{3,2,1,0:T(8,128)}, f32[64,2,64,64]{3,2,1,0:T(8,128)S(1)}, u32[]{:S(2)}) copy-start(f32[64,2,64,64]{3,2,1,0:T(8,128)S(1)} %multiply_add_fusion) | copy-start | bytes 6291460
  25.2 3.8 %copy-start.7 = (f32[128]{0:T(128)S(1)}, f32[128]{0:T(128)}, u32[]{:S(2)}) copy-start(f32[128]{0:T(128)} %param.32) | copy-start | bytes 1540
  25.2 4.2 %copy-start.4 = (bf16[128,2048]{1,0:T(8,128)(2,1)S(1)}, bf16[128,2048]{1,0:T(8,128)(2,1)}, u32[]{:S(2)}) copy-start(bf16[128,2048]{1,0:T(8,128)(2,1)} %param.33) | copy-start | bytes 1572868
  25.2 15.1 %copy-start.3 = (bf16[64,2048]{1,0:T(8,128)(2,1)S(1)}, bf16[64,2048]{1,0:T(8,128)(2,1)}, u32[]{:S(2)}) copy-start(bf16[64,2048]{1,0:T(8,128)(2,1)} %param.19) | copy-start | bytes 786436
  25.2 15.2 %copy-start.5 = (s32[64,2]{0,1:T(2,128)S(1)}, s32[64,2]{0,1:T(2,128)}, u32[]{:S(2)}) copy-start(s32[64,2]{0,1:T(2,128)} %param.21) | copy-start | bytes 1540
  30.4 21.6 %all-to-all-start = ((bf16[16,64,128]{2,1,0:T(8,128)(2,1)}), bf16[16,64,128]{2,1,0:T(8,128)(2,1)S(1)}, u32[]{:S(2)}, u32[]{:S(2)}) async-start(bf16[16,64,128]{2,1,0:T(8,128)(2,1)} %bitcast.53), calls=%async_computation | async-start | bytes 524288 | tf_op jit(solution)/shard_map/all_to_all | solution.py:23
  52.7 10.0 %all-to-all-start.1 = ((f32[16,1,64]{2,1,0:T(1,128)}), f32[16,1,64]{2,1,0:T(1,128)S(1)}, u32[]{:S(2)}, u32[]{:S(2)}) async-start(f32[16,1,64]{2,1,0:T(1,128)} %broadcast_in_dim.12), calls=%async_computation.1 | async-start | bytes 16384 | tf_op jit(solution)/shard_map/all_to_all | solution.py:29
  104.7 5.8 %copy-start.6 = (f32[64,2]{0,1:T(2,128)S(1)}, f32[64,2]{0,1:T(2,128)}, u32[]{:S(2)}) copy-start(f32[64,2]{0,1:T(2,128)} %param.22) | copy-start | bytes 1540
  106.9 16.1 %all-to-all-start.3 = ((bf16[16,12,2048]{2,1,0:T(8,128)(2,1)}), bf16[16,12,2048]{2,1,0:T(8,128)(2,1)S(1)}, u32[]{:S(2)}, u32[]{:S(2)}) async-start(bf16[16,12,2048]{2,1,0:T(8,128)(2,1)} %copy.85), calls=%async_computation.3 | async-start | bytes 2097152 | tf_op jit(solution)/shard_map/all_to_all | solution.py:182
where the time goes:
time: 148 us; the launch traced here: 147 us
  blocking collectives  58.4 us (39%)
  waiting for transfers between devices  28.6 us (19%)
  matrix products  26 us (18%)
  starting transfers between devices  17 us (11%)
  local copies, waits for them, and re-layouts  8.66 us (6%)
  other arithmetic  7.79 us (5%)
    all_gather x2, blocking collectives, gather_axes(): shard = lax.all_gather(shard, axis, axis=dim, tiled=True)  24.3 us
    all_to_all x1, blocking collectives, sum_at_owner(): lax.all_to_all(pieces, axis, split_axis=0, concat_axis=0, tiled=True)  21 us
    all_to_all x1, blocking collectives, local(): lax.all_to_all(outgoing.reshape(group_count, capacity, share_cols), 'ep',...  13.1 us
    all_to_all x1, waiting for transfers between devices, local(): lax.all_to_all(expert_part.reshape(group_count, capacity, full_width).ast...  12.3 us
    all_to_all x1, waiting for transfers between devices, sum_at_owner(): lax.all_to_all(pieces, axis, split_axis=0, concat_axis=0, tiled=True)  10.6 us
    all_to_all x1, starting transfers between devices, sum_at_owner(): lax.all_to_all(pieces, axis, split_axis=0, concat_axis=0, tiled=True)  9.97 us
    dot_general x1, matrix products, mix_heads(): removed = jnp.einsum('bhvk,bhk->bhv', state, unit_key, precision=HIGHEST)  8.46 us
    dot_general x5, matrix products, project(): return rounded(jnp.dot(normed, weight, preferred_element_type=jnp.float32))  7.09 us
  transfers between devices with their start and end apart: 3, of which 3 were waited for; matrix products, arithmetic and copies ran while one was open for 1% of the time, Pallas kernels for 0%

commit v1 on v0

v1 whole, which is shorter than its diff:
```python
import jax
import jax.numpy as jnp
from jax import lax
from jax.experimental import pallas as pl
from jax.experimental.pallas import tpu as pltpu
from jax.sharding import Mesh
from jax.sharding import PartitionSpec as P

TP = ("tp_0", "tp_1")

RMS_EPS = 1e-06
GROUP_EPS = 0.00064
UNIT_EPS = 6.4e-05
HIGHEST = lax.Precision.HIGHEST
F32 = jnp.float32
BF16 = jnp.bfloat16
VMEM = pltpu.VMEM
HEAD = 64
LANES = 128


def head_sums(values):
    rows = lax.broadcasted_iota(jnp.int32, (LANES, LANES), 0) // HEAD
    cols = lax.broadcasted_iota(jnp.int32, (LANES, LANES), 1) // HEAD
    ones = (rows == cols).astype(F32)
    return jnp.dot(values, ones, precision=HIGHEST, preferred_element_type=F32)


def mix_kernel(
    core_ref,
    tokens_hbm,
    state_hbm,
    w_recept_hbm,
    w_key_hbm,
    w_value_hbm,
    w_decay_hbm,
    w_rate_hbm,
    w_output_hbm,
    mix_gain_ref,
    decay_base_ref,
    rate_base_ref,
    key_gain_ref,
    group_gain_ref,
    keep_ref,
    send_ref,
    removed_ref,
    unit_rate_ref,
    decay_ref,
    key_ref,
    value_ref,
    tokens_ref,
    weights_ref,
    w_output_ref,
    state_ref,
    vectors_ref,
    products_ref,
    sems,
):
    seqs = tokens_ref.shape[0]
    chunks = state_ref.shape[0]
    chunk_rows = state_ref.shape[1]
    copies = [pltpu.make_async_copy(tokens_hbm, tokens_ref, sems.at[0])]
    sources = (w_key_hbm, w_value_hbm, w_recept_hbm, w_decay_hbm, w_rate_hbm)
    for place, source in enumerate(sources):
        target = weights_ref.at[:, pl.ds(place * LANES, LANES)]
        copies.append(pltpu.make_async_copy(source, target, sems.at[1 + place]))
    for chunk in range(chunks):
        source = state_hbm.at[pl.ds(chunk * chunk_rows, chunk_rows)]
        copies.append(pltpu.make_async_copy(source, state_ref.at[chunk], sems.at[6 + chunk]))
    copies.append(pltpu.make_async_copy(w_output_hbm, w_output_ref, sems.at[6 + chunks]))
    for copy in copies:
        copy.start()

    copies[0].wait()
    values = tokens_ref[...].astype(F32)
    mean_square = jnp.mean(values * values, axis=1, keepdims=True)
    normed = (values * lax.rsqrt(mean_square + RMS_EPS) * mix_gain_ref[...]).astype(BF16)

    def project(first, count):
        for place in range(first, first + count):
            copies[1 + place].wait()
        weight = weights_ref[:, first * LANES : (first + count) * LANES]
        return jnp.dot(normed, weight, preferred_element_type=F32).astype(BF16).astype(F32)

    key_value = project(0, 2)
    keys_now = key_value[:, :LANES]
    values_now = key_value[:, LANES:]
    recept_decay = project(2, 2)
    recept = recept_decay[:, :LANES]
    decay_pre = recept_decay[:, LANES:] + decay_base_ref[...]
    rate_pre = project(4, 1) + rate_base_ref[...]
    decay_now = jnp.exp(-jnp.exp(-jax.nn.softplus(-decay_pre) - 0.5))
    rate_now = jax.nn.sigmoid(rate_pre)
    scaled = keys_now * key_gain_ref[...]
    unit_key = scaled * lax.rsqrt(head_sums(scaled * scaled) + UNIT_EPS)
    unit_rate = unit_key * rate_now
    decayed_recept = decay_now * recept
    unit_rate_ref[...] = unit_rate
    decay_ref[...] = decay_now
    key_ref[...] = keys_now
    value_ref[...] = values_now

    vectors_ref[...] = jnp.zeros_like(vectors_ref)
    vectors_ref[pl.ds(0, seqs, stride=8), :] = unit_key
    vectors_ref[pl.ds(1, seqs, stride=8), :] = decayed_recept
    vectors_ref[pl.ds(2, seqs, stride=8), :] = pltpu.roll(unit_key, HEAD, 1)
    vectors_ref[pl.ds(3, seqs, stride=8), :] = pltpu.roll(decayed_recept, HEAD, 1)
    per_chunk = chunk_rows // LANES
    for chunk in range(chunks):
        copies[6 + chunk].wait()
        for inner in range(per_chunk):
            seq = chunk * per_chunk + inner
            left = vectors_ref[seq * 8 : seq * 8 + 8, :HEAD].astype(BF16)
            right = state_ref[chunk, inner * LANES : (inner + 1) * LANES, :].astype(BF16)
            products_ref[seq * 8 : seq * 8 + 8, :] = lax.dot_general(
                left, right, (((1,), (1,)), ((), ())), preferred_element_type=F32
            )
    first_head = lax.broadcasted_iota(jnp.int32, (seqs, LANES), 1) < HEAD
    removed = jnp.where(
        first_head,
        products_ref[pl.ds(0, seqs, stride=8), :],
        products_ref[pl.ds(2, seqs, stride=8), :],
    )
    faded = jnp.where(
        first_head,
        products_ref[pl.ds(1, seqs, stride=8), :],
        products_ref[pl.ds(3, seqs, stride=8), :],
    )
    removed_ref[...] = removed
    readout = (
        faded - removed * head_sums(unit_rate * recept) + values_now * head_sums(keys_now * recept)
    )
    centred = readout - head_sums(readout) * (1.0 / HEAD)
    spread = head_sums(centred * centred) * (1.0 / HEAD)
    mixed = (centred * lax.rsqrt(spread + GROUP_EPS) * group_gain_ref[...]).astype(BF16)
    copies[6 + chunks].wait()
    core = core_ref[0]
    for z in range(keep_ref.shape[0]):
        own = w_output_ref[:, pl.ds(pl.multiple_of((2 * z + core) * LANES, LANES), LANES)]
        keep_ref[z] = jnp.dot(mixed, own, preferred_element_type=F32)
        other = w_output_ref[:, pl.ds(pl.multiple_of((2 * z + 1 - core) * LANES, LANES), LANES)]
        send_ref[z] = jnp.dot(mixed, other, preferred_element_type=F32).astype(BF16)


def mix(core, tokens, state_rows, projections, w_output, mix_gain, vectors, z_count):
    seqs, full_width = tokens.shape
    chunks = 4
    chunk_rows = state_rows.shape[0] // chunks
    small = jax.ShapeDtypeStruct((seqs, LANES), F32)
    hbm = pl.BlockSpec(memory_space=pl.ANY)
    vmem = pl.BlockSpec(memory_space=VMEM)
    return pl.pallas_call(
        mix_kernel,
        out_shape=(
            jax.ShapeDtypeStruct((z_count, seqs, LANES), F32),
            jax.ShapeDtypeStruct((z_count, seqs, LANES), BF16),
            small,
            small,
            small,
            small,
            small,
        ),
        in_specs=[pl.BlockSpec(memory_space=pltpu.SMEM)] + [hbm] * 8 + [vmem] * 5,
        out_specs=(vmem,) * 7,
        scratch_shapes=[
            VMEM((seqs, full_width), BF16),
            VMEM((full_width, 5 * LANES), BF16),
            VMEM((LANES, full_width), BF16),
            VMEM((chunks, chunk_rows, HEAD), F32),
            VMEM((seqs * 8, LANES), F32),
            VMEM((seqs * 8, LANES), F32),
            pltpu.SemaphoreType.DMA((7 + chunks,)),
        ],
        compiler_params=pltpu.CompilerParams(vmem_limit_bytes=24 << 20),
        name="mix",
    )(core, tokens, state_rows, *projections, w_output, mix_gain, *vectors)


def update_kernel(
    state_ref,
    removed_ref,
    unit_rate_ref,
    decay_ref,
    key_ref,
    value_ref,
    out_ref,
    left_ref,
    right_ref,
):
    block = removed_ref.shape[0]
    first_head = lax.broadcasted_iota(jnp.int32, (block, LANES), 1) < HEAD
    removed = -removed_ref[...]
    removed_high = removed.astype(BF16).astype(F32)
    removed_low = removed - removed_high
    unit_rate = unit_rate_ref[...]
    unit_high = unit_rate.astype(BF16).astype(F32)
    unit_low = unit_rate - unit_high
    key = key_ref[...]
    lefts = (removed_high, removed_low, removed_high, value_ref[...])
    rights = (unit_high, unit_high, unit_low, key)
    for place in range(4):
        left_ref[pl.ds(place, block, stride=8), :] = jnp.where(first_head, lefts[place], 0.0)
        left_ref[pl.ds(place + 4, block, stride=8), :] = jnp.where(first_head, 0.0, lefts[place])
        right_ref[pl.ds(place, block, stride=8), :] = rights[place]
        right_ref[pl.ds(place + 4, block, stride=8), :] = pltpu.roll(rights[place], HEAD, 1)
    decay = decay_ref[...]
    decay_rolled = pltpu.roll(decay, HEAD, 1)
    for seq in range(block):
        left = left_ref[seq * 8 : seq * 8 + 8, :].astype(BF16)
        right = right_ref[seq * 8 : seq * 8 + 8, :HEAD].astype(BF16)
        change = lax.dot_general(
            left, right, (((0,), (0,)), ((), ())), preferred_element_type=F32
        )
        base = seq * LANES
        old = state_ref[base : base + HEAD, :]
        out_ref[base : base + HEAD, :] = old * decay[seq : seq + 1, :HEAD] + change[:HEAD]
        old = state_ref[base + HEAD : base + LANES, :]
        out_ref[base + HEAD : base + LANES, :] = (
            old * decay_rolled[seq : seq + 1, :HEAD] + change[HEAD:]
        )


def update_state(state_rows, removed, unit_rate, decay, key, value):
    seqs = removed.shape[0]
    steps = 8
    block = seqs // steps
    rows = pl.BlockSpec((block * LANES, HEAD), lambda i: (i, 0))
    small = pl.BlockSpec((block, LANES), lambda i: (i, 0))
    return pl.pallas_call(
        update_kernel,
        grid=(steps,),
        out_shape=jax.ShapeDtypeStruct(state_rows.shape, F32),
        in_specs=[rows] + [small] * 5,
        out_specs=rows,
        scratch_shapes=[VMEM((block * 8, LANES), F32), VMEM((block * 8, LANES), F32)],
        compiler_params=pltpu.CompilerParams(vmem_limit_bytes=8 << 20),
        cost_estimate=pl.CostEstimate(
            flops=2_000_000_000, bytes_accessed=8 << 20, transcendentals=0
        ),
        name="update_state",
    )(state_rows, removed, unit_rate, decay, key, value)


def pick_kernel(pick_ref, rows_ref, out_ref):
    for z in range(rows_ref.shape[0]):
        out_ref[:, z * LANES : (z + 1) * LANES] = jnp.dot(
            pick_ref[...], rows_ref[z], preferred_element_type=F32
        ).astype(BF16)


def pick_rows(pick, rows):
    return pl.pallas_call(
        pick_kernel,
        out_shape=jax.ShapeDtypeStruct((pick.shape[0], rows.shape[0] * LANES), BF16),
        compiler_params=pltpu.CompilerParams(vmem_limit_bytes=8 << 20),
        name="pick_rows",
    )(pick, rows)


def expert_kernel(
    core_ref,
    own_ref,
    other_ref,
    gain_ref,
    gate_ref,
    up_ref,
    down_ref,
    keep_ref,
    send_ref,
    x_ref,
    out_ref,
):
    core = core_ref[0]
    full_width = x_ref.shape[1]
    blocks = full_width // (2 * LANES)
    own = own_ref[...].astype(F32)
    other = other_ref[...].astype(F32)
    square_sum = jnp.sum(own * own, axis=1, keepdims=True) + jnp.sum(
        other * other, axis=1, keepdims=True
    )
    scale = lax.rsqrt(square_sum / full_width + RMS_EPS)
    for z in range(blocks):
        here = slice(z * LANES, (z + 1) * LANES)
        cols = pl.ds(pl.multiple_of((2 * z + core) * LANES, LANES), LANES)
        x_ref[:, cols] = (own[:, here] * scale * gain_ref[:, cols]).astype(BF16)
        cols = pl.ds(pl.multiple_of((2 * z + 1 - core) * LANES, LANES), LANES)
        x_ref[:, cols] = (other[:, here] * scale * gain_ref[:, cols]).astype(BF16)
    x = x_ref[...]
    across = (((1,), (1,)), ((), ()))
    gate_act = lax.dot_general(x, gate_ref[...], across, preferred_element_type=F32)
    upward = lax.dot_general(x, up_ref[...], across, preferred_element_type=F32)
    hidden = (jax.nn.silu(gate_act) * upward).astype(BF16)
    out_ref[...] = jnp.dot(hidden, down_ref[...], preferred_element_type=F32)
    for z in range(blocks):
        here = slice(z * LANES, (z + 1) * LANES)
        cols = pl.ds(pl.multiple_of((2 * z + core) * LANES, LANES), LANES)
        keep_ref[:, here] = out_ref[:, cols]
        cols = pl.ds(pl.multiple_of((2 * z + 1 - core) * LANES, LANES), LANES)
        send_ref[:, here] = out_ref[:, cols].astype(BF16)


def run_expert(core, own, other, gain, gate, up, down):
    rows, half = own.shape
    vmem = pl.BlockSpec(memory_space=VMEM)
    return pl.pallas_call(
        expert_kernel,
        out_shape=(
            jax.ShapeDtypeStruct((rows, half), F32),
            jax.ShapeDtypeStruct((rows, half), BF16),
        ),
        in_specs=[pl.BlockSpec(memory_space=pltpu.SMEM)] + [vmem] * 6,
        out_specs=(vmem, vmem),
        scratch_shapes=[VMEM((rows, 2 * half), BF16), VMEM((rows, 2 * half), F32)],
        compiler_params=pltpu.CompilerParams(vmem_limit_bytes=24 << 20),
        name="expert",
    )(core, own, other, gain, gate, up, down)


def combine_kernel(weight_ref, rows_ref, out_ref):
    weight = weight_ref[...]
    high = weight.astype(BF16)
    low = (weight - high.astype(F32)).astype(BF16)
    for z in range(out_ref.shape[0]):
        rows = rows_ref[:, z * LANES : (z + 1) * LANES]
        total = jnp.dot(high, rows, preferred_element_type=F32) + jnp.dot(
            low, rows, preferred_element_type=F32
        )
        out_ref[z] = total.astype(BF16)


def combine_rows(weight, rows):
    z_count = rows.shape[1] // LANES
    return pl.pallas_call(
        combine_kernel,
        out_shape=jax.ShapeDtypeStruct((z_count, weight.shape[0], LANES), BF16),
        compiler_params=pltpu.CompilerParams(vmem_limit_bytes=8 << 20),
        name="combine",
    )(weight, rows)


def slot_numbers(route_rows, expert_count, capacity):
    flat_routes = route_rows.reshape(-1)
    one_hot = (flat_routes[:, None] == jnp.arange(expert_count, dtype=jnp.int32)[None, :]).astype(
        jnp.int32
    )
    earlier = jnp.cumsum(one_hot, axis=0) - one_hot
    placed = jnp.sum(earlier * one_hot, axis=1)
    return (flat_routes * capacity + placed).reshape(route_rows.shape)


def swap(shard):
    return lax.ppermute(shard, "tp_1", [(0, 1), (1, 0)])


def exchange(shard, axis):
    return lax.all_to_all(shard, axis, split_axis=0, concat_axis=0, tiled=True)


def local(
    tokens,
    state,
    routes,
    route_logits,
    mix_gain,
    w_recept,
    w_key,
    w_value,
    w_decay,
    w_rate,
    decay_base,
    rate_base,
    key_gain,
    group_gain,
    w_output,
    ffn_gain,
    w_gate,
    w_up,
    w_down,
):
    seq_rows, full_width = tokens.shape
    z_count = lax.axis_size("tp_0")
    share_cols = full_width // lax.axis_size(TP)
    tp_index = lax.axis_index(TP)
    core = lax.axis_index("tp_1").astype(jnp.int32).reshape(1)
    group_count = lax.axis_size("ep")
    slot_rows = 16
    slot_count = group_count * slot_rows
    half = full_width // 2

    state_rows = state.reshape(-1, HEAD)
    keep, send, removed, unit_rate, decay, key, value = mix(
        core,
        tokens,
        state_rows,
        (w_recept, w_key, w_value, w_decay, w_rate),
        w_output,
        mix_gain.reshape(1, -1),
        [v.reshape(1, -1) for v in (decay_base, rate_base, key_gain, group_gain)],
        z_count,
    )
    pair_sum = (keep + swap(send).astype(F32)).astype(BF16)
    parts = exchange(pair_sum, "tp_0")
    new_state = update_state(state_rows, removed, unit_rate, decay, key, value)

    slot_ids = slot_numbers(routes, group_count, slot_rows)
    slot_range = jnp.arange(slot_count, dtype=jnp.int32)
    pick = jnp.any(slot_ids[None, :, :] == slot_range[:, None, None], axis=2).astype(BF16)
    route_exp = jnp.exp(route_logits)
    route_weight = route_exp / jnp.sum(route_exp, axis=1, keepdims=True)
    weight = jnp.sum(
        jnp.where(slot_ids[:, :, None] == slot_range[None, None, :], route_weight[:, :, None], 0.0),
        axis=1,
    )

    own_vals = lax.dynamic_slice_in_dim(tokens, tp_index * share_cols, share_cols, 1)
    resid_own = (own_vals.astype(F32) + parts.astype(F32).sum(axis=0)).astype(BF16)
    resid_half = exchange(jnp.broadcast_to(resid_own, (z_count, *resid_own.shape)), "tp_0")
    outgoing = pick_rows(pick, resid_half)
    arrived = exchange(outgoing.reshape(group_count, slot_rows, half), "ep")
    arrived = arrived.reshape(slot_count, half)
    keep, send = run_expert(
        core,
        arrived,
        swap(arrived),
        ffn_gain.reshape(1, -1),
        jnp.swapaxes(w_gate[0], 0, 1),
        jnp.swapaxes(w_up[0], 0, 1),
        w_down[0],
    )
    pair_sum = (keep + swap(send).astype(F32)).astype(BF16)
    returned = exchange(pair_sum.reshape(group_count, slot_rows, half), "ep")
    moe_parts = exchange(combine_rows(weight, returned.reshape(slot_count, half)), "tp_0")
    moe_own = moe_parts.astype(F32).sum(axis=0)
    output = (resid_own.astype(F32) + moe_own).astype(BF16)
    return (output, new_state.reshape(state.shape))


def solution(mesh):
    torus = Mesh(mesh.devices.reshape(mesh.shape["ep"], 8, 2), ("ep", "tp_0", "tp_1"))
    return jax.shard_map(
        local,
        mesh=torus,
        in_specs=(
            P("ep", None),
            P("ep", TP, None, None),
            P("ep", None),
            P("ep", None),
            P(),
            P(None, TP),
            P(None, TP),
            P(None, TP),
            P(None, TP),
            P(None, TP),
            P(TP),
            P(TP),
            P(TP),
            P(TP),
            P(TP, None),
            P(),
            P("ep", None, TP),
            P("ep", None, TP),
            P("ep", TP, None),
        ),
        out_specs=(P("ep", TP), P("ep", TP, None, None)),
        check_vma=False,
    )
```

time: 148 us -> 110 us (0.74)
  blocking collectives: 58.4 us -> 15.5 us
  matrix products: 26 us -> 0 us
  Pallas kernels: 0 us -> 13.3 us
  local copies, waits for them, and re-layouts: 8.66 us -> 19.1 us
  starting transfers between devices: 17 us -> 25.1 us
  other arithmetic: 7.79 us -> 3.7 us
  waiting for transfers between devices: 28.6 us -> 30.6 us
    dot_general x13 -> x0, matrix products: 26 us -> none  [the longest x1 8.46 us: mix_heads(): removed = jnp.einsum('bhvk,bhk->bhv', state, unit_key, precision=HIGHEST)]
    all_gather x2 -> x0, blocking collectives: 24.3 us -> none  [gather_axes(): shard = lax.all_gather(shard, axis, axis=dim, tiled=True)]
    all_to_all x2 -> x1, blocking collectives: 34.1 us -> 15.5 us  [exchange(): return lax.all_to_all(shard, axis, split_axis=0, concat_axis=0, tiled=True)]
    unnamed x17 -> x41, local copies, waits for them, and re-layouts: 2.14 us -> 18 us
    pallas_call x0 -> x5, Pallas kernels: none -> 13.3 us  [the longest x1 4.71 us: mix(): pl.pallas_call(mix_kernel, out_shape=(jax.ShapeDtypeStruct((z_count, seqs...]
    ppermute x0 -> x3, starting transfers between devices: none -> 8.34 us  [swap(): return lax.ppermute(shard, 'tp_1', [(0, 1), (1, 0)])]
    ppermute x0 -> x3, waiting for transfers between devices: none -> 3.83 us  [swap(): return lax.ppermute(shard, 'tp_1', [(0, 1), (1, 0)])]
    add x1 -> x0, other arithmetic: 2.75 us -> none  [mix_heads(): state * decay_now[:, :, None, :]]
  transfers between devices with their start and end apart: 3 -> 7, of which waited for: 3 -> 7; matrix products, arithmetic and copies ran while one was open for 1% -> 1% of each run, Pallas kernels for 0% -> 4%
where the time goes in v1:
time: 110 us; the launch traced here: 108 us
  waiting for transfers between devices  30.6 us (28%)
  starting transfers between devices  25.1 us (23%)
  local copies, waits for them, and re-layouts  19.1 us (17%)
  blocking collectives  15.5 us (14%)
  Pallas kernels  13.3 us (12%)
  other arithmetic  3.7 us (3%)
    all_to_all x4, waiting for transfers between devices, exchange(): return lax.all_to_all(shard, axis, split_axis=0, concat_axis=0, tiled=True)  26.8 us
    unnamed x41, local copies, waits for them, and re-layouts  18 us
    all_to_all x4, starting transfers between devices, exchange(): return lax.all_to_all(shard, axis, split_axis=0, concat_axis=0, tiled=True)  16.8 us
    all_to_all x1, blocking collectives, exchange(): return lax.all_to_all(shard, axis, split_axis=0, concat_axis=0, tiled=True)  15.5 us
    ppermute x3, starting transfers between devices, swap(): return lax.ppermute(shard, 'tp_1', [(0, 1), (1, 0)])  8.34 us
    pallas_call x1, Pallas kernels, mix(): pl.pallas_call(mix_kernel, out_shape=(jax.ShapeDtypeStruct((z_count, seqs...  4.71 us
    pallas_call x1, Pallas kernels, update_state(): pl.pallas_call(update_kernel, grid=(steps,), out_shape=jax.ShapeDtypeStru...  4.61 us
    ppermute x3, waiting for transfers between devices, swap(): return lax.ppermute(shard, 'tp_1', [(0, 1), (1, 0)])  3.83 us
  transfers between devices with their start and end apart: 7, of which 7 were waited for; matrix products, arithmetic and copies ran while one was open for 1% of the time, Pallas kernels for 4%

profile of v1, /device:TPU:1, one launch (start us, length us, event | category | flops | bytes accessed | tf_op | source)
XLA Modules:
  0.0 108.3 jit_solution(9402283577950819551)
XLA Ops:
  0.7 2.2 %copy-done = f32[64,2,64,64]{3,2,1,0:T(8,128)S(1)} copy-done((f32[64,2,64,64]{3,2,1,0:T(8,128)S(1)}, f32[64,2,64,64]{3,2,1,0:T(8,128)}, u32[]{:S(2)}) %copy-start) | copy-done | bytes 2097176
  2.8 1.0 copy-done.5
  3.9 1.0 copy-done.6
  4.9 1.0 copy-done.7
  6.0 1.0 copy-done.8
  7.0 1.0 copy-done.9
  8.0 1.0 copy-done.10
  9.1 0.9 copy-done.11
  10.0 0.7 copy-done.12
  13.4 4.7 %mix.1 = (f32[8,64,128]{2,1,0:T(8,128)S(1)}, bf16[8,64,128]{2,1,0:T(8,128)(2,1)S(1)}, f32[64,128]{1,0:T(8,128)S(1)}, f32[64,128]{1,0:T(8,128)S(1)}, f32[64,128]{...) custom-call(s32[1]{0:T(128)} %bitcast.core_ref, bf16[64,2048]{1,0:T(8,128)(2,1)S(1)} %copy-done.11, ...), custom_call_target="tpu_custom_call" | custom-call | tf_op jit(solution)/shard_map/mix/pallas_call | solution.py:152
  18.1 3.3 %collective-permute-start = (bf16[8,64,128]{2,1,0:T(8,128)(2,1)S(1)}, bf16[8,64,128]{2,1,0:T(8,128)(2,1)S(1)}, u32[]{:S(2)}, u32[]{:S(2)}) collective-permute-start(bf16[8,64,128]{2,1,0:T(8,128)(2,1)S(1)} %get-tuple-element.12), channel_id=1, source_target_pairs={{0,1},{1,0},{2,3},{3,2},{4,5},{5,4},{6,7},{7,6},{8,9},{9,8},{10,11... | collective-permute-start | bytes 393224 | tf_op jit(solution)/shard_map/ppermute | solution.py:352
  21.6 0.7 collective-permute-done
  23.0 6.5 %all-to-all-start = ((bf16[8,64,128]{2,1,0:T(8,128)(2,1)}), bf16[8,64,128]{2,1,0:T(8,128)(2,1)S(1)}, u32[]{:S(2)}, u32[]{:S(2)}) async-start(bf16[8,64,128]{2,1,0:T(8,128)(2,1)} %add_convert_fusion.1), calls=%async_computation | async-start | bytes 262144 | tf_op jit(solution)/shard_map/all_to_all | solution.py:356
  30.2 7.3 %all-to-all-done = bf16[8,64,128]{2,1,0:T(8,128)(2,1)S(1)} async-done(((bf16[8,64,128]{2,1,0:T(8,128)(2,1)}), bf16[8,64,128]{2,1,0:T(8,128)(2,1)S(1)}, u32[]{:S(2)}, u32[]{:S(2)}) %all-to-all-start) | async-done | bytes 131104 | tf_op jit(solution)/shard_map/all_to_all | solution.py:356
  37.5 0.7 add_convert_fusion.3
  38.9 3.4 %all-to-all-start.1 = ((bf16[8,64,128]{2,1,0:T(8,128)(2,1)}), bf16[8,64,128]{2,1,0:T(8,128)(2,1)S(1)}, u32[]{:S(2)}, u32[]{:S(2)}) async-start(bf16[8,64,128]{2,1,0:T(8,128)(2,1)} %broadcast_in_dim.22), calls=%async_computation.1 | async-start | bytes 262144 | tf_op jit(solution)/shard_map/all_to_all | solution.py:356
  42.5 7.7 %all-to-all-done.1.rows_ref = bf16[8,64,128]{2,1,0:T(8,128)(2,1)S(1)} async-done(((bf16[8,64,128]{2,1,0:T(8,128)(2,1)}), bf16[8,64,128]{2,1,0:T(8,128)(2,1)S(1)}, u32[]{:S(2)}, u32[]{:S(2)}) %all-to-all-start.1) | async-done | bytes 131104 | tf_op jit(solution)/shard_map/all_to_all | solution.py:356
  50.5 15.5 %all_to_all.25 = bf16[16,16,1024]{2,1,0:T(8,128)(2,1)S(1)} all-to-all(bf16[16,16,1024]{2,1,0:T(8,128)(2,1)S(1)} %bitcast.23), channel_id=1, replica_groups=mesh['ep'=16,'tp_0'=8,'tp_1'=2] {'ep'}, dimensions={0} | all-to-all | bytes 1048576 | tf_op jit(solution)/shard_map/all_to_all | solution.py:356
  66.0 4.6 %collective-permute-start.1 = (bf16[256,1024]{1,0:T(8,128)(2,1)S(1)}, bf16[256,1024]{1,0:T(8,128)(2,1)S(1)}, u32[]{:S(2)}, u32[]{:S(2)}) collective-permute-start(bf16[256,1024]{1,0:T(8,128)(2,1)S(1)} %bitcast.24), channel_id=1, source_target_pairs={{0,1},{1,0},{2,3},{3,2},{4,5},{5,4},{6,7},{7,6},{8,9},{9,8},{10,11... | collective-permute-start | bytes 1572872 | tf_op jit(solution)/shard_map/ppermute | solution.py:352
  70.6 1.5 %collective-permute-done.1.other_ref = bf16[256,1024]{1,0:T(8,128)(2,1)S(1)} collective-permute-done((bf16[256,1024]{1,0:T(8,128)(2,1)S(1)}, bf16[256,1024]{1,0:T(8,128)(2,1)S(1)}, u32[]{:S(2)}, u32[]{:S(2)}) %collective-permute-start.1) | collective-permute-done | bytes 524320 | tf_op jit(solution)/shard_map/ppermute | solution.py:352
  72.2 1.5 %copy-done.3 = bf16[1,2048,448]{1,2,0:T(8,128)(2,1)S(1)} copy-done((bf16[1,2048,448]{1,2,0:T(8,128)(2,1)S(1)}, bf16[1,2048,448]{1,2,0:T(8,128)(2,1)}, u32[]{:S(2)}) %copy-start.3) | copy-done | bytes 1835032
  73.7 1.5 %copy-done.4 = bf16[1,448,2048]{2,1,0:T(8,128)(2,1)S(1)} copy-done((bf16[1,448,2048]{2,1,0:T(8,128)(2,1)S(1)}, bf16[1,448,2048]{2,1,0:T(8,128)(2,1)}, u32[]{:S(2)}) %copy-start.4) | copy-done | bytes 1835032
  75.2 2.8 %expert.1 = (f32[256,1024]{1,0:T(8,128)S(1)}, bf16[256,1024]{1,0:T(8,128)(2,1)S(1)}) custom-call(s32[1]{0:T(128)} %bitcast.core_ref, bf16[256,1024]{1,0:T(8,128)(2,1)S(1)} %bitcast.25, bf16[256,1024]{1,0:T(8,128)(2,1)S(1)} %collective-permute-done.1.other_ref, f32[1,2048]{1,0:T(1,128)S(1)} %bitcast.30, bf16[448,2048]{1,0:T(8,128)(2,1)S(1)} %bitcast.26, ...), custom_call_target="tpu_custom_call" | custom-call | tf_op jit(solution)/shard_map/expert/pallas_call | solution.py:305
  78.4 1.5 %collective-permute-done.2 = bf16[256,1024]{1,0:T(8,128)(2,1)S(1)} collective-permute-done((bf16[256,1024]{1,0:T(8,128)(2,1)S(1)}, bf16[256,1024]{1,0:T(8,128)(2,1)S(1)}, u32[]{:S(2)}, u32[]{:S(2)}) %collective-permute-start.2) | collective-permute-done | bytes 524320 | tf_op jit(solution)/shard_map/ppermute | solution.py:352
  80.0 1.0 add_convert_fusion
  80.9 3.6 %all-to-all-start.3 = ((bf16[16,16,1024]{2,1,0:T(8,128)(2,1)}), bf16[16,16,1024]{2,1,0:T(8,128)(2,1)S(1)}, u32[]{:S(2)}, u32[]{:S(2)}) async-start(bf16[16,16,1024]{2,1,0:T(8,128)(2,1)} %bitcast.15), calls=%async_computation.3 | async-start | bytes 1048576 | tf_op jit(solution)/shard_map/all_to_all | solution.py:356
  84.7 10.8 %all-to-all-done.3 = bf16[16,16,1024]{2,1,0:T(8,128)(2,1)S(1)} async-done(((bf16[16,16,1024]{2,1,0:T(8,128)(2,1)}), bf16[16,16,1024]{2,1,0:T(8,128)(2,1)S(1)}, u32[]{:S(2)}, u32[]{:S(2)}) %all-to-all-start.3) | async-done | bytes 524320 | tf_op jit(solution)/shard_map/all_to_all | solution.py:356
  95.5 1.0 combine.1
  96.4 3.4 %all-to-all-start.4 = ((bf16[8,64,128]{2,1,0:T(8,128)(2,1)}), bf16[8,64,128]{2,1,0:T(8,128)(2,1)S(1)}, u32[]{:S(2)}, u32[]{:S(2)}) async-start(bf16[8,64,128]{2,1,0:T(8,128)(2,1)} %combine.1), calls=%async_computation.4 | async-start | bytes 262144 | tf_op jit(solution)/shard_map/all_to_all | solution.py:356
  99.8 2.2 %copy-done.1 = f32[64,2,64,64]{3,2,1,0:T(8,128)S(1)} copy-done((f32[64,2,64,64]{3,2,1,0:T(8,128)S(1)}, f32[64,2,64,64]{3,2,1,0:T(8,128)}, u32[]{:S(2)}) %copy-start.1) | copy-done | bytes 2097176
  102.0 4.6 %update_state.1 = f32[8192,64]{1,0:T(8,128)} custom-call(f32[8192,64]{1,0:T(8,128)S(1)} %bitcast.21, f32[64,128]{1,0:T(8,128)S(1)} %get-tuple-element.15.removed_ref, f32[64,128]{1,0:T(8,128)S(1)} %get-tuple-element.16.unit_rate_ref, f32[64,128]{1,0:T(8,128)S(1)} %get-tuple-element.17.decay_ref, f32[64,128]{1,0:T(8,128)S(1)} %get-tuple-element.18.key_ref, ...), custom_call_target="tpu_custom_call" | custom-call | flops 2000000000 | bytes 8388608 | tf_op jit(solution)/shard_map/update_state/pallas_call | solution.py:229
  106.6 1.1 all-to-all-done.4
  (49 shorter events, 6.6 us)
Async XLA Ops:
  0.6 2.2 %copy-start = (f32[64,2,64,64]{3,2,1,0:T(8,128)S(1)}, f32[64,2,64,64]{3,2,1,0:T(8,128)}, u32[]{:S(2)}) copy-start(f32[64,2,64,64]{3,2,1,0:T(8,128)} %param.20) | copy-start | bytes 6291460
  2.8 1.0 copy-start.5
  3.9 1.0 copy-start.6
  4.9 1.0 copy-start.7
  6.0 1.0 copy-start.8
  7.0 1.0 copy-start.9
  8.0 1.0 copy-start.10
  9.1 0.9 copy-start.11
  10.0 0.7 copy-start.12
  10.7 0.7 copy-start.14
  11.4 0.7 copy-start.15
  12.0 0.7 copy-start.16
  12.7 0.7 copy-start.17
  13.4 8.0 %copy-start.18 = (s32[64,2]{0,1:T(2,128)S(1)}, s32[64,2]{0,1:T(2,128)}, u32[]{:S(2)}) copy-start(s32[64,2]{0,1:T(2,128)} %param.21) | copy-start | bytes 1540
  18.1 4.3 %collective-permute-start = (bf16[8,64,128]{2,1,0:T(8,128)(2,1)S(1)}, bf16[8,64,128]{2,1,0:T(8,128)(2,1)S(1)}, u32[]{:S(2)}, u32[]{:S(2)}) collective-permute-start(bf16[8,64,128]{2,1,0:T(8,128)(2,1)S(1)} %get-tuple-element.12), channel_id=1, source_target_pairs={{0,1},{1,0},{2,3},{3,2},{4,5},{5,4},{6,7},{7,6},{8,9},{9,8},{10,11... | collective-permute-start | bytes 393224 | tf_op jit(solution)/shard_map/ppermute | solution.py:352
  22.3 49.8 %copy-start.2 = (bf16[1,2048,448]{1,2,0:T(8,128)(2,1)S(1)}, bf16[1,2048,448]{1,2,0:T(8,128)(2,1)}, u32[]{:S(2)}) copy-start(bf16[1,2048,448]{1,2,0:T(8,128)(2,1)} %param.35) | copy-start | bytes 5505028
  22.3 49.8 %copy-start.13 = (f32[2048]{0:T(1024)S(1)}, f32[2048]{0:T(1024)}, u32[]{:S(2)}) copy-start(f32[2048]{0:T(1024)} %param.34) | copy-start | bytes 24580
  23.0 14.4 %all-to-all-start = ((bf16[8,64,128]{2,1,0:T(8,128)(2,1)}), bf16[8,64,128]{2,1,0:T(8,128)(2,1)S(1)}, u32[]{:S(2)}, u32[]{:S(2)}) async-start(bf16[8,64,128]{2,1,0:T(8,128)(2,1)} %add_convert_fusion.1), calls=%async_computation | async-start | bytes 262144 | tf_op jit(solution)/shard_map/all_to_all | solution.py:356
  38.9 11.3 %all-to-all-start.1 = ((bf16[8,64,128]{2,1,0:T(8,128)(2,1)}), bf16[8,64,128]{2,1,0:T(8,128)(2,1)S(1)}, u32[]{:S(2)}, u32[]{:S(2)}) async-start(bf16[8,64,128]{2,1,0:T(8,128)(2,1)} %broadcast_in_dim.22), calls=%async_computation.1 | async-start | bytes 262144 | tf_op jit(solution)/shard_map/all_to_all | solution.py:356
  66.0 6.1 %collective-permute-start.1 = (bf16[256,1024]{1,0:T(8,128)(2,1)S(1)}, bf16[256,1024]{1,0:T(8,128)(2,1)S(1)}, u32[]{:S(2)}, u32[]{:S(2)}) collective-permute-start(bf16[256,1024]{1,0:T(8,128)(2,1)S(1)} %bitcast.24), channel_id=1, source_target_pairs={{0,1},{1,0},{2,3},{3,2},{4,5},{5,4},{6,7},{7,6},{8,9},{9,8},{10,11... | collective-permute-start | bytes 1572872 | tf_op jit(solution)/shard_map/ppermute | solution.py:352
  72.2 1.5 %copy-start.3 = (bf16[1,2048,448]{1,2,0:T(8,128)(2,1)S(1)}, bf16[1,2048,448]{1,2,0:T(8,128)(2,1)}, u32[]{:S(2)}) copy-start(bf16[1,2048,448]{1,2,0:T(8,128)(2,1)} %param.36) | copy-start | bytes 5505028
  73.7 1.5 %copy-start.4 = (bf16[1,448,2048]{2,1,0:T(8,128)(2,1)S(1)}, bf16[1,448,2048]{2,1,0:T(8,128)(2,1)}, u32[]{:S(2)}) copy-start(bf16[1,448,2048]{2,1,0:T(8,128)(2,1)} %param.37) | copy-start | bytes 5505028
  78.0 6.6 %copy-start.19 = (f32[64,2]{0,1:T(2,128)S(1)}, f32[64,2]{0,1:T(2,128)}, u32[]{:S(2)}) copy-start(f32[64,2]{0,1:T(2,128)} %param.22) | copy-start | bytes 1540
  78.0 2.0 %collective-permute-start.2 = (bf16[256,1024]{1,0:T(8,128)(2,1)S(1)}, bf16[256,1024]{1,0:T(8,128)(2,1)S(1)}, u32[]{:S(2)}, u32[]{:S(2)}) collective-permute-start(bf16[256,1024]{1,0:T(8,128)(2,1)S(1)} %get-tuple-element.14), channel_id=1, source_target_pairs={{0,1},{1,0},{2,3},{3,2},{4,5},{5,4},{6,7},{7,6},{8,9},{9,8},{10,11... | collective-permute-start | bytes 1572872 | tf_op jit(solution)/shard_map/ppermute | solution.py:352
  80.9 14.5 %all-to-all-start.3 = ((bf16[16,16,1024]{2,1,0:T(8,128)(2,1)}), bf16[16,16,1024]{2,1,0:T(8,128)(2,1)S(1)}, u32[]{:S(2)}, u32[]{:S(2)}) async-start(bf16[16,16,1024]{2,1,0:T(8,128)(2,1)} %bitcast.15), calls=%async_computation.3 | async-start | bytes 1048576 | tf_op jit(solution)/shard_map/all_to_all | solution.py:356
  96.4 11.2 %all-to-all-start.4 = ((bf16[8,64,128]{2,1,0:T(8,128)(2,1)}), bf16[8,64,128]{2,1,0:T(8,128)(2,1)S(1)}, u32[]{:S(2)}, u32[]{:S(2)}) async-start(bf16[8,64,128]{2,1,0:T(8,128)(2,1)} %combine.1), calls=%async_computation.4 | async-start | bytes 262144 | tf_op jit(solution)/shard_map/all_to_all | solution.py:356
  99.8 2.2 %copy-start.1 = (f32[64,2,64,64]{3,2,1,0:T(8,128)S(1)}, f32[64,2,64,64]{3,2,1,0:T(8,128)}, u32[]{:S(2)}) copy-start(f32[64,2,64,64]{3,2,1,0:T(8,128)} %param.20) | copy-start | bytes 6291460

commit v2 on v1

--- a/solution.py
+++ b/solution.py
@@ -17,6 +17,10 @@
 VMEM = pltpu.VMEM
 HEAD = 64
 LANES = 128
+
+
+def in_hbm(array):
+    return pltpu.with_memory_space_constraint(array, pltpu.HBM)
 
 
 def head_sums(values):
@@ -36,11 +40,11 @@
     w_decay_hbm,
     w_rate_hbm,
     w_output_hbm,
-    mix_gain_ref,
-    decay_base_ref,
-    rate_base_ref,
-    key_gain_ref,
-    group_gain_ref,
+    mix_gain_hbm,
+    decay_base_hbm,
+    rate_base_hbm,
+    key_gain_hbm,
+    group_gain_hbm,
     keep_ref,
     send_ref,
     removed_ref,
@@ -52,14 +56,32 @@
     weights_ref,
     w_output_ref,
     state_ref,
+    mix_gain_ref,
+    decay_base_ref,
+    rate_base_ref,
+    key_gain_ref,
+    group_gain_ref,
     vectors_ref,
     products_ref,
     sems,
+    small_sems,
 ):
     seqs = tokens_ref.shape[0]
     chunks = state_ref.shape[0]
     chunk_rows = state_ref.shape[1]
     copies = [pltpu.make_async_copy(tokens_hbm, tokens_ref, sems.at[0])]
+    smalls = [
+        pltpu.make_async_copy(source, target, small_sems.at[place])
+        for place, (source, target) in enumerate(
+            (
+                (mix_gain_hbm, mix_gain_ref),
+                (key_gain_hbm, key_gain_ref),
+                (decay_base_hbm, decay_base_ref),
+                (rate_base_hbm, rate_base_ref),
+                (group_gain_hbm, group_gain_ref),
+            )
+        )
+    ]
     sources = (w_key_hbm, w_value_hbm, w_recept_hbm, w_decay_hbm, w_rate_hbm)
     for place, source in enumerate(sources):
         target = weights_ref.at[:, pl.ds(place * LANES, LANES)]
@@ -68,10 +90,15 @@
         source = state_hbm.at[pl.ds(chunk * chunk_rows, chunk_rows)]
         copies.append(pltpu.make_async_copy(source, state_ref.at[chunk], sems.at[6 + chunk]))
     copies.append(pltpu.make_async_copy(w_output_hbm, w_output_ref, sems.at[6 + chunks]))
-    for copy in copies:
+    copies[0].start()
+    for copy in smalls:
         copy.start()
+    for copy in copies[1:]:
+        copy.start()
 
     copies[0].wait()
+    for copy in smalls:
+        copy.wait()
     values = tokens_ref[...].astype(F32)
     mean_square = jnp.mean(values * values, axis=1, keepdims=True)
     normed = (values * lax.rsqrt(mean_square + RMS_EPS) * mix_gain_ref[...]).astype(BF16)
@@ -160,20 +187,26 @@
             small,
             small,
         ),
-        in_specs=[pl.BlockSpec(memory_space=pltpu.SMEM)] + [hbm] * 8 + [vmem] * 5,
+        in_specs=[pl.BlockSpec(memory_space=pltpu.SMEM)] + [hbm] * 13,
         out_specs=(vmem,) * 7,
         scratch_shapes=[
             VMEM((seqs, full_width), BF16),
             VMEM((full_width, 5 * LANES), BF16),
             VMEM((LANES, full_width), BF16),
             VMEM((chunks, chunk_rows, HEAD), F32),
+            VMEM((1, full_width), F32),
+            VMEM((1, LANES), F32),
+            VMEM((1, LANES), F32),
+            VMEM((1, LANES), F32),
+            VMEM((1, LANES), F32),
             VMEM((seqs * 8, LANES), F32),
             VMEM((seqs * 8, LANES), F32),
             pltpu.SemaphoreType.DMA((7 + chunks,)),
+            pltpu.SemaphoreType.DMA((5,)),
         ],
-        compiler_params=pltpu.CompilerParams(vmem_limit_bytes=24 << 20),
+        compiler_params=pltpu.CompilerParams(vmem_limit_bytes=16 << 20),
         name="mix",
-    )(core, tokens, state_rows, *projections, w_output, mix_gain, *vectors)
+    )(core, *map(in_hbm, (tokens, state_rows, *projections, w_output, mix_gain, *vectors)))
 
 
 def update_kernel(
@@ -238,23 +271,57 @@
             flops=2_000_000_000, bytes_accessed=8 << 20, transcendentals=0
         ),
         name="update_state",
-    )(state_rows, removed, unit_rate, decay, key, value)
-
-
-def pick_kernel(pick_ref, rows_ref, out_ref):
-    for z in range(rows_ref.shape[0]):
-        out_ref[:, z * LANES : (z + 1) * LANES] = jnp.dot(
-            pick_ref[...], rows_ref[z], preferred_element_type=F32
-        ).astype(BF16)
-
-
-def pick_rows(pick, rows):
+    )(in_hbm(state_rows), removed, unit_rate, decay, key, value)
+
+
+def stage_kernel(after_ref, gate_hbm, up_hbm, down_hbm, gate_ref, up_ref, down_ref, sems):
+    copies = [
+        pltpu.make_async_copy(source, target, sems.at[place])
+        for place, (source, target) in enumerate(
+            ((gate_hbm, gate_ref), (up_hbm, up_ref), (down_hbm, down_ref))
+        )
+    ]
+    for copy in copies:
+        copy.start()
+    for copy in copies:
+        copy.wait()
+
+
+def stage_weights(after, gate, up, down):
+    weights = (gate, up, down)
     return pl.pallas_call(
-        pick_kernel,
-        out_shape=jax.ShapeDtypeStruct((pick.shape[0], rows.shape[0] * LANES), BF16),
-        compiler_params=pltpu.CompilerParams(vmem_limit_bytes=8 << 20),
-        name="pick_rows",
-    )(pick, rows)
+        stage_kernel,
+        out_shape=tuple(jax.ShapeDtypeStruct(w.shape, w.dtype) for w in weights),
+        in_specs=[pl.BlockSpec(memory_space=pl.ANY)] * 4,
+        out_specs=(pl.BlockSpec(memory_space=VMEM),) * 3,
+        scratch_shapes=[pltpu.SemaphoreType.DMA((3,))],
+        compiler_params=pltpu.CompilerParams(vmem_limit_bytes=1 << 20),
+        name="stage_weights",
+    )(after, *map(in_hbm, weights))
+
+
+def dispatch_kernel(parts_ref, tokens_ref, pick_ref, resid_ref, out_ref):
+    total = tokens_ref[...].astype(F32)
+    mix = parts_ref[0].astype(F32)
+    for z in range(1, parts_ref.shape[0]):
+        mix = mix + parts_ref[z].astype(F32)
+    resid = (total + mix).astype(BF16)
+    resid_ref[...] = resid
+    picked = jnp.dot(pick_ref[...], resid, preferred_element_type=F32).astype(BF16)
+    for z in range(out_ref.shape[0]):
+        out_ref[z] = picked
+
+
+def dispatch_rows(parts, tokens, pick):
+    return pl.pallas_call(
+        dispatch_kernel,
+        out_shape=(
+            jax.ShapeDtypeStruct(tokens.shape, BF16),
+            jax.ShapeDtypeStruct((parts.shape[0], pick.shape[0], LANES), BF16),
+        ),
+        compiler_params=pltpu.CompilerParams(vmem_limit_bytes=4 << 20),
+        name="dispatch_rows",
+    )(parts, tokens, pick)
 
 
 def expert_kernel(
@@ -272,19 +339,17 @@
 ):
     core = core_ref[0]
     full_width = x_ref.shape[1]
-    blocks = full_width // (2 * LANES)
-    own = own_ref[...].astype(F32)
-    other = other_ref[...].astype(F32)
-    square_sum = jnp.sum(own * own, axis=1, keepdims=True) + jnp.sum(
-        other * other, axis=1, keepdims=True
-    )
-    scale = lax.rsqrt(square_sum / full_width + RMS_EPS)
+    blocks = own_ref.shape[0]
+    squares = jnp.zeros(own_ref.shape[1:], F32)
     for z in range(blocks):
-        here = slice(z * LANES, (z + 1) * LANES)
-        cols = pl.ds(pl.multiple_of((2 * z + core) * LANES, LANES), LANES)
-        x_ref[:, cols] = (own[:, here] * scale * gain_ref[:, cols]).astype(BF16)
-        cols = pl.ds(pl.multiple_of((2 * z + 1 - core) * LANES, LANES), LANES)
-        x_ref[:, cols] = (other[:, here] * scale * gain_ref[:, cols]).astype(BF16)
+        for part in (own_ref, other_ref):
+            rows = part[z].astype(F32)
+            squares = squares + rows * rows
+    scale = lax.rsqrt(jnp.sum(squares, axis=1, keepdims=True) / full_width + RMS_EPS)
+    for z in range(blocks):
+        for part, place in ((own_ref, 2 * z + core), (other_ref, 2 * z + 1 - core)):
+            cols = pl.ds(pl.multiple_of(place * LANES, LANES), LANES)
+            x_ref[:, cols] = (part[z].astype(F32) * scale * gain_ref[:, cols]).astype(BF16)
     x = x_ref[...]
     across = (((1,), (1,)), ((), ()))
     gate_act = lax.dot_general(x, gate_ref[...], across, preferred_element_type=F32)
@@ -292,50 +357,45 @@
     hidden = (jax.nn.silu(gate_act) * upward).astype(BF16)
     out_ref[...] = jnp.dot(hidden, down_ref[...], preferred_element_type=F32)
     for z in range(blocks):
-        here = slice(z * LANES, (z + 1) * LANES)
         cols = pl.ds(pl.multiple_of((2 * z + core) * LANES, LANES), LANES)
-        keep_ref[:, here] = out_ref[:, cols]
+        keep_ref[z] = out_ref[:, cols]
         cols = pl.ds(pl.multiple_of((2 * z + 1 - core) * LANES, LANES), LANES)
-        send_ref[:, here] = out_ref[:, cols].astype(BF16)
+        send_ref[z] = out_ref[:, cols].astype(BF16)
 
 
 def run_expert(core, own, other, gain, gate, up, down):
-    rows, half = own.shape
+    rows = own.shape[1]
+    full_width = gate.shape[1]
     vmem = pl.BlockSpec(memory_space=VMEM)
     return pl.pallas_call(
         expert_kernel,
         out_shape=(
-            jax.ShapeDtypeStruct((rows, half), F32),
-            jax.ShapeDtypeStruct((rows, half), BF16),
+            jax.ShapeDtypeStruct(own.shape, F32),
+            jax.ShapeDtypeStruct(own.shape, BF16),
         ),
         in_specs=[pl.BlockSpec(memory_space=pltpu.SMEM)] + [vmem] * 6,
         out_specs=(vmem, vmem),
-        scratch_shapes=[VMEM((rows, 2 * half), BF16), VMEM((rows, 2 * half), F32)],
-        compiler_params=pltpu.CompilerParams(vmem_limit_bytes=24 << 20),
+        scratch_shapes=[VMEM((rows, full_width), BF16), VMEM((rows, full_width), F32)],
+        compiler_params=pltpu.CompilerParams(vmem_limit_bytes=10 << 20),
         name="expert",
     )(core, own, other, gain, gate, up, down)
 
 
-def combine_kernel(weight_ref, rows_ref, out_ref):
-    weight = weight_ref[...]
-    high = weight.astype(BF16)
-    low = (weight - high.astype(F32)).astype(BF16)
-    for z in range(out_ref.shape[0]):
-        rows = rows_ref[:, z * LANES : (z + 1) * LANES]
-        total = jnp.dot(high, rows, preferred_element_type=F32) + jnp.dot(
-            low, rows, preferred_element_type=F32
-        )
-        out_ref[z] = total.astype(BF16)
-
-
-def combine_rows(weight, rows):
-    z_count = rows.shape[1] // LANES
+def combine_kernel(weight_ref, rows_ref, resid_ref, out_ref):
+    rows = rows_ref[0].astype(F32)
+    for z in range(1, rows_ref.shape[0]):
+        rows = rows + rows_ref[z].astype(F32)
+    moe = jnp.dot(weight_ref[...], rows, precision=HIGHEST, preferred_element_type=F32)
+    out_ref[...] = (resid_ref[...].astype(F32) + moe).astype(BF16)
+
+
+def combine_rows(weight, rows, resid):
     return pl.pallas_call(
         combine_kernel,
-        out_shape=jax.ShapeDtypeStruct((z_count, weight.shape[0], LANES), BF16),
-        compiler_params=pltpu.CompilerParams(vmem_limit_bytes=8 << 20),
+        out_shape=jax.ShapeDtypeStruct(resid.shape, BF16),
+        compiler_params=pltpu.CompilerParams(vmem_limit_bytes=4 << 20),
         name="combine",
-    )(weight, rows)
+    )(weight, rows, resid)
 
 
 def slot_numbers(route_rows, expert_count, capacity):
@@ -354,6 +414,12 @@
 
 def exchange(shard, axis):
     return lax.all_to_all(shard, axis, split_axis=0, concat_axis=0, tiled=True)
+
+
+def exchange_rows(shard):
+    groups = lax.axis_size("ep") * lax.axis_size("tp_0")
+    chunks = shard.reshape(groups, -1, 4, LANES)
+    return exchange(chunks, ("tp_0", "ep")).reshape(shard.shape)
 
 
 def local(
@@ -383,9 +449,8 @@
     tp_index = lax.axis_index(TP)
     core = lax.axis_index("tp_1").astype(jnp.int32).reshape(1)
     group_count = lax.axis_size("ep")
-    slot_rows = 16
+    slot_rows = max(2, 3 * routes.shape[1] * seq_rows // (2 * group_count))
     slot_count = group_count * slot_rows
-    half = full_width // 2
 
     state_rows = state.reshape(-1, HEAD)
     keep, send, removed, unit_rate, decay, key, value = mix(
@@ -412,26 +477,19 @@
         axis=1,
     )
 
-    own_vals = lax.dynamic_slice_in_dim(tokens, tp_index * share_cols, share_cols, 1)
-    resid_own = (own_vals.astype(F32) + parts.astype(F32).sum(axis=0)).astype(BF16)
-    resid_half = exchange(jnp.broadcast_to(resid_own, (z_count, *resid_own.shape)), "tp_0")
-    outgoing = pick_rows(pick, resid_half)
-    arrived = exchange(outgoing.reshape(group_count, slot_rows, half), "ep")
-    arrived = arrived.reshape(slot_count, half)
-    keep, send = run_expert(
-        core,
-        arrived,
-        swap(arrived),
-        ffn_gain.reshape(1, -1),
-        jnp.swapaxes(w_gate[0], 0, 1),
-        jnp.swapaxes(w_up[0], 0, 1),
-        w_down[0],
-    )
+    own_tokens = lax.dynamic_slice_in_dim(tokens, tp_index * share_cols, share_cols, 1)
+    gain = ffn_gain.reshape(1, -1)
+    parts, new_state, pick, weight, own_tokens, gain = lax.optimization_barrier(
+        (parts, new_state, pick, weight, own_tokens, gain)
+    )
+    resid_own, outgoing = dispatch_rows(parts, own_tokens, pick)
+    arrived = exchange_rows(outgoing)
+    weights = stage_weights(
+        arrived, jnp.swapaxes(w_gate[0], 0, 1), jnp.swapaxes(w_up[0], 0, 1), w_down[0]
+    )
+    keep, send = run_expert(core, arrived, swap(arrived), gain, *weights)
     pair_sum = (keep + swap(send).astype(F32)).astype(BF16)
-    returned = exchange(pair_sum.reshape(group_count, slot_rows, half), "ep")
-    moe_parts = exchange(combine_rows(weight, returned.reshape(slot_count, half)), "tp_0")
-    moe_own = moe_parts.astype(F32).sum(axis=0)
-    output = (resid_own.astype(F32) + moe_own).astype(BF16)
+    output = combine_rows(weight, exchange_rows(pair_sum), resid_own)
     return (output, new_state.reshape(state.shape))
 
 

time: 110 us -> 90.7 us (0.82); the launches traced: 108 us -> 90.2 us
  blocking collectives: 15.5 us -> 51.9 us
  waiting for transfers between devices: 30.6 us -> 1.74 us
  local copies, waits for them, and re-layouts: 19.1 us -> 1.29 us
  starting transfers between devices: 25.1 us -> 12.8 us
  Pallas kernels: 13.3 us -> 20.2 us
  other arithmetic: 3.7 us -> 1.46 us
    all_to_all x1 -> x2, blocking collectives: 15.5 us -> 51.9 us  [exchange(): return lax.all_to_all(shard, axis, split_axis=0, concat_axis=0, tiled=True)]
    all_to_all x4 -> x1, waiting for transfers between devices: 26.8 us -> 0.03 us  [exchange(): return lax.all_to_all(shard, axis, split_axis=0, concat_axis=0, tiled=True)]
    unnamed x41 -> x7, local copies, waits for them, and re-layouts: 18 us -> 0.11 us
    all_to_all x4 -> x1, starting transfers between devices: 16.8 us -> 6.48 us  [exchange(): return lax.all_to_all(shard, axis, split_axis=0, concat_axis=0, tiled=True)]
    pallas_call x1, Pallas kernels: 4.61 us -> 7.46 us  [update_state(): pl.pallas_call(update_kernel, grid=(steps,), out_shape=jax.ShapeDtypeStru...]
    ppermute x3, waiting for transfers between devices: 3.83 us -> 1.71 us  [swap(): return lax.ppermute(shard, 'tp_1', [(0, 1), (1, 0)])]
    pallas_call x1, Pallas kernels: 4.71 us -> 6.75 us  [mix(): pl.pallas_call(mix_kernel, out_shape=(jax.ShapeDtypeStruct((z_count, seqs...]
    ppermute x3, starting transfers between devices: 8.34 us -> 6.32 us  [swap(): return lax.ppermute(shard, 'tp_1', [(0, 1), (1, 0)])]
  transfers between devices with their start and end apart: 7 -> 4, of which waited for: 7 -> 1; matrix products, arithmetic and copies ran while one was open for 1% -> 2% of each run, Pallas kernels for 4% -> 11%
where the time goes in v2:
time: 90.7 us; the launch traced here: 90.2 us
  blocking collectives  51.9 us (57%)
  Pallas kernels  20.2 us (22%)
  starting transfers between devices  12.8 us (14%)
  waiting for transfers between devices  1.74 us (2%)
  other arithmetic  1.46 us (2%)
  local copies, waits for them, and re-layouts  1.29 us (1%)
    all_to_all x2, blocking collectives, exchange(): return lax.all_to_all(shard, axis, split_axis=0, concat_axis=0, tiled=True)  51.9 us
    pallas_call x1, Pallas kernels, update_state(): pl.pallas_call(update_kernel, grid=(steps,), out_shape=jax.ShapeDtypeStru...  7.46 us
    pallas_call x1, Pallas kernels, mix(): pl.pallas_call(mix_kernel, out_shape=(jax.ShapeDtypeStruct((z_count, seqs...  6.75 us
    all_to_all x1, starting transfers between devices, exchange(): return lax.all_to_all(shard, axis, split_axis=0, concat_axis=0, tiled=True)  6.48 us
    ppermute x3, starting transfers between devices, swap(): return lax.ppermute(shard, 'tp_1', [(0, 1), (1, 0)])  6.32 us
    pallas_call x1, Pallas kernels, stage_weights(): pl.pallas_call(stage_kernel, out_shape=tuple((jax.ShapeDtypeStruct(w.shap...  2.64 us
    pallas_call x1, Pallas kernels, run_expert(): pl.pallas_call(expert_kernel, out_shape=(jax.ShapeDtypeStruct(own.shape,...  2.29 us
  transfers between devices with their start and end apart: 4, of which 1 were waited for; matrix products, arithmetic and copies ran while one was open for 2% of the time, Pallas kernels for 11%

profile of v2, /device:TPU:1, one launch (start us, length us, event | category | flops | bytes accessed | tf_op | source)
XLA Modules:
  0.0 90.2 jit_solution(6001264317644568570)
XLA Ops:
  0.6 0.0 copy-start.2
  0.7 0.0 copy-start.1
  0.7 6.7 %mix.1 = (f32[8,64,128]{2,1,0:T(8,128)S(1)}, bf16[8,64,128]{2,1,0:T(8,128)(2,1)S(1)}, f32[64,128]{1,0:T(8,128)S(1)}, f32[64,128]{1,0:T(8,128)S(1)}, f32[64,128]{...) custom-call(s32[1]{0:T(128)} %bitcast.core_ref, bf16[64,2048]{1,0:T(8,128)(2,1)} %tokens_hbm.1, ...), custom_call_target="tpu_custom_call" | custom-call | tf_op jit(solution)/shard_map/mix/pallas_call | solution.py:179
  7.4 3.3 %collective-permute-start = (bf16[8,64,128]{2,1,0:T(8,128)(2,1)S(1)}, bf16[8,64,128]{2,1,0:T(8,128)(2,1)S(1)}, u32[]{:S(2)}, u32[]{:S(2)}) collective-permute-start(bf16[8,64,128]{2,1,0:T(8,128)(2,1)S(1)} %get-tuple-element.23), channel_id=1, source_target_pairs={{0,1},{1,0},{2,3},{3,2},{4,5},{5,4},{6,7},{7,6},{8,9},{9,8},{10,11... | collective-permute-start | bytes 393224 | tf_op jit(solution)/shard_map/ppermute | solution.py:412
  10.7 0.0 copy-done.1
  10.7 0.1 copy.35
  10.8 0.1 eq.20
  11.0 0.1 fusion.1
  11.1 0.2 reduce_window_sum.11
  11.3 0.2 select_reduce_fusion.1
  11.4 0.1 reduce_sum.30
  11.6 0.1 copy.36
  11.7 0.1 fusion
  11.8 0.1 select_reduce_fusion.weight_ref
  11.9 0.0 collective-permute-done
  11.9 0.7 add_convert_fusion.1
  12.6 6.5 %all-to-all-start = ((bf16[8,64,128]{2,1,0:T(8,128)(2,1)}), bf16[8,64,128]{2,1,0:T(8,128)(2,1)S(1)}, u32[]{:S(2)}, u32[]{:S(2)}) async-start(bf16[8,64,128]{2,1,0:T(8,128)(2,1)} %add_convert_fusion.1), calls=%async_computation | async-start | bytes 262144 | tf_op jit(solution)/shard_map/all_to_all | solution.py:416
  19.0 0.7 constant_dynamic-slice_fusion.tokens_ref
  19.8 0.1 copy.37
  19.9 7.5 %update_state.1 = f32[8192,64]{1,0:T(8,128)} custom-call(f32[8192,64]{1,0:T(8,128)} %bitcast.27, f32[64,128]{1,0:T(8,128)S(1)} %get-tuple-element.24.removed_ref, f32[64,128]{1,0:T(8,128)S(1)} %get-tuple-element.25.unit_rate_ref, f32[64,128]{1,0:T(8,128)S(1)} %get-tuple-element.26.decay_ref, f32[64,128]{1,0:T(8,128)S(1)} %get-tuple-element.27.key_ref, ...), custom_call_target="tpu_custom_call" | custom-call | flops 2000000000 | bytes 8388608 | tf_op jit(solution)/shard_map/update_state/pallas_call | solution.py:262
  27.4 0.0 all-to-all-done.parts_ref
  27.4 0.2 dispatch_rows.1
  27.6 29.7 %all_to_all.15 = bf16[128,3,4,128]{3,2,1,0:T(4,128)(2,1)S(1)} all-to-all(bf16[128,3,4,128]{3,2,1,0:T(4,128)(2,1)S(1)} %bitcast.24), channel_id=1, replica_groups=mesh['ep'=16,'tp_0'=8,'tp_1'=2] {'tp_0','ep'}, dimensions={0} | all-to-all | bytes 786432 | tf_op jit(solution)/shard_map/all_to_all | solution.py:416
  57.3 2.9 %collective-permute-start.1 = (bf16[8,192,128]{2,1,0:T(8,128)(2,1)S(1)}, bf16[8,192,128]{2,1,0:T(8,128)(2,1)S(1)}, u32[]{:S(2)}, u32[]{:S(2)}) collective-permute-start(bf16[8,192,128]{2,1,0:T(8,128)(2,1)S(1)} %bitcast.20), channel_id=1, source_target_pairs={{0,1},{1,0},{2,3},{3,2},{4,5},{5,4},{6,7},{7,6},{8,9},{9,8},{10,11... | collective-permute-start | bytes 1179656 | tf_op jit(solution)/shard_map/ppermute | solution.py:412
  60.2 2.6 %stage_weights.1 = (bf16[448,2048]{1,0:T(8,128)(2,1)S(1)}, bf16[448,2048]{1,0:T(8,128)(2,1)S(1)}, bf16[448,2048]{1,0:T(8,128)(2,1)S(1)}) custom-call(bf16[8,192,128]{2,1,0:T(8,128)(2,1)S(1)} %bitcast.21, bf16[448,2048]{1,0:T(8,128)(2,1)} %bitcast.29, bf16[448,2048]{1,0:T(8,128)(2,1)} %bitcast.30, bf16[448,2048]{1,0:T(8,128)(2,1)} %bitcast.31), custom_call_target="tpu_custom_call" | custom-call | tf_op jit(solution)/shard_map/stage_weights/pallas_call | solution.py:292
  62.9 0.0 collective-permute-done.1.other_ref
  62.9 2.3 %expert.1 = (f32[8,192,128]{2,1,0:T(8,128)S(1)}, bf16[8,192,128]{2,1,0:T(8,128)(2,1)S(1)}) custom-call(s32[1]{0:T(128)} %bitcast.core_ref, bf16[8,192,128]{2,1,0:T(8,128)(2,1)S(1)} %bitcast.22, bf16[8,192,128]{2,1,0:T(8,128)(2,1)S(1)} %collective-permute-done.1.other_ref, f32[1,2048]{1,0:T(1,128)S(1)} %bitcast.25, ...), custom_call_target="tpu_custom_call" | custom-call | tf_op jit(solution)/shard_map/expert/pallas_call | solution.py:370
  65.2 0.1 collective-permute-start.2
  65.3 1.7 %collective-permute-done.2 = bf16[8,192,128]{2,1,0:T(8,128)(2,1)S(1)} collective-permute-done((bf16[8,192,128]{2,1,0:T(8,128)(2,1)S(1)}, bf16[8,192,128]{2,1,0:T(8,128)(2,1)S(1)}, u32[]{:S(2)}, u32[]{:S(2)}) %collective-permute-start.2) | collective-permute-done | bytes 393248 | tf_op jit(solution)/shard_map/ppermute | solution.py:412
  67.0 0.1 add_convert_fusion
  67.1 22.2 %all_to_all.16 = bf16[128,3,4,128]{3,2,1,0:T(4,128)(2,1)S(1)} all-to-all(bf16[128,3,4,128]{3,2,1,0:T(4,128)(2,1)S(1)} %bitcast.32), channel_id=1, replica_groups=mesh['ep'=16,'tp_0'=8,'tp_1'=2] {'tp_0','ep'}, dimensions={0} | all-to-all | bytes 786432 | tf_op jit(solution)/shard_map/all_to_all | solution.py:416
  89.3 0.9 combine.1
  (7 shorter events, 0.1 us)
Async XLA Ops:
  0.6 10.1 %copy-start.2 = (f32[64,2]{0,1:T(2,128)S(1)}, f32[64,2]{0,1:T(2,128)}, u32[]{:S(2)}) copy-start(f32[64,2]{0,1:T(2,128)} %param.22) | copy-start | bytes 1540
  0.7 10.1 %copy-start.1 = (s32[64,2]{0,1:T(2,128)S(1)}, s32[64,2]{0,1:T(2,128)}, u32[]{:S(2)}) copy-start(s32[64,2]{0,1:T(2,128)} %param.21) | copy-start | bytes 1540
  7.4 4.5 %collective-permute-start = (bf16[8,64,128]{2,1,0:T(8,128)(2,1)S(1)}, bf16[8,64,128]{2,1,0:T(8,128)(2,1)S(1)}, u32[]{:S(2)}, u32[]{:S(2)}) collective-permute-start(bf16[8,64,128]{2,1,0:T(8,128)(2,1)S(1)} %get-tuple-element.23), channel_id=1, source_target_pairs={{0,1},{1,0},{2,3},{3,2},{4,5},{5,4},{6,7},{7,6},{8,9},{9,8},{10,11... | collective-permute-start | bytes 393224 | tf_op jit(solution)/shard_map/ppermute | solution.py:412
  12.6 14.8 %all-to-all-start = ((bf16[8,64,128]{2,1,0:T(8,128)(2,1)}), bf16[8,64,128]{2,1,0:T(8,128)(2,1)S(1)}, u32[]{:S(2)}, u32[]{:S(2)}) async-start(bf16[8,64,128]{2,1,0:T(8,128)(2,1)} %add_convert_fusion.1), calls=%async_computation | async-start | bytes 262144 | tf_op jit(solution)/shard_map/all_to_all | solution.py:416
  57.3 5.6 %collective-permute-start.1 = (bf16[8,192,128]{2,1,0:T(8,128)(2,1)S(1)}, bf16[8,192,128]{2,1,0:T(8,128)(2,1)S(1)}, u32[]{:S(2)}, u32[]{:S(2)}) collective-permute-start(bf16[8,192,128]{2,1,0:T(8,128)(2,1)S(1)} %bitcast.20), channel_id=1, source_target_pairs={{0,1},{1,0},{2,3},{3,2},{4,5},{5,4},{6,7},{7,6},{8,9},{9,8},{10,11... | collective-permute-start | bytes 1179656 | tf_op jit(solution)/shard_map/ppermute | solution.py:412
  60.2 2.7 %copy-start = (f32[2048]{0:T(1024)S(1)}, f32[2048]{0:T(1024)}, u32[]{:S(2)}) copy-start(f32[2048]{0:T(1024)} %param.34) | copy-start | bytes 24580
  65.2 1.8 %collective-permute-start.2 = (bf16[8,192,128]{2,1,0:T(8,128)(2,1)S(1)}, bf16[8,192,128]{2,1,0:T(8,128)(2,1)S(1)}, u32[]{:S(2)}, u32[]{:S(2)}) collective-permute-start(bf16[8,192,128]{2,1,0:T(8,128)(2,1)S(1)} %get-tuple-element.39), channel_id=1, source_target_pairs={{0,1},{1,0},{2,3},{3,2},{4,5},{5,4},{6,7},{7,6},{8,9},{9,8},{10,11... | collective-permute-start | bytes 1179656 | tf_op jit(solution)/shard_map/ppermute | solution.py:412

commit v3 on v2

--- a/solution.py
+++ b/solution.py
@@ -30,45 +30,68 @@
     return jnp.dot(values, ones, precision=HIGHEST, preferred_element_type=F32)
 
 
-def mix_kernel(
-    core_ref,
+def route_slots(routes, logits, pick_ref, share_ref):
+    slots, seqs = pick_ref.shape
+    experts = lax.axis_size("ep")
+    first, second = routes[0:1, :], routes[1:2, :]
+    expert = lax.broadcasted_iota(jnp.int32, (experts, seqs), 0)
+    named = [(expert == choice).astype(F32) for choice in (first, second)]
+    earlier = lax.broadcasted_iota(jnp.int32, (seqs, seqs), 0) < lax.broadcasted_iota(
+        jnp.int32, (seqs, seqs), 1
+    )
+    counts = jnp.dot(
+        (named[0] + named[1]).astype(BF16),
+        earlier.astype(F32).astype(BF16),
+        preferred_element_type=F32,
+    )
+    exps = jnp.exp(logits)
+    total = exps[0:1, :] + exps[1:2, :]
+    slot = lax.broadcasted_iota(jnp.int32, (slots, seqs), 0)
+    picked = jnp.zeros((slots, seqs), F32)
+    shares = jnp.zeros((slots, seqs), F32)
+    for k, choice in enumerate((first, second)):
+        placed = jnp.sum(named[k] * counts, axis=0, keepdims=True).astype(jnp.int32)
+        here = slot == choice * (slots // experts) + placed
+        picked = jnp.where(here, 1.0, picked)
+        shares = jnp.where(here, exps[k : k + 1, :] / total, shares)
+    pick_ref[...] = picked.astype(BF16)
+    share_ref[...] = shares
+
+
+def project_kernel(
     tokens_hbm,
-    state_hbm,
     w_recept_hbm,
     w_key_hbm,
     w_value_hbm,
     w_decay_hbm,
     w_rate_hbm,
-    w_output_hbm,
     mix_gain_hbm,
     decay_base_hbm,
     rate_base_hbm,
     key_gain_hbm,
-    group_gain_hbm,
-    keep_ref,
-    send_ref,
-    removed_ref,
+    routes_hbm,
+    logits_hbm,
+    vectors_ref,
+    recept_ref,
     unit_rate_ref,
     decay_ref,
     key_ref,
     value_ref,
+    own_ref,
+    pick_ref,
+    share_ref,
     tokens_ref,
     weights_ref,
-    w_output_ref,
-    state_ref,
     mix_gain_ref,
     decay_base_ref,
     rate_base_ref,
     key_gain_ref,
-    group_gain_ref,
-    vectors_ref,
-    products_ref,
+    routes_ref,
+    logits_ref,
     sems,
     small_sems,
 ):
     seqs = tokens_ref.shape[0]
-    chunks = state_ref.shape[0]
-    chunk_rows = state_ref.shape[1]
     copies = [pltpu.make_async_copy(tokens_hbm, tokens_ref, sems.at[0])]
     smalls = [
         pltpu.make_async_copy(source, target, small_sems.at[place])
@@ -78,7 +101,8 @@
                 (key_gain_hbm, key_gain_ref),
                 (decay_base_hbm, decay_base_ref),
                 (rate_base_hbm, rate_base_ref),
-                (group_gain_hbm, group_gain_ref),
+                (routes_hbm, routes_ref),
+                (logits_hbm, logits_ref),
             )
         )
     ]
@@ -86,19 +110,17 @@
     for place, source in enumerate(sources):
         target = weights_ref.at[:, pl.ds(place * LANES, LANES)]
         copies.append(pltpu.make_async_copy(source, target, sems.at[1 + place]))
-    for chunk in range(chunks):
-        source = state_hbm.at[pl.ds(chunk * chunk_rows, chunk_rows)]
-        copies.append(pltpu.make_async_copy(source, state_ref.at[chunk], sems.at[6 + chunk]))
-    copies.append(pltpu.make_async_copy(w_output_hbm, w_output_ref, sems.at[6 + chunks]))
     copies[0].start()
     for copy in smalls:
         copy.start()
     for copy in copies[1:]:
         copy.start()
 
-    copies[0].wait()
     for copy in smalls:
         copy.wait()
+    route_slots(routes_ref[...], logits_ref[...], pick_ref, share_ref)
+    copies[0].wait()
+    own_ref[...] = tokens_ref[:, pl.ds(pl.multiple_of(lax.axis_index(TP) * LANES, LANES), LANES)]
     values = tokens_ref[...].astype(F32)
     mean_square = jnp.mean(values * values, axis=1, keepdims=True)
     normed = (values * lax.rsqrt(mean_square + RMS_EPS) * mix_gain_ref[...]).astype(BF16)
@@ -111,37 +133,83 @@
 
     key_value = project(0, 2)
     keys_now = key_value[:, :LANES]
-    values_now = key_value[:, LANES:]
+    key_ref[...] = keys_now
+    value_ref[...] = key_value[:, LANES:]
+    scaled = keys_now * key_gain_ref[...]
+    unit_key = scaled * lax.rsqrt(head_sums(scaled * scaled) + UNIT_EPS)
+    vectors_ref[...] = jnp.zeros_like(vectors_ref)
+    vectors_ref[pl.ds(0, seqs, stride=8), :] = unit_key
+    vectors_ref[pl.ds(2, seqs, stride=8), :] = pltpu.roll(unit_key, HEAD, 1)
     recept_decay = project(2, 2)
     recept = recept_decay[:, :LANES]
+    recept_ref[...] = recept
     decay_pre = recept_decay[:, LANES:] + decay_base_ref[...]
+    decay_now = jnp.exp(-jnp.exp(-jax.nn.softplus(-decay_pre) - 0.5))
+    decay_ref[...] = decay_now
+    decayed_recept = decay_now * recept
+    vectors_ref[pl.ds(1, seqs, stride=8), :] = decayed_recept
+    vectors_ref[pl.ds(3, seqs, stride=8), :] = pltpu.roll(decayed_recept, HEAD, 1)
     rate_pre = project(4, 1) + rate_base_ref[...]
-    decay_now = jnp.exp(-jnp.exp(-jax.nn.softplus(-decay_pre) - 0.5))
-    rate_now = jax.nn.sigmoid(rate_pre)
-    scaled = keys_now * key_gain_ref[...]
-    unit_key = scaled * lax.rsqrt(head_sums(scaled * scaled) + UNIT_EPS)
-    unit_rate = unit_key * rate_now
-    decayed_recept = decay_now * recept
-    unit_rate_ref[...] = unit_rate
-    decay_ref[...] = decay_now
-    key_ref[...] = keys_now
-    value_ref[...] = values_now
-
-    vectors_ref[...] = jnp.zeros_like(vectors_ref)
-    vectors_ref[pl.ds(0, seqs, stride=8), :] = unit_key
-    vectors_ref[pl.ds(1, seqs, stride=8), :] = decayed_recept
-    vectors_ref[pl.ds(2, seqs, stride=8), :] = pltpu.roll(unit_key, HEAD, 1)
-    vectors_ref[pl.ds(3, seqs, stride=8), :] = pltpu.roll(decayed_recept, HEAD, 1)
-    per_chunk = chunk_rows // LANES
-    for chunk in range(chunks):
-        copies[6 + chunk].wait()
-        for inner in range(per_chunk):
-            seq = chunk * per_chunk + inner
-            left = vectors_ref[seq * 8 : seq * 8 + 8, :HEAD].astype(BF16)
-            right = state_ref[chunk, inner * LANES : (inner + 1) * LANES, :].astype(BF16)
-            products_ref[seq * 8 : seq * 8 + 8, :] = lax.dot_general(
-                left, right, (((1,), (1,)), ((), ())), preferred_element_type=F32
-            )
+    unit_rate_ref[...] = unit_key * jax.nn.sigmoid(rate_pre)
+
+
+def project_heads(tokens, projections, mix_gain, vectors, routes, logits, slots):
+    seqs, full_width = tokens.shape
+    small = jax.ShapeDtypeStruct((seqs, LANES), F32)
+    hbm = pl.BlockSpec(memory_space=pl.ANY)
+    vmem = pl.BlockSpec(memory_space=VMEM)
+    return pl.pallas_call(
+        project_kernel,
+        out_shape=(jax.ShapeDtypeStruct((seqs * 8, LANES), F32),)
+        + (small,) * 5
+        + (
+            jax.ShapeDtypeStruct((seqs, LANES), BF16),
+            jax.ShapeDtypeStruct((slots, seqs), BF16),
+            jax.ShapeDtypeStruct((slots, seqs), F32),
+        ),
+        in_specs=[hbm] * 12,
+        out_specs=(vmem,) * 9,
+        scratch_shapes=[
+            VMEM((seqs, full_width), BF16),
+            VMEM((full_width, 5 * LANES), BF16),
+            VMEM((1, full_width), F32),
+            VMEM((1, LANES), F32),
+            VMEM((1, LANES), F32),
+            VMEM((1, LANES), F32),
+            VMEM(routes.shape, jnp.int32),
+            VMEM(logits.shape, F32),
+            pltpu.SemaphoreType.DMA((6,)),
+            pltpu.SemaphoreType.DMA((6,)),
+        ],
+        compiler_params=pltpu.CompilerParams(vmem_limit_bytes=12 << 20),
+        cost_estimate=pl.CostEstimate(
+            flops=3_000_000_000, bytes_accessed=6 << 20, transcendentals=0
+        ),
+        name="project_heads",
+    )(*map(in_hbm, (tokens, *projections, mix_gain, *vectors, routes, logits)))
+
+
+def mix_kernel(
+    state_ref,
+    vectors_ref,
+    recept_ref,
+    unit_rate_ref,
+    key_ref,
+    value_ref,
+    w_output_ref,
+    group_gain_ref,
+    keep_ref,
+    send_ref,
+    removed_ref,
+    products_ref,
+):
+    seqs = recept_ref.shape[0]
+    for seq in range(seqs):
+        left = vectors_ref[seq * 8 : seq * 8 + 8, :HEAD].astype(BF16)
+        right = state_ref[seq * LANES : (seq + 1) * LANES, :].astype(BF16)
+        products_ref[seq * 8 : seq * 8 + 8, :] = lax.dot_general(
+            left, right, (((1,), (1,)), ((), ())), preferred_element_type=F32
+        )
     first_head = lax.broadcasted_iota(jnp.int32, (seqs, LANES), 1) < HEAD
     removed = jnp.where(
         first_head,
@@ -154,14 +222,16 @@
         products_ref[pl.ds(3, seqs, stride=8), :],
     )
     removed_ref[...] = removed
+    recept = recept_ref[...]
     readout = (
-        faded - removed * head_sums(unit_rate * recept) + values_now * head_sums(keys_now * recept)
+        faded
+        - removed * head_sums(unit_rate_ref[...] * recept)
+        + value_ref[...] * head_sums(key_ref[...] * recept)
     )
     centred = readout - head_sums(readout) * (1.0 / HEAD)
     spread = head_sums(centred * centred) * (1.0 / HEAD)
     mixed = (centred * lax.rsqrt(spread + GROUP_EPS) * group_gain_ref[...]).astype(BF16)
-    copies[6 + chunks].wait()
-    core = core_ref[0]
+    core = lax.axis_index("tp_1")
     for z in range(keep_ref.shape[0]):
         own = w_output_ref[:, pl.ds(pl.multiple_of((2 * z + core) * LANES, LANES), LANES)]
         keep_ref[z] = jnp.dot(mixed, own, preferred_element_type=F32)
@@ -169,44 +239,22 @@
         send_ref[z] = jnp.dot(mixed, other, preferred_element_type=F32).astype(BF16)
 
 
-def mix(core, tokens, state_rows, projections, w_output, mix_gain, vectors, z_count):
-    seqs, full_width = tokens.shape
-    chunks = 4
-    chunk_rows = state_rows.shape[0] // chunks
-    small = jax.ShapeDtypeStruct((seqs, LANES), F32)
-    hbm = pl.BlockSpec(memory_space=pl.ANY)
+def mix(state_rows, vectors, recept, unit_rate, key, value, w_output, group_gain, z_count):
+    seqs = recept.shape[0]
     vmem = pl.BlockSpec(memory_space=VMEM)
     return pl.pallas_call(
         mix_kernel,
         out_shape=(
             jax.ShapeDtypeStruct((z_count, seqs, LANES), F32),
             jax.ShapeDtypeStruct((z_count, seqs, LANES), BF16),
-            small,
-            small,
-            small,
-            small,
-            small,
-        ),
-        in_specs=[pl.BlockSpec(memory_space=pltpu.SMEM)] + [hbm] * 13,
-        out_specs=(vmem,) * 7,
-        scratch_shapes=[
-            VMEM((seqs, full_width), BF16),
-            VMEM((full_width, 5 * LANES), BF16),
-            VMEM((LANES, full_width), BF16),
-            VMEM((chunks, chunk_rows, HEAD), F32),
-            VMEM((1, full_width), F32),
-            VMEM((1, LANES), F32),
-            VMEM((1, LANES), F32),
-            VMEM((1, LANES), F32),
-            VMEM((1, LANES), F32),
-            VMEM((seqs * 8, LANES), F32),
-            VMEM((seqs * 8, LANES), F32),
-            pltpu.SemaphoreType.DMA((7 + chunks,)),
-            pltpu.SemaphoreType.DMA((5,)),
-        ],
-        compiler_params=pltpu.CompilerParams(vmem_limit_bytes=16 << 20),
+            jax.ShapeDtypeStruct((seqs, LANES), F32),
+        ),
+        in_specs=[vmem] * 8,
+        out_specs=(vmem,) * 3,
+        scratch_shapes=[VMEM((seqs * 8, LANES), F32)],
+        compiler_params=pltpu.CompilerParams(vmem_limit_bytes=12 << 20),
         name="mix",
-    )(core, *map(in_hbm, (tokens, state_rows, *projections, w_output, mix_gain, *vectors)))
+    )(state_rows, vectors, recept, unit_rate, key, value, w_output, group_gain)
 
 
 def update_kernel(
@@ -274,11 +322,11 @@
     )(in_hbm(state_rows), removed, unit_rate, decay, key, value)
 
 
-def stage_kernel(after_ref, gate_hbm, up_hbm, down_hbm, gate_ref, up_ref, down_ref, sems):
+def stage_kernel(after_ref, gate_hbm, up_hbm, gate_ref, up_ref, sems):
     copies = [
         pltpu.make_async_copy(source, target, sems.at[place])
         for place, (source, target) in enumerate(
-            ((gate_hbm, gate_ref), (up_hbm, up_ref), (down_hbm, down_ref))
+            ((gate_hbm, gate_ref), (up_hbm, up_ref))
         )
     ]
     for copy in copies:
@@ -287,14 +335,14 @@
         copy.wait()
 
 
-def stage_weights(after, gate, up, down):
-    weights = (gate, up, down)
+def stage_weights(after, gate, up):
+    weights = (gate, up)
     return pl.pallas_call(
         stage_kernel,
         out_shape=tuple(jax.ShapeDtypeStruct(w.shape, w.dtype) for w in weights),
-        in_specs=[pl.BlockSpec(memory_space=pl.ANY)] * 4,
-        out_specs=(pl.BlockSpec(memory_space=VMEM),) * 3,
-        scratch_shapes=[pltpu.SemaphoreType.DMA((3,))],
+        in_specs=[pl.BlockSpec(memory_space=pl.ANY)] * 3,
+        out_specs=(pl.BlockSpec(memory_space=VMEM),) * 2,
+        scratch_shapes=[pltpu.SemaphoreType.DMA((2,))],
         compiler_params=pltpu.CompilerParams(vmem_limit_bytes=1 << 20),
         name="stage_weights",
     )(after, *map(in_hbm, weights))
@@ -325,19 +373,22 @@
 
 
 def expert_kernel(
-    core_ref,
     own_ref,
     other_ref,
     gain_ref,
     gate_ref,
     up_ref,
-    down_ref,
+    down_hbm,
     keep_ref,
     send_ref,
     x_ref,
     out_ref,
+    down_ref,
+    sem,
 ):
-    core = core_ref[0]
+    down_copy = pltpu.make_async_copy(down_hbm, down_ref, sem)
+    down_copy.start()
+    core = lax.axis_index("tp_1")
     full_width = x_ref.shape[1]
     blocks = own_ref.shape[0]
     squares = jnp.zeros(own_ref.shape[1:], F32)
@@ -355,6 +406,7 @@
     gate_act = lax.dot_general(x, gate_ref[...], across, preferred_element_type=F32)
     upward = lax.dot_general(x, up_ref[...], across, preferred_element_type=F32)
     hidden = (jax.nn.silu(gate_act) * upward).astype(BF16)
+    down_copy.wait()
     out_ref[...] = jnp.dot(hidden, down_ref[...], preferred_element_type=F32)
     for z in range(blocks):
         cols = pl.ds(pl.multiple_of((2 * z + core) * LANES, LANES), LANES)
@@ -363,7 +415,7 @@
         send_ref[z] = out_ref[:, cols].astype(BF16)
 
 
-def run_expert(core, own, other, gain, gate, up, down):
+def run_expert(own, other, gain, gate, up, down):
     rows = own.shape[1]
     full_width = gate.shape[1]
     vmem = pl.BlockSpec(memory_space=VMEM)
@@ -373,39 +425,40 @@
             jax.ShapeDtypeStruct(own.shape, F32),
             jax.ShapeDtypeStruct(own.shape, BF16),
         ),
-        in_specs=[pl.BlockSpec(memory_space=pltpu.SMEM)] + [vmem] * 6,
+        in_specs=[vmem] * 5 + [pl.BlockSpec(memory_space=pl.ANY)],
         out_specs=(vmem, vmem),
-        scratch_shapes=[VMEM((rows, full_width), BF16), VMEM((rows, full_width), F32)],
+        scratch_shapes=[
+            VMEM((rows, full_width), BF16),
+            VMEM((rows, full_width), F32),
+            VMEM(down.shape, BF16),
+            pltpu.SemaphoreType.DMA(()),
+        ],
         compiler_params=pltpu.CompilerParams(vmem_limit_bytes=10 << 20),
         name="expert",
-    )(core, own, other, gain, gate, up, down)
-
-
-def combine_kernel(weight_ref, rows_ref, resid_ref, out_ref):
+    )(own, other, gain, gate, up, in_hbm(down))
+
+
+def combine_kernel(share_ref, rows_ref, resid_ref, out_ref):
     rows = rows_ref[0].astype(F32)
     for z in range(1, rows_ref.shape[0]):
         rows = rows + rows_ref[z].astype(F32)
-    moe = jnp.dot(weight_ref[...], rows, precision=HIGHEST, preferred_element_type=F32)
+    moe = lax.dot_general(
+        share_ref[...],
+        rows,
+        (((0,), (0,)), ((), ())),
+        precision=HIGHEST,
+        preferred_element_type=F32,
+    )
     out_ref[...] = (resid_ref[...].astype(F32) + moe).astype(BF16)
 
 
-def combine_rows(weight, rows, resid):
+def combine_rows(share, rows, resid):
     return pl.pallas_call(
         combine_kernel,
         out_shape=jax.ShapeDtypeStruct(resid.shape, BF16),
         compiler_params=pltpu.CompilerParams(vmem_limit_bytes=4 << 20),
         name="combine",
-    )(weight, rows, resid)
-
-
-def slot_numbers(route_rows, expert_count, capacity):
-    flat_routes = route_rows.reshape(-1)
-    one_hot = (flat_routes[:, None] == jnp.arange(expert_count, dtype=jnp.int32)[None, :]).astype(
-        jnp.int32
-    )
-    earlier = jnp.cumsum(one_hot, axis=0) - one_hot
-    placed = jnp.sum(earlier * one_hot, axis=1)
-    return (flat_routes * capacity + placed).reshape(route_rows.shape)
+    )(share, rows, resid)
 
 
 def swap(shard):
@@ -443,53 +496,46 @@
     w_up,
     w_down,
 ):
-    seq_rows, full_width = tokens.shape
+    seq_rows = tokens.shape[0]
     z_count = lax.axis_size("tp_0")
-    share_cols = full_width // lax.axis_size(TP)
-    tp_index = lax.axis_index(TP)
-    core = lax.axis_index("tp_1").astype(jnp.int32).reshape(1)
     group_count = lax.axis_size("ep")
     slot_rows = max(2, 3 * routes.shape[1] * seq_rows // (2 * group_count))
     slot_count = group_count * slot_rows
 
     state_rows = state.reshape(-1, HEAD)
-    keep, send, removed, unit_rate, decay, key, value = mix(
-        core,
+    vectors, recept, unit_rate, decay, key, value, own_tokens, pick, share = project_heads(
         tokens,
+        (w_recept, w_key, w_value, w_decay, w_rate),
+        mix_gain.reshape(1, -1),
+        [v.reshape(1, -1) for v in (decay_base, rate_base, key_gain)],
+        routes.T,
+        route_logits.T,
+        slot_count,
+    )
+    keep, send, removed = mix(
         state_rows,
-        (w_recept, w_key, w_value, w_decay, w_rate),
+        vectors,
+        recept,
+        unit_rate,
+        key,
+        value,
         w_output,
-        mix_gain.reshape(1, -1),
-        [v.reshape(1, -1) for v in (decay_base, rate_base, key_gain, group_gain)],
+        group_gain.reshape(1, -1),
         z_count,
     )
     pair_sum = (keep + swap(send).astype(F32)).astype(BF16)
     parts = exchange(pair_sum, "tp_0")
     new_state = update_state(state_rows, removed, unit_rate, decay, key, value)
 
-    slot_ids = slot_numbers(routes, group_count, slot_rows)
-    slot_range = jnp.arange(slot_count, dtype=jnp.int32)
-    pick = jnp.any(slot_ids[None, :, :] == slot_range[:, None, None], axis=2).astype(BF16)
-    route_exp = jnp.exp(route_logits)
-    route_weight = route_exp / jnp.sum(route_exp, axis=1, keepdims=True)
-    weight = jnp.sum(
-        jnp.where(slot_ids[:, :, None] == slot_range[None, None, :], route_weight[:, :, None], 0.0),
-        axis=1,
-    )
-
-    own_tokens = lax.dynamic_slice_in_dim(tokens, tp_index * share_cols, share_cols, 1)
-    gain = ffn_gain.reshape(1, -1)
-    parts, new_state, pick, weight, own_tokens, gain = lax.optimization_barrier(
-        (parts, new_state, pick, weight, own_tokens, gain)
-    )
     resid_own, outgoing = dispatch_rows(parts, own_tokens, pick)
     arrived = exchange_rows(outgoing)
     weights = stage_weights(
-        arrived, jnp.swapaxes(w_gate[0], 0, 1), jnp.swapaxes(w_up[0], 0, 1), w_down[0]
-    )
-    keep, send = run_expert(core, arrived, swap(arrived), gain, *weights)
+        arrived, jnp.swapaxes(w_gate[0], 0, 1), jnp.swapaxes(w_up[0], 0, 1)
+    )
+    gain = ffn_gain.reshape(1, -1)
+    keep, send = run_expert(arrived, swap(arrived), gain, *weights, w_down[0])
     pair_sum = (keep + swap(send).astype(F32)).astype(BF16)
-    output = combine_rows(weight, exchange_rows(pair_sum), resid_own)
+    output = combine_rows(share, exchange_rows(pair_sum), resid_own)
     return (output, new_state.reshape(state.shape))
 
 

time: 90.7 us -> 85.9 us (0.947)
  blocking collectives: 51.9 us -> 39.2 us
  waiting for transfers between devices: 1.74 us -> 11.9 us
  local copies, waits for them, and re-layouts: 1.29 us -> 0.02 us
    all_to_all x2, blocking collectives: 51.9 us -> 39.2 us  [exchange(): return lax.all_to_all(shard, axis, split_axis=0, concat_axis=0, tiled=True)]
    all_to_all x1, waiting for transfers between devices: 0.03 us -> 9.24 us  [exchange(): return lax.all_to_all(shard, axis, split_axis=0, concat_axis=0, tiled=True)]
    pallas_call x1, Pallas kernels: 6.75 us -> 2 us  [mix(): pl.pallas_call(mix_kernel, out_shape=(jax.ShapeDtypeStruct((z_count, seqs...]
    pallas_call x0 -> x1, Pallas kernels: none -> 3.57 us  [project_heads(): pl.pallas_call(project_kernel, out_shape=(jax.ShapeDtypeStruct((seqs * 8,...]
    pallas_call x1, Pallas kernels: 2.29 us -> 3.63 us  [run_expert(): pl.pallas_call(expert_kernel, out_shape=(jax.ShapeDtypeStruct(own.shape,...]
    ppermute x3, waiting for transfers between devices: 1.71 us -> 2.7 us  [swap(): return lax.ppermute(shard, 'tp_1', [(0, 1), (1, 0)])]
  transfers between devices with their start and end apart: 4 -> 4, of which waited for: 1 -> 3; matrix products, arithmetic and copies ran while one was open for 2% -> 0% of each run, Pallas kernels for 11% -> 11%
where the time goes in v3:
time: 85.9 us; the launch traced here: 85.5 us
  blocking collectives  39.2 us (46%)
  Pallas kernels  19.8 us (23%)
  starting transfers between devices  13 us (15%)
  waiting for transfers between devices  11.9 us (14%)
    all_to_all x2, blocking collectives, exchange(): return lax.all_to_all(shard, axis, split_axis=0, concat_axis=0, tiled=True)  39.2 us
    all_to_all x1, waiting for transfers between devices, exchange(): return lax.all_to_all(shard, axis, split_axis=0, concat_axis=0, tiled=True)  9.24 us
    pallas_call x1, Pallas kernels, update_state(): pl.pallas_call(update_kernel, grid=(steps,), out_shape=jax.ShapeDtypeStru...  7.47 us
    ppermute x3, starting transfers between devices, swap(): return lax.ppermute(shard, 'tp_1', [(0, 1), (1, 0)])  6.82 us
    all_to_all x1, starting transfers between devices, exchange(): return lax.all_to_all(shard, axis, split_axis=0, concat_axis=0, tiled=True)  6.16 us
    pallas_call x1, Pallas kernels, run_expert(): pl.pallas_call(expert_kernel, out_shape=(jax.ShapeDtypeStruct(own.shape,...  3.63 us
    pallas_call x1, Pallas kernels, project_heads(): pl.pallas_call(project_kernel, out_shape=(jax.ShapeDtypeStruct((seqs * 8,...  3.57 us
    ppermute x3, waiting for transfers between devices, swap(): return lax.ppermute(shard, 'tp_1', [(0, 1), (1, 0)])  2.7 us
  transfers between devices with their start and end apart: 4, of which 3 were waited for; matrix products, arithmetic and copies ran while one was open for 0% of the time, Pallas kernels for 11%

profile of v3, /device:TPU:1, one launch (start us, length us, event | category | flops | bytes accessed | tf_op | source)
XLA Modules:
  0.0 85.5 jit_solution(10533185276340157278)
XLA Ops:
  0.6 0.0 copy-start
  0.6 0.0 copy-start.1
  0.7 0.0 copy-start.3
  0.7 3.6 %project_heads.1 = (f32[512,128]{1,0:T(8,128)S(1)}, f32[64,128]{1,0:T(8,128)S(1)}, f32[64,128]{1,0:T(8,128)S(1)}, f32[64,128]{1,0:T(8,128)S(1)}, f32[64,128]{1,0...) custom-call(bf16[64,2048]{1,0:T(8,128)(2,1)} %tokens_hbm.1, ...), custom_call_target="tpu_custom_call" | custom-call | flops 3000000000 | bytes 6291456 | tf_op jit(solution)/shard_map/project_heads/pallas_call | solution.py:161
  4.2 0.0 copy-done
  4.3 0.0 copy-done.1
  4.3 0.0 copy-done.3
  4.3 2.0 %mix.1 = (f32[8,64,128]{2,1,0:T(8,128)S(1)}, bf16[8,64,128]{2,1,0:T(8,128)(2,1)S(1)}, f32[64,128]{1,0:T(8,128)S(1)}) custom-call(f32[8192,64]{1,0:T(8,128)S(1)} %bitcast.22, f32[512,128]{1,0:T(8,128)S(1)} %get-tuple-element.21.vectors_ref, f32[64,128]{1,0:T(8,128)S(1)} %get-tuple-element.22.recept_ref, f32[64,128]{1,0:T(8,128)S(1)} %get-tuple-element.23.unit_rate_ref, ...), custom_call_target="tpu_custom_call" | custom-call | tf_op jit(solution)/shard_map/mix/pallas_call | solution.py:245
  6.3 3.3 %collective-permute-start = (bf16[8,64,128]{2,1,0:T(8,128)(2,1)S(1)}, bf16[8,64,128]{2,1,0:T(8,128)(2,1)S(1)}, u32[]{:S(2)}, u32[]{:S(2)}) collective-permute-start(bf16[8,64,128]{2,1,0:T(8,128)(2,1)S(1)} %get-tuple-element.27), channel_id=1, source_target_pairs={{0,1},{1,0},{2,3},{3,2},{4,5},{5,4},{6,7},{7,6},{8,9},{9,8},{10,11... | collective-permute-start | bytes 393224 | tf_op jit(solution)/shard_map/ppermute | solution.py:465
  9.6 1.0 %collective-permute-done = bf16[8,64,128]{2,1,0:T(8,128)(2,1)S(1)} collective-permute-done((bf16[8,64,128]{2,1,0:T(8,128)(2,1)S(1)}, bf16[8,64,128]{2,1,0:T(8,128)(2,1)S(1)}, u32[]{:S(2)}, u32[]{:S(2)}) %collective-permute-start) | collective-permute-done | bytes 131104 | tf_op jit(solution)/shard_map/ppermute | solution.py:465
  10.6 14.2 %all_to_all.15.parts_ref = bf16[8,64,128]{2,1,0:T(8,128)(2,1)S(1)} all-to-all(bf16[8,64,128]{2,1,0:T(8,128)(2,1)S(1)} %add_convert_fusion.1), channel_id=1, replica_groups=mesh['ep'=16,'tp_0'=8,'tp_1'=2] {'tp_0'}, dimensions={0} | all-to-all | bytes 262144 | tf_op jit(solution)/shard_map/all_to_all | solution.py:469
  24.8 0.2 dispatch_rows.1
  24.9 25.0 %all_to_all.16 = bf16[128,3,4,128]{3,2,1,0:T(4,128)(2,1)S(1)} all-to-all(bf16[128,3,4,128]{3,2,1,0:T(4,128)(2,1)S(1)} %bitcast.27), channel_id=1, replica_groups=mesh['ep'=16,'tp_0'=8,'tp_1'=2] {'tp_0','ep'}, dimensions={0} | all-to-all | bytes 786432 | tf_op jit(solution)/shard_map/all_to_all | solution.py:469
  49.9 3.4 %collective-permute-start.1 = (bf16[8,192,128]{2,1,0:T(8,128)(2,1)S(1)}, bf16[8,192,128]{2,1,0:T(8,128)(2,1)S(1)}, u32[]{:S(2)}, u32[]{:S(2)}) collective-permute-start(bf16[8,192,128]{2,1,0:T(8,128)(2,1)S(1)} %bitcast.23), channel_id=1, source_target_pairs={{0,1},{1,0},{2,3},{3,2},{4,5},{5,4},{6,7},{7,6},{8,9},{9,8},{10,11... | collective-permute-start | bytes 1179656 | tf_op jit(solution)/shard_map/ppermute | solution.py:465
  53.4 0.0 copy-start.2
  53.4 2.1 %stage_weights.1 = (bf16[448,2048]{1,0:T(8,128)(2,1)S(1)}, bf16[448,2048]{1,0:T(8,128)(2,1)S(1)}) custom-call(bf16[8,192,128]{2,1,0:T(8,128)(2,1)S(1)} %bitcast.24, bf16[448,2048]{1,0:T(8,128)(2,1)} %bitcast.31, bf16[448,2048]{1,0:T(8,128)(2,1)} %bitcast.32), custom_call_target="tpu_custom_call" | custom-call | tf_op jit(solution)/shard_map/stage_weights/pallas_call | solution.py:340
  55.5 0.0 collective-permute-done.1.other_ref
  55.5 0.0 copy-done.2
  55.5 3.6 %expert.1 = (f32[8,192,128]{2,1,0:T(8,128)S(1)}, bf16[8,192,128]{2,1,0:T(8,128)(2,1)S(1)}) custom-call(bf16[8,192,128]{2,1,0:T(8,128)(2,1)S(1)} %bitcast.25, bf16[8,192,128]{2,1,0:T(8,128)(2,1)S(1)} %collective-permute-done.1.other_ref, f32[1,2048]{1,0:T(1,128)S(1)} %bitcast.28, bf16[448,2048]{1,0:T(8,128)(2,1)S(1)} %get-tuple-element.31.gate_ref, ...), custom_call_target="tpu_custom_call" | custom-call | tf_op jit(solution)/shard_map/expert/pallas_call | solution.py:422
  59.1 0.1 collective-permute-start.2
  59.2 1.7 %collective-permute-done.2 = bf16[8,192,128]{2,1,0:T(8,128)(2,1)S(1)} collective-permute-done((bf16[8,192,128]{2,1,0:T(8,128)(2,1)S(1)}, bf16[8,192,128]{2,1,0:T(8,128)(2,1)S(1)}, u32[]{:S(2)}, u32[]{:S(2)}) %collective-permute-start.2) | collective-permute-done | bytes 393248 | tf_op jit(solution)/shard_map/ppermute | solution.py:465
  60.9 0.8 add_convert_fusion
  61.8 6.2 %all-to-all-start.2 = ((bf16[128,3,4,128]{3,2,1,0:T(4,128)(2,1)}), bf16[128,3,4,128]{3,2,1,0:T(4,128)(2,1)S(1)}, u32[]{:S(2)}, u32[]{:S(2)}) async-start(bf16[128,3,4,128]{3,2,1,0:T(4,128)(2,1)} %bitcast.16), calls=%async_computation.2 | async-start | bytes 786432 | tf_op jit(solution)/shard_map/all_to_all | solution.py:469
  67.9 7.5 %update_state.1 = f32[8192,64]{1,0:T(8,128)} custom-call(f32[8192,64]{1,0:T(8,128)} %bitcast.21, f32[64,128]{1,0:T(8,128)S(1)} %get-tuple-element.36.removed_ref, f32[64,128]{1,0:T(8,128)S(1)} %get-tuple-element.23.unit_rate_ref, f32[64,128]{1,0:T(8,128)S(1)} %get-tuple-element.37.decay_ref, f32[64,128]{1,0:T(8,128)S(1)} %get-tuple-element.24.key_ref, ...), custom_call_target="tpu_custom_call" | custom-call | flops 2000000000 | bytes 8388608 | tf_op jit(solution)/shard_map/update_state/pallas_call | solution.py:310
  75.4 9.2 %all-to-all-done.2 = bf16[128,3,4,128]{3,2,1,0:T(4,128)(2,1)S(1)} async-done(((bf16[128,3,4,128]{3,2,1,0:T(4,128)(2,1)}), bf16[128,3,4,128]{3,2,1,0:T(4,128)(2,1)S(1)}, u32[]{:S(2)}, u32[]{:S(2)}) %all-to-all-start.2) | async-done | bytes 393248 | tf_op jit(solution)/shard_map/all_to_all | solution.py:469
  84.6 0.9 %combine.1 = bf16[64,128]{1,0:T(8,128)(2,1)} custom-call(f32[192,64]{1,0:T(8,128)S(1)} %get-tuple-element.20.share_ref, bf16[8,192,128]{2,1,0:T(8,128)(2,1)S(1)} %bitcast.26, bf16[64,128]{1,0:T(8,128)(2,1)S(1)} %get-tuple-element.35.resid_ref), custom_call_target="tpu_custom_call" | custom-call | tf_op jit(solution)/shard_map/combine/pallas_call | solution.py:456
  (1 shorter events, 0.0 us)
Async XLA Ops:
  0.6 3.6 %copy-start = (f32[64,2,64,64]{3,2,1,0:T(8,128)S(1)}, f32[64,2,64,64]{3,2,1,0:T(8,128)}, u32[]{:S(2)}) copy-start(f32[64,2,64,64]{3,2,1,0:T(8,128)} %param.20) | copy-start | bytes 6291460
  0.6 3.6 %copy-start.1 = (bf16[128,2048]{1,0:T(8,128)(2,1)S(1)}, bf16[128,2048]{1,0:T(8,128)(2,1)}, u32[]{:S(2)}) copy-start(bf16[128,2048]{1,0:T(8,128)(2,1)} %w_output_ref.1) | copy-start | bytes 1572868
  0.7 3.6 %copy-start.3 = (f32[128]{0:T(128)S(1)}, f32[128]{0:T(128)}, u32[]{:S(2)}) copy-start(f32[128]{0:T(128)} %param.32) | copy-start | bytes 1540
  6.3 4.3 %collective-permute-start = (bf16[8,64,128]{2,1,0:T(8,128)(2,1)S(1)}, bf16[8,64,128]{2,1,0:T(8,128)(2,1)S(1)}, u32[]{:S(2)}, u32[]{:S(2)}) collective-permute-start(bf16[8,64,128]{2,1,0:T(8,128)(2,1)S(1)} %get-tuple-element.27), channel_id=1, source_target_pairs={{0,1},{1,0},{2,3},{3,2},{4,5},{5,4},{6,7},{7,6},{8,9},{9,8},{10,11... | collective-permute-start | bytes 393224 | tf_op jit(solution)/shard_map/ppermute | solution.py:465
  49.9 5.5 %collective-permute-start.1 = (bf16[8,192,128]{2,1,0:T(8,128)(2,1)S(1)}, bf16[8,192,128]{2,1,0:T(8,128)(2,1)S(1)}, u32[]{:S(2)}, u32[]{:S(2)}) collective-permute-start(bf16[8,192,128]{2,1,0:T(8,128)(2,1)S(1)} %bitcast.23), channel_id=1, source_target_pairs={{0,1},{1,0},{2,3},{3,2},{4,5},{5,4},{6,7},{7,6},{8,9},{9,8},{10,11... | collective-permute-start | bytes 1179656 | tf_op jit(solution)/shard_map/ppermute | solution.py:465
  53.4 2.1 %copy-start.2 = (f32[2048]{0:T(1024)S(1)}, f32[2048]{0:T(1024)}, u32[]{:S(2)}) copy-start(f32[2048]{0:T(1024)} %param.34) | copy-start | bytes 24580
  59.1 1.8 %collective-permute-start.2 = (bf16[8,192,128]{2,1,0:T(8,128)(2,1)S(1)}, bf16[8,192,128]{2,1,0:T(8,128)(2,1)S(1)}, u32[]{:S(2)}, u32[]{:S(2)}) collective-permute-start(bf16[8,192,128]{2,1,0:T(8,128)(2,1)S(1)} %get-tuple-element.34), channel_id=1, source_target_pairs={{0,1},{1,0},{2,3},{3,2},{4,5},{5,4},{6,7},{7,6},{8,9},{9,8},{10,11... | collective-permute-start | bytes 1179656 | tf_op jit(solution)/shard_map/ppermute | solution.py:465
  61.8 22.9 %all-to-all-start.2 = ((bf16[128,3,4,128]{3,2,1,0:T(4,128)(2,1)}), bf16[128,3,4,128]{3,2,1,0:T(4,128)(2,1)S(1)}, u32[]{:S(2)}, u32[]{:S(2)}) async-start(bf16[128,3,4,128]{3,2,1,0:T(4,128)(2,1)} %bitcast.16), calls=%async_computation.2 | async-start | bytes 786432 | tf_op jit(solution)/shard_map/all_to_all | solution.py:469

commit v4 on v3

--- a/solution.py
+++ b/solution.py
@@ -322,32 +322,6 @@
     )(in_hbm(state_rows), removed, unit_rate, decay, key, value)
 
 
-def stage_kernel(after_ref, gate_hbm, up_hbm, gate_ref, up_ref, sems):
-    copies = [
-        pltpu.make_async_copy(source, target, sems.at[place])
-        for place, (source, target) in enumerate(
-            ((gate_hbm, gate_ref), (up_hbm, up_ref))
-        )
-    ]
-    for copy in copies:
-        copy.start()
-    for copy in copies:
-        copy.wait()
-
-
-def stage_weights(after, gate, up):
-    weights = (gate, up)
-    return pl.pallas_call(
-        stage_kernel,
-        out_shape=tuple(jax.ShapeDtypeStruct(w.shape, w.dtype) for w in weights),
-        in_specs=[pl.BlockSpec(memory_space=pl.ANY)] * 3,
-        out_specs=(pl.BlockSpec(memory_space=VMEM),) * 2,
-        scratch_shapes=[pltpu.SemaphoreType.DMA((2,))],
-        compiler_params=pltpu.CompilerParams(vmem_limit_bytes=1 << 20),
-        name="stage_weights",
-    )(after, *map(in_hbm, weights))
-
-
 def dispatch_kernel(parts_ref, tokens_ref, pick_ref, resid_ref, out_ref):
     total = tokens_ref[...].astype(F32)
     mix = parts_ref[0].astype(F32)
@@ -378,16 +352,12 @@
     gain_ref,
     gate_ref,
     up_ref,
-    down_hbm,
+    down_ref,
     keep_ref,
     send_ref,
     x_ref,
     out_ref,
-    down_ref,
-    sem,
 ):
-    down_copy = pltpu.make_async_copy(down_hbm, down_ref, sem)
-    down_copy.start()
     core = lax.axis_index("tp_1")
     full_width = x_ref.shape[1]
     blocks = own_ref.shape[0]
@@ -406,7 +376,6 @@
     gate_act = lax.dot_general(x, gate_ref[...], across, preferred_element_type=F32)
     upward = lax.dot_general(x, up_ref[...], across, preferred_element_type=F32)
     hidden = (jax.nn.silu(gate_act) * upward).astype(BF16)
-    down_copy.wait()
     out_ref[...] = jnp.dot(hidden, down_ref[...], preferred_element_type=F32)
     for z in range(blocks):
         cols = pl.ds(pl.multiple_of((2 * z + core) * LANES, LANES), LANES)
@@ -425,17 +394,12 @@
             jax.ShapeDtypeStruct(own.shape, F32),
             jax.ShapeDtypeStruct(own.shape, BF16),
         ),
-        in_specs=[vmem] * 5 + [pl.BlockSpec(memory_space=pl.ANY)],
+        in_specs=[vmem] * 6,
         out_specs=(vmem, vmem),
-        scratch_shapes=[
-            VMEM((rows, full_width), BF16),
-            VMEM((rows, full_width), F32),
-            VMEM(down.shape, BF16),
-            pltpu.SemaphoreType.DMA(()),
-        ],
+        scratch_shapes=[VMEM((rows, full_width), BF16), VMEM((rows, full_width), F32)],
         compiler_params=pltpu.CompilerParams(vmem_limit_bytes=10 << 20),
         name="expert",
-    )(own, other, gain, gate, up, in_hbm(down))
+    )(own, other, gain, gate, up, down)
 
 
 def combine_kernel(share_ref, rows_ref, resid_ref, out_ref):
@@ -529,11 +493,15 @@
 
     resid_own, outgoing = dispatch_rows(parts, own_tokens, pick)
     arrived = exchange_rows(outgoing)
-    weights = stage_weights(
-        arrived, jnp.swapaxes(w_gate[0], 0, 1), jnp.swapaxes(w_up[0], 0, 1)
-    )
     gain = ffn_gain.reshape(1, -1)
-    keep, send = run_expert(arrived, swap(arrived), gain, *weights, w_down[0])
+    keep, send = run_expert(
+        arrived,
+        swap(arrived),
+        gain,
+        jnp.swapaxes(w_gate[0], 0, 1),
+        jnp.swapaxes(w_up[0], 0, 1),
+        w_down[0],
+    )
     pair_sum = (keep + swap(send).astype(F32)).astype(BF16)
     output = combine_rows(share, exchange_rows(pair_sum), resid_own)
     return (output, new_state.reshape(state.shape))

time: 85.9 us -> 83.7 us (0.974)
  Pallas kernels: 19.8 us -> 16.3 us
  waiting for transfers between devices: 11.9 us -> 12.8 us
    pallas_call x1 -> x0, Pallas kernels: 2.08 us -> none  [stage_weights(): pl.pallas_call(stage_kernel, out_shape=tuple((jax.ShapeDtypeStruct(w.shap...]
    pallas_call x1, Pallas kernels: 3.63 us -> 2.23 us  [run_expert(): pl.pallas_call(expert_kernel, out_shape=(jax.ShapeDtypeStruct(own.shape,...]
    ppermute x3, waiting for transfers between devices: 2.7 us -> 3.69 us  [swap(): return lax.ppermute(shard, 'tp_1', [(0, 1), (1, 0)])]
  transfers between devices with their start and end apart: 4 -> 4, of which waited for: 3 -> 4; matrix products, arithmetic and copies ran while one was open for 0% -> 0% of each run, Pallas kernels for 11% -> 9%
where the time goes in v4:
time: 83.7 us; the launch traced here: 83.3 us
  blocking collectives  39.2 us (47%)
  Pallas kernels  16.3 us (19%)
  starting transfers between devices  13.3 us (16%)
  waiting for transfers between devices  12.8 us (15%)
  other arithmetic  0.86 us (1%)
    all_to_all x2, blocking collectives, exchange(): return lax.all_to_all(shard, axis, split_axis=0, concat_axis=0, tiled=True)  39.2 us
    all_to_all x1, waiting for transfers between devices, exchange(): return lax.all_to_all(shard, axis, split_axis=0, concat_axis=0, tiled=True)  9.09 us
    pallas_call x1, Pallas kernels, update_state(): pl.pallas_call(update_kernel, grid=(steps,), out_shape=jax.ShapeDtypeStru...  7.47 us
    ppermute x3, starting transfers between devices, swap(): return lax.ppermute(shard, 'tp_1', [(0, 1), (1, 0)])  7.19 us
    all_to_all x1, starting transfers between devices, exchange(): return lax.all_to_all(shard, axis, split_axis=0, concat_axis=0, tiled=True)  6.16 us
    ppermute x3, waiting for transfers between devices, swap(): return lax.ppermute(shard, 'tp_1', [(0, 1), (1, 0)])  3.69 us
    pallas_call x1, Pallas kernels, project_heads(): pl.pallas_call(project_kernel, out_shape=(jax.ShapeDtypeStruct((seqs * 8,...  3.57 us
    pallas_call x1, Pallas kernels, run_expert(): pl.pallas_call(expert_kernel, out_shape=(jax.ShapeDtypeStruct(own.shape,...  2.23 us
  transfers between devices with their start and end apart: 4, of which 4 were waited for; matrix products, arithmetic and copies ran while one was open for 0% of the time, Pallas kernels for 9%

profile of v4, /device:TPU:1, one launch (start us, length us, event | category | flops | bytes accessed | tf_op | source)
XLA Modules:
  0.0 83.3 jit_solution(10141459478521841913)
XLA Ops:
  0.6 0.0 copy-start
  0.6 0.0 copy-start.4
  0.7 0.0 copy-start.6
  0.7 3.6 %project_heads.1 = (f32[512,128]{1,0:T(8,128)S(1)}, f32[64,128]{1,0:T(8,128)S(1)}, f32[64,128]{1,0:T(8,128)S(1)}, f32[64,128]{1,0:T(8,128)S(1)}, f32[64,128]{1,0...) custom-call(bf16[64,2048]{1,0:T(8,128)(2,1)} %tokens_hbm.1, ...), custom_call_target="tpu_custom_call" | custom-call | flops 3000000000 | bytes 6291456 | tf_op jit(solution)/shard_map/project_heads/pallas_call | solution.py:161
  4.2 0.0 copy-done
  4.3 0.0 copy-done.4
  4.3 0.0 copy-done.6
  4.3 0.0 copy-start.1
  4.3 0.0 copy-start.2
  4.3 0.0 copy-start.3
  4.3 0.0 copy-start.5
  4.3 2.0 %mix.1 = (f32[8,64,128]{2,1,0:T(8,128)S(1)}, bf16[8,64,128]{2,1,0:T(8,128)(2,1)S(1)}, f32[64,128]{1,0:T(8,128)S(1)}) custom-call(f32[8192,64]{1,0:T(8,128)S(1)} %bitcast.22, f32[512,128]{1,0:T(8,128)S(1)} %get-tuple-element.19.vectors_ref, f32[64,128]{1,0:T(8,128)S(1)} %get-tuple-element.20.recept_ref, f32[64,128]{1,0:T(8,128)S(1)} %get-tuple-element.21.unit_rate_ref, ...), custom_call_target="tpu_custom_call" | custom-call | tf_op jit(solution)/shard_map/mix/pallas_call | solution.py:245
  6.3 3.3 %collective-permute-start = (bf16[8,64,128]{2,1,0:T(8,128)(2,1)S(1)}, bf16[8,64,128]{2,1,0:T(8,128)(2,1)S(1)}, u32[]{:S(2)}, u32[]{:S(2)}) collective-permute-start(bf16[8,64,128]{2,1,0:T(8,128)(2,1)S(1)} %get-tuple-element.25), channel_id=1, source_target_pairs={{0,1},{1,0},{2,3},{3,2},{4,5},{5,4},{6,7},{7,6},{8,9},{9,8},{10,11... | collective-permute-start | bytes 393224 | tf_op jit(solution)/shard_map/ppermute | solution.py:429
  9.6 1.0 %collective-permute-done = bf16[8,64,128]{2,1,0:T(8,128)(2,1)S(1)} collective-permute-done((bf16[8,64,128]{2,1,0:T(8,128)(2,1)S(1)}, bf16[8,64,128]{2,1,0:T(8,128)(2,1)S(1)}, u32[]{:S(2)}, u32[]{:S(2)}) %collective-permute-start) | collective-permute-done | bytes 131104 | tf_op jit(solution)/shard_map/ppermute | solution.py:429
  10.6 14.2 %all_to_all.15.parts_ref = bf16[8,64,128]{2,1,0:T(8,128)(2,1)S(1)} all-to-all(bf16[8,64,128]{2,1,0:T(8,128)(2,1)S(1)} %add_convert_fusion.1), channel_id=1, replica_groups=mesh['ep'=16,'tp_0'=8,'tp_1'=2] {'tp_0'}, dimensions={0} | all-to-all | bytes 262144 | tf_op jit(solution)/shard_map/all_to_all | solution.py:433
  24.8 0.2 dispatch_rows.1
  25.0 25.0 %all_to_all.16 = bf16[128,3,4,128]{3,2,1,0:T(4,128)(2,1)S(1)} all-to-all(bf16[128,3,4,128]{3,2,1,0:T(4,128)(2,1)S(1)} %bitcast.29), channel_id=1, replica_groups=mesh['ep'=16,'tp_0'=8,'tp_1'=2] {'tp_0','ep'}, dimensions={0} | all-to-all | bytes 786432 | tf_op jit(solution)/shard_map/all_to_all | solution.py:433
  50.0 3.4 %collective-permute-start.1 = (bf16[8,192,128]{2,1,0:T(8,128)(2,1)S(1)}, bf16[8,192,128]{2,1,0:T(8,128)(2,1)S(1)}, u32[]{:S(2)}, u32[]{:S(2)}) collective-permute-start(bf16[8,192,128]{2,1,0:T(8,128)(2,1)S(1)} %bitcast.27), channel_id=1, source_target_pairs={{0,1},{1,0},{2,3},{3,2},{4,5},{5,4},{6,7},{7,6},{8,9},{9,8},{10,11... | collective-permute-start | bytes 1179656 | tf_op jit(solution)/shard_map/ppermute | solution.py:429
  53.4 1.3 %collective-permute-done.1.other_ref = bf16[8,192,128]{2,1,0:T(8,128)(2,1)S(1)} collective-permute-done((bf16[8,192,128]{2,1,0:T(8,128)(2,1)S(1)}, bf16[8,192,128]{2,1,0:T(8,128)(2,1)S(1)}, u32[]{:S(2)}, u32[]{:S(2)}) %collective-permute-start.1) | collective-permute-done | bytes 393248 | tf_op jit(solution)/shard_map/ppermute | solution.py:429
  54.8 0.0 copy-done.1
  54.8 0.0 copy-done.2
  54.8 0.0 copy-done.3
  54.8 0.0 copy-done.5
  54.8 2.2 %expert.1 = (f32[8,192,128]{2,1,0:T(8,128)S(1)}, bf16[8,192,128]{2,1,0:T(8,128)(2,1)S(1)}) custom-call(bf16[8,192,128]{2,1,0:T(8,128)(2,1)S(1)} %bitcast.28, bf16[8,192,128]{2,1,0:T(8,128)(2,1)S(1)} %collective-permute-done.1.other_ref, f32[1,2048]{1,0:T(1,128)S(1)} %bitcast.30, bf16[448,2048]{1,0:T(8,128)(2,1)S(1)} %bitcast.23, ...), custom_call_target="tpu_custom_call" | custom-call | tf_op jit(solution)/shard_map/expert/pallas_call | solution.py:391
  57.0 0.5 collective-permute-start.2
  57.5 1.3 %collective-permute-done.2 = bf16[8,192,128]{2,1,0:T(8,128)(2,1)S(1)} collective-permute-done((bf16[8,192,128]{2,1,0:T(8,128)(2,1)S(1)}, bf16[8,192,128]{2,1,0:T(8,128)(2,1)S(1)}, u32[]{:S(2)}, u32[]{:S(2)}) %collective-permute-start.2) | collective-permute-done | bytes 393248 | tf_op jit(solution)/shard_map/ppermute | solution.py:429
  58.8 0.8 add_convert_fusion
  59.7 6.2 %all-to-all-start.2 = ((bf16[128,3,4,128]{3,2,1,0:T(4,128)(2,1)}), bf16[128,3,4,128]{3,2,1,0:T(4,128)(2,1)S(1)}, u32[]{:S(2)}, u32[]{:S(2)}) async-start(bf16[128,3,4,128]{3,2,1,0:T(4,128)(2,1)} %bitcast.16), calls=%async_computation.2 | async-start | bytes 786432 | tf_op jit(solution)/shard_map/all_to_all | solution.py:433
  65.8 7.5 %update_state.1 = f32[8192,64]{1,0:T(8,128)} custom-call(f32[8192,64]{1,0:T(8,128)} %bitcast.21, f32[64,128]{1,0:T(8,128)S(1)} %get-tuple-element.32.removed_ref, f32[64,128]{1,0:T(8,128)S(1)} %get-tuple-element.21.unit_rate_ref, f32[64,128]{1,0:T(8,128)S(1)} %get-tuple-element.33.decay_ref, f32[64,128]{1,0:T(8,128)S(1)} %get-tuple-element.22.key_ref, ...), custom_call_target="tpu_custom_call" | custom-call | flops 2000000000 | bytes 8388608 | tf_op jit(solution)/shard_map/update_state/pallas_call | solution.py:310
  73.3 9.1 %all-to-all-done.2 = bf16[128,3,4,128]{3,2,1,0:T(4,128)(2,1)S(1)} async-done(((bf16[128,3,4,128]{3,2,1,0:T(4,128)(2,1)}), bf16[128,3,4,128]{3,2,1,0:T(4,128)(2,1)S(1)}, u32[]{:S(2)}, u32[]{:S(2)}) %all-to-all-start.2) | async-done | bytes 393248 | tf_op jit(solution)/shard_map/all_to_all | solution.py:433
  82.4 0.9 %combine.1 = bf16[64,128]{1,0:T(8,128)(2,1)} custom-call(f32[192,64]{1,0:T(8,128)S(1)} %get-tuple-element.18.share_ref, bf16[8,192,128]{2,1,0:T(8,128)(2,1)S(1)} %bitcast.26, bf16[64,128]{1,0:T(8,128)(2,1)S(1)} %get-tuple-element.31.resid_ref), custom_call_target="tpu_custom_call" | custom-call | tf_op jit(solution)/shard_map/combine/pallas_call | solution.py:420
  (1 shorter events, 0.0 us)
Async XLA Ops:
  0.6 3.6 %copy-start = (f32[64,2,64,64]{3,2,1,0:T(8,128)S(1)}, f32[64,2,64,64]{3,2,1,0:T(8,128)}, u32[]{:S(2)}) copy-start(f32[64,2,64,64]{3,2,1,0:T(8,128)} %param.20) | copy-start | bytes 6291460
  0.6 3.6 %copy-start.4 = (bf16[128,2048]{1,0:T(8,128)(2,1)S(1)}, bf16[128,2048]{1,0:T(8,128)(2,1)}, u32[]{:S(2)}) copy-start(bf16[128,2048]{1,0:T(8,128)(2,1)} %w_output_ref.1) | copy-start | bytes 1572868
  0.7 3.6 %copy-start.6 = (f32[128]{0:T(128)S(1)}, f32[128]{0:T(128)}, u32[]{:S(2)}) copy-start(f32[128]{0:T(128)} %param.32) | copy-start | bytes 1540
  4.3 50.5 %copy-start.1 = (bf16[1,2048,448]{1,2,0:T(8,128)(2,1)S(1)}, bf16[1,2048,448]{1,2,0:T(8,128)(2,1)}, u32[]{:S(2)}) copy-start(bf16[1,2048,448]{1,2,0:T(8,128)(2,1)} %param.35) | copy-start | bytes 5505028
  4.3 50.5 %copy-start.2 = (bf16[1,2048,448]{1,2,0:T(8,128)(2,1)S(1)}, bf16[1,2048,448]{1,2,0:T(8,128)(2,1)}, u32[]{:S(2)}) copy-start(bf16[1,2048,448]{1,2,0:T(8,128)(2,1)} %param.36) | copy-start | bytes 5505028
  4.3 50.5 %copy-start.3 = (bf16[1,448,2048]{2,1,0:T(8,128)(2,1)S(1)}, bf16[1,448,2048]{2,1,0:T(8,128)(2,1)}, u32[]{:S(2)}) copy-start(bf16[1,448,2048]{2,1,0:T(8,128)(2,1)} %param.37) | copy-start | bytes 5505028
  4.3 50.5 %copy-start.5 = (f32[2048]{0:T(1024)S(1)}, f32[2048]{0:T(1024)}, u32[]{:S(2)}) copy-start(f32[2048]{0:T(1024)} %param.34) | copy-start | bytes 24580
  6.3 4.3 %collective-permute-start = (bf16[8,64,128]{2,1,0:T(8,128)(2,1)S(1)}, bf16[8,64,128]{2,1,0:T(8,128)(2,1)S(1)}, u32[]{:S(2)}, u32[]{:S(2)}) collective-permute-start(bf16[8,64,128]{2,1,0:T(8,128)(2,1)S(1)} %get-tuple-element.25), channel_id=1, source_target_pairs={{0,1},{1,0},{2,3},{3,2},{4,5},{5,4},{6,7},{7,6},{8,9},{9,8},{10,11... | collective-permute-start | bytes 393224 | tf_op jit(solution)/shard_map/ppermute | solution.py:429
  50.0 4.8 %collective-permute-start.1 = (bf16[8,192,128]{2,1,0:T(8,128)(2,1)S(1)}, bf16[8,192,128]{2,1,0:T(8,128)(2,1)S(1)}, u32[]{:S(2)}, u32[]{:S(2)}) collective-permute-start(bf16[8,192,128]{2,1,0:T(8,128)(2,1)S(1)} %bitcast.27), channel_id=1, source_target_pairs={{0,1},{1,0},{2,3},{3,2},{4,5},{5,4},{6,7},{7,6},{8,9},{9,8},{10,11... | collective-permute-start | bytes 1179656 | tf_op jit(solution)/shard_map/ppermute | solution.py:429
  57.0 1.8 %collective-permute-start.2 = (bf16[8,192,128]{2,1,0:T(8,128)(2,1)S(1)}, bf16[8,192,128]{2,1,0:T(8,128)(2,1)S(1)}, u32[]{:S(2)}, u32[]{:S(2)}) collective-permute-start(bf16[8,192,128]{2,1,0:T(8,128)(2,1)S(1)} %get-tuple-element.30), channel_id=1, source_target_pairs={{0,1},{1,0},{2,3},{3,2},{4,5},{5,4},{6,7},{7,6},{8,9},{9,8},{10,11... | collective-permute-start | bytes 1179656 | tf_op jit(solution)/shard_map/ppermute | solution.py:429
  59.7 22.7 %all-to-all-start.2 = ((bf16[128,3,4,128]{3,2,1,0:T(4,128)(2,1)}), bf16[128,3,4,128]{3,2,1,0:T(4,128)(2,1)S(1)}, u32[]{:S(2)}, u32[]{:S(2)}) async-start(bf16[128,3,4,128]{3,2,1,0:T(4,128)(2,1)} %bitcast.16), calls=%async_computation.2 | async-start | bytes 786432 | tf_op jit(solution)/shard_map/all_to_all | solution.py:433

commit v5 on v4

--- a/solution.py
+++ b/solution.py
@@ -346,60 +346,122 @@
     )(parts, tokens, pick)
 
 
-def expert_kernel(
-    own_ref,
-    other_ref,
+ACROSS = (((1,), (1,)), ((), ()))
+
+
+def core_columns(ref, core):
+    blocks = ref.shape[1] // (2 * LANES)
+    return jnp.concatenate(
+        [
+            ref[:, pl.ds(pl.multiple_of((2 * z + core) * LANES, LANES), LANES)]
+            for z in range(blocks)
+        ],
+        axis=1,
+    )
+
+
+def half_products(rows_ref, gain_ref, gate_ref, up_ref, core):
+    gain = core_columns(gain_ref, core)
+    squares = jnp.zeros(rows_ref.shape[1:], F32)
+    parts = []
+    for z in range(rows_ref.shape[0]):
+        rows = rows_ref[z].astype(F32)
+        squares = squares + rows * rows
+        parts.append((rows * gain[:, z * LANES : (z + 1) * LANES]).astype(BF16))
+    x = jnp.concatenate(parts, axis=1)
+    gate = lax.dot_general(
+        x, core_columns(gate_ref, core), ACROSS, preferred_element_type=F32
+    )
+    upward = lax.dot_general(
+        x, core_columns(up_ref, core), ACROSS, preferred_element_type=F32
+    )
+    return squares, gate, upward
+
+
+def own_half_kernel(rows_ref, gain_ref, gate_ref, up_ref, squares_ref, gate_out, up_out):
+    core = lax.axis_index("tp_1")
+    squares_ref[...], gate_out[...], up_out[...] = half_products(
+        rows_ref, gain_ref, gate_ref, up_ref, core
+    )
+
+
+def other_half_kernel(
+    rows_ref,
     gain_ref,
     gate_ref,
     up_ref,
     down_ref,
-    keep_ref,
+    squares_ref,
+    gate_part_ref,
+    up_part_ref,
+    hidden_ref,
     send_ref,
-    x_ref,
-    out_ref,
 ):
+    other = 1 - lax.axis_index("tp_1")
+    squares, gate, upward = half_products(rows_ref, gain_ref, gate_ref, up_ref, other)
+    square_sum = jnp.sum(squares + squares_ref[...], axis=1, keepdims=True)
+    scale = lax.rsqrt(square_sum / gate_ref.shape[1] + RMS_EPS)
+    gate = (gate + gate_part_ref[...]) * scale
+    upward = (upward + up_part_ref[...]) * scale
+    hidden = (jax.nn.silu(gate) * upward).astype(BF16)
+    hidden_ref[...] = hidden
+    out = jnp.dot(hidden, core_columns(down_ref, other), preferred_element_type=F32)
+    for z in range(send_ref.shape[0]):
+        send_ref[z] = out[:, z * LANES : (z + 1) * LANES].astype(BF16)
+
+
+def keep_kernel(hidden_ref, down_ref, keep_ref):
     core = lax.axis_index("tp_1")
-    full_width = x_ref.shape[1]
-    blocks = own_ref.shape[0]
-    squares = jnp.zeros(own_ref.shape[1:], F32)
-    for z in range(blocks):
-        for part in (own_ref, other_ref):
-            rows = part[z].astype(F32)
-            squares = squares + rows * rows
-    scale = lax.rsqrt(jnp.sum(squares, axis=1, keepdims=True) / full_width + RMS_EPS)
-    for z in range(blocks):
-        for part, place in ((own_ref, 2 * z + core), (other_ref, 2 * z + 1 - core)):
-            cols = pl.ds(pl.multiple_of(place * LANES, LANES), LANES)
-            x_ref[:, cols] = (part[z].astype(F32) * scale * gain_ref[:, cols]).astype(BF16)
-    x = x_ref[...]
-    across = (((1,), (1,)), ((), ()))
-    gate_act = lax.dot_general(x, gate_ref[...], across, preferred_element_type=F32)
-    upward = lax.dot_general(x, up_ref[...], across, preferred_element_type=F32)
-    hidden = (jax.nn.silu(gate_act) * upward).astype(BF16)
-    out_ref[...] = jnp.dot(hidden, down_ref[...], preferred_element_type=F32)
-    for z in range(blocks):
-        cols = pl.ds(pl.multiple_of((2 * z + core) * LANES, LANES), LANES)
-        keep_ref[z] = out_ref[:, cols]
-        cols = pl.ds(pl.multiple_of((2 * z + 1 - core) * LANES, LANES), LANES)
-        send_ref[z] = out_ref[:, cols].astype(BF16)
-
-
-def run_expert(own, other, gain, gate, up, down):
+    out = jnp.dot(hidden_ref[...], core_columns(down_ref, core), preferred_element_type=F32)
+    for z in range(keep_ref.shape[0]):
+        keep_ref[z] = out[:, z * LANES : (z + 1) * LANES]
+
+
+def run_expert(own, gain, gate, up, down):
     rows = own.shape[1]
-    full_width = gate.shape[1]
     vmem = pl.BlockSpec(memory_space=VMEM)
-    return pl.pallas_call(
-        expert_kernel,
+    part = jax.ShapeDtypeStruct((rows, gate.shape[0]), F32)
+
+    def call(body, name, *operands, out_shape):
+        return pl.pallas_call(
+            body,
+            out_shape=out_shape,
+            in_specs=[vmem] * len(operands),
+            out_specs=jax.tree.map(lambda _: vmem, out_shape),
+            compiler_params=pltpu.CompilerParams(vmem_limit_bytes=10 << 20),
+            name=name,
+        )(*operands)
+
+    other = swap(own)
+    partial = call(
+        own_half_kernel,
+        "own_half",
+        own,
+        gain,
+        gate,
+        up,
+        out_shape=(jax.ShapeDtypeStruct((rows, LANES), F32), part, part),
+    )
+    other, partial = lax.optimization_barrier((other, partial))
+    hidden, send = call(
+        other_half_kernel,
+        "other_half",
+        other,
+        gain,
+        gate,
+        up,
+        down,
+        *partial,
         out_shape=(
-            jax.ShapeDtypeStruct(own.shape, F32),
+            jax.ShapeDtypeStruct((rows, gate.shape[0]), BF16),
             jax.ShapeDtypeStruct(own.shape, BF16),
         ),
-        in_specs=[vmem] * 6,
-        out_specs=(vmem, vmem),
-        scratch_shapes=[VMEM((rows, full_width), BF16), VMEM((rows, full_width), F32)],
-        compiler_params=pltpu.CompilerParams(vmem_limit_bytes=10 << 20),
-        name="expert",
-    )(own, other, gain, gate, up, down)
+    )
+    received = swap(send)
+    keep = call(
+        keep_kernel, "keep_half", hidden, down, out_shape=jax.ShapeDtypeStruct(own.shape, F32)
+    )
+    return (keep + received.astype(F32)).astype(BF16)
 
 
 def combine_kernel(share_ref, rows_ref, resid_ref, out_ref):
@@ -494,15 +556,13 @@
     resid_own, outgoing = dispatch_rows(parts, own_tokens, pick)
     arrived = exchange_rows(outgoing)
     gain = ffn_gain.reshape(1, -1)
-    keep, send = run_expert(
+    pair_sum = run_expert(
         arrived,
-        swap(arrived),
         gain,
         jnp.swapaxes(w_gate[0], 0, 1),
         jnp.swapaxes(w_up[0], 0, 1),
         w_down[0],
     )
-    pair_sum = (keep + swap(send).astype(F32)).astype(BF16)
     output = combine_rows(share, exchange_rows(pair_sum), resid_own)
     return (output, new_state.reshape(state.shape))
 

time: 83.7 us -> 82.9 us (level)
  waiting for transfers between devices: 12.8 us -> 11.7 us
    ppermute x3, waiting for transfers between devices: 3.69 us -> 2.59 us  [swap(): return lax.ppermute(shard, 'tp_1', [(0, 1), (1, 0)])]
    convert_element_type x0 -> x1, other arithmetic: none -> 0.86 us  [run_expert(): return (keep + received.astype(F32)).astype(BF16)]
    pallas_call x1 -> x3, Pallas kernels: 2.23 us -> 2.45 us  [call(): pl.pallas_call(body, out_shape=out_shape, in_specs=[vmem] * len(operands)...]
  transfers between devices with their start and end apart: 4 -> 4, of which waited for: 4 -> 4; matrix products, arithmetic and copies ran while one was open for 0% -> 0% of each run, Pallas kernels for 9% -> 11%
where the time goes in v5:
time: 82.9 us; the launch traced here: 82.5 us
  blocking collectives  39.2 us (47%)
  Pallas kernels  16.5 us (20%)
  starting transfers between devices  13.2 us (16%)
  waiting for transfers between devices  11.7 us (14%)
  other arithmetic  0.89 us (1%)
    all_to_all x2, blocking collectives, exchange(): return lax.all_to_all(shard, axis, split_axis=0, concat_axis=0, tiled=True)  39.2 us
    all_to_all x1, waiting for transfers between devices, exchange(): return lax.all_to_all(shard, axis, split_axis=0, concat_axis=0, tiled=True)  9.1 us
    pallas_call x1, Pallas kernels, update_state(): pl.pallas_call(update_kernel, grid=(steps,), out_shape=jax.ShapeDtypeStru...  7.47 us
    ppermute x3, starting transfers between devices, swap(): return lax.ppermute(shard, 'tp_1', [(0, 1), (1, 0)])  7.04 us
    all_to_all x1, starting transfers between devices, exchange(): return lax.all_to_all(shard, axis, split_axis=0, concat_axis=0, tiled=True)  6.16 us
    pallas_call x1, Pallas kernels, project_heads(): pl.pallas_call(project_kernel, out_shape=(jax.ShapeDtypeStruct((seqs * 8,...  3.57 us
    ppermute x3, waiting for transfers between devices, swap(): return lax.ppermute(shard, 'tp_1', [(0, 1), (1, 0)])  2.59 us
    pallas_call x3, Pallas kernels, call(): pl.pallas_call(body, out_shape=out_shape, in_specs=[vmem] * len(operands)...  2.45 us
  transfers between devices with their start and end apart: 4, of which 4 were waited for; matrix products, arithmetic and copies ran while one was open for 0% of the time, Pallas kernels for 11%

profile of v5, /device:TPU:1, one launch (start us, length us, event | category | flops | bytes accessed | tf_op | source)
XLA Modules:
  0.0 82.5 jit_solution(1662900293874262052)
XLA Ops:
  0.6 0.0 copy-start
  0.6 0.0 copy-start.4
  0.7 0.0 copy-start.6
  0.7 3.6 %project_heads.1 = (f32[512,128]{1,0:T(8,128)S(1)}, f32[64,128]{1,0:T(8,128)S(1)}, f32[64,128]{1,0:T(8,128)S(1)}, f32[64,128]{1,0:T(8,128)S(1)}, f32[64,128]{1,0...) custom-call(bf16[64,2048]{1,0:T(8,128)(2,1)} %tokens_hbm.1, ...), custom_call_target="tpu_custom_call" | custom-call | flops 3000000000 | bytes 6291456 | tf_op jit(solution)/shard_map/project_heads/pallas_call | solution.py:161
  4.2 0.0 copy-done
  4.3 0.0 copy-done.4
  4.3 0.0 copy-done.6
  4.3 0.0 copy-start.1
  4.3 0.0 copy-start.2
  4.3 0.0 copy-start.5
  4.3 2.0 %mix.1 = (f32[8,64,128]{2,1,0:T(8,128)S(1)}, bf16[8,64,128]{2,1,0:T(8,128)(2,1)S(1)}, f32[64,128]{1,0:T(8,128)S(1)}) custom-call(f32[8192,64]{1,0:T(8,128)S(1)} %bitcast.22, f32[512,128]{1,0:T(8,128)S(1)} %get-tuple-element.26.vectors_ref, f32[64,128]{1,0:T(8,128)S(1)} %get-tuple-element.27.recept_ref, f32[64,128]{1,0:T(8,128)S(1)} %get-tuple-element.28.unit_rate_ref, ...), custom_call_target="tpu_custom_call" | custom-call | tf_op jit(solution)/shard_map/mix/pallas_call | solution.py:245
  6.3 3.3 %collective-permute-start = (bf16[8,64,128]{2,1,0:T(8,128)(2,1)S(1)}, bf16[8,64,128]{2,1,0:T(8,128)(2,1)S(1)}, u32[]{:S(2)}, u32[]{:S(2)}) collective-permute-start(bf16[8,64,128]{2,1,0:T(8,128)(2,1)S(1)} %get-tuple-element.32), channel_id=1, source_target_pairs={{0,1},{1,0},{2,3},{3,2},{4,5},{5,4},{6,7},{7,6},{8,9},{9,8},{10,11... | collective-permute-start | bytes 393224 | tf_op jit(solution)/shard_map/ppermute | solution.py:491
  9.6 1.0 %collective-permute-done = bf16[8,64,128]{2,1,0:T(8,128)(2,1)S(1)} collective-permute-done((bf16[8,64,128]{2,1,0:T(8,128)(2,1)S(1)}, bf16[8,64,128]{2,1,0:T(8,128)(2,1)S(1)}, u32[]{:S(2)}, u32[]{:S(2)}) %collective-permute-start) | collective-permute-done | bytes 131104 | tf_op jit(solution)/shard_map/ppermute | solution.py:491
  10.6 14.2 %all_to_all.15.parts_ref = bf16[8,64,128]{2,1,0:T(8,128)(2,1)S(1)} all-to-all(bf16[8,64,128]{2,1,0:T(8,128)(2,1)S(1)} %add_convert_fusion.1), channel_id=1, replica_groups=mesh['ep'=16,'tp_0'=8,'tp_1'=2] {'tp_0'}, dimensions={0} | all-to-all | bytes 262144 | tf_op jit(solution)/shard_map/all_to_all | solution.py:495
  24.8 0.2 dispatch_rows.1
  25.0 25.0 %all_to_all.16 = bf16[128,3,4,128]{3,2,1,0:T(4,128)(2,1)S(1)} all-to-all(bf16[128,3,4,128]{3,2,1,0:T(4,128)(2,1)S(1)} %bitcast.32), channel_id=1, replica_groups=mesh['ep'=16,'tp_0'=8,'tp_1'=2] {'tp_0','ep'}, dimensions={0} | all-to-all | bytes 786432 | tf_op jit(solution)/shard_map/all_to_all | solution.py:495
  50.0 3.4 %collective-permute-start.1 = (bf16[8,192,128]{2,1,0:T(8,128)(2,1)S(1)}, bf16[8,192,128]{2,1,0:T(8,128)(2,1)S(1)}, u32[]{:S(2)}, u32[]{:S(2)}) collective-permute-start(bf16[8,192,128]{2,1,0:T(8,128)(2,1)S(1)} %bitcast.30), channel_id=1, source_target_pairs={{0,1},{1,0},{2,3},{3,2},{4,5},{5,4},{6,7},{7,6},{8,9},{9,8},{10,11... | collective-permute-start | bytes 1179656 | tf_op jit(solution)/shard_map/ppermute | solution.py:491
  53.4 0.0 copy-done.1
  53.4 0.0 copy-done.2
  53.4 0.0 copy-done.5
  53.4 0.8 own_half.1
  54.2 0.6 collective-permute-done.1.rows_ref
  54.8 0.2 copy-done.3
  54.9 1.2 %other_half.1 = (bf16[192,448]{1,0:T(8,128)(2,1)S(1)}, bf16[8,192,128]{2,1,0:T(8,128)(2,1)S(1)}) custom-call(bf16[8,192,128]{2,1,0:T(8,128)(2,1)S(1)} %collective-permute-done.1.rows_ref, f32[1,2048]{1,0:T(1,128)S(1)} %bitcast.34, bf16[448,2048]{1,0:T(8,128)(2,1)S(1)} %bitcast.24, bf16[448,2048]{1,0:T(8,128)(2,1)S(1)} %bitcast.26, ...), custom_call_target="tpu_custom_call" | custom-call | tf_op jit(solution)/shard_map/other_half/pallas_call | solution.py:426
  56.2 0.3 collective-permute-start.2
  56.5 0.5 keep_half.1
  56.9 1.0 %collective-permute-done.2 = bf16[8,192,128]{2,1,0:T(8,128)(2,1)S(1)} collective-permute-done((bf16[8,192,128]{2,1,0:T(8,128)(2,1)S(1)}, bf16[8,192,128]{2,1,0:T(8,128)(2,1)S(1)}, u32[]{:S(2)}, u32[]{:S(2)}) %collective-permute-start.2) | collective-permute-done | bytes 393248 | tf_op jit(solution)/shard_map/ppermute | solution.py:491
  58.0 0.9 %add_convert_fusion = bf16[8,192,128]{2,1,0:T(8,128)(2,1)} fusion(f32[8,192,128]{2,1,0:T(8,128)S(1)} %keep_half.1, bf16[8,192,128]{2,1,0:T(8,128)(2,1)S(1)} %collective-permute-done.2), kind=kLoop, calls=%fused_computation | loop fusion | flops 589824 | bytes 1572864 | tf_op jit(solution)/shard_map/convert_element_type | solution.py:464
  58.8 6.2 %all-to-all-start.2 = ((bf16[128,3,4,128]{3,2,1,0:T(4,128)(2,1)}), bf16[128,3,4,128]{3,2,1,0:T(4,128)(2,1)S(1)}, u32[]{:S(2)}, u32[]{:S(2)}) async-start(bf16[128,3,4,128]{3,2,1,0:T(4,128)(2,1)} %bitcast.16), calls=%async_computation.2 | async-start | bytes 786432 | tf_op jit(solution)/shard_map/all_to_all | solution.py:495
  65.0 7.5 %update_state.1 = f32[8192,64]{1,0:T(8,128)} custom-call(f32[8192,64]{1,0:T(8,128)} %bitcast.21, f32[64,128]{1,0:T(8,128)S(1)} %get-tuple-element.46.removed_ref, f32[64,128]{1,0:T(8,128)S(1)} %get-tuple-element.28.unit_rate_ref, f32[64,128]{1,0:T(8,128)S(1)} %get-tuple-element.47.decay_ref, f32[64,128]{1,0:T(8,128)S(1)} %get-tuple-element.29.key_ref, ...), custom_call_target="tpu_custom_call" | custom-call | flops 2000000000 | bytes 8388608 | tf_op jit(solution)/shard_map/update_state/pallas_call | solution.py:310
  72.5 9.1 %all-to-all-done.2 = bf16[128,3,4,128]{3,2,1,0:T(4,128)(2,1)S(1)} async-done(((bf16[128,3,4,128]{3,2,1,0:T(4,128)(2,1)}), bf16[128,3,4,128]{3,2,1,0:T(4,128)(2,1)S(1)}, u32[]{:S(2)}, u32[]{:S(2)}) %all-to-all-start.2) | async-done | bytes 393248 | tf_op jit(solution)/shard_map/all_to_all | solution.py:495
  81.6 0.9 %combine.1 = bf16[64,128]{1,0:T(8,128)(2,1)} custom-call(f32[192,64]{1,0:T(8,128)S(1)} %get-tuple-element.25.share_ref, bf16[8,192,128]{2,1,0:T(8,128)(2,1)S(1)} %bitcast.29, bf16[64,128]{1,0:T(8,128)(2,1)S(1)} %get-tuple-element.45.resid_ref), custom_call_target="tpu_custom_call" | custom-call | tf_op jit(solution)/shard_map/combine/pallas_call | solution.py:482
  (2 shorter events, 0.0 us)
Async XLA Ops:
  0.6 3.6 %copy-start = (f32[64,2,64,64]{3,2,1,0:T(8,128)S(1)}, f32[64,2,64,64]{3,2,1,0:T(8,128)}, u32[]{:S(2)}) copy-start(f32[64,2,64,64]{3,2,1,0:T(8,128)} %param.20) | copy-start | bytes 6291460
  0.6 3.6 %copy-start.4 = (bf16[128,2048]{1,0:T(8,128)(2,1)S(1)}, bf16[128,2048]{1,0:T(8,128)(2,1)}, u32[]{:S(2)}) copy-start(bf16[128,2048]{1,0:T(8,128)(2,1)} %w_output_ref.1) | copy-start | bytes 1572868
  0.7 3.6 %copy-start.6 = (f32[128]{0:T(128)S(1)}, f32[128]{0:T(128)}, u32[]{:S(2)}) copy-start(f32[128]{0:T(128)} %param.32) | copy-start | bytes 1540
  4.3 49.1 %copy-start.1 = (bf16[1,2048,448]{1,2,0:T(8,128)(2,1)S(1)}, bf16[1,2048,448]{1,2,0:T(8,128)(2,1)}, u32[]{:S(2)}) copy-start(bf16[1,2048,448]{1,2,0:T(8,128)(2,1)} %param.35) | copy-start | bytes 5505028
  4.3 49.1 %copy-start.2 = (bf16[1,2048,448]{1,2,0:T(8,128)(2,1)S(1)}, bf16[1,2048,448]{1,2,0:T(8,128)(2,1)}, u32[]{:S(2)}) copy-start(bf16[1,2048,448]{1,2,0:T(8,128)(2,1)} %param.36) | copy-start | bytes 5505028
  4.3 49.1 %copy-start.5 = (f32[2048]{0:T(1024)S(1)}, f32[2048]{0:T(1024)}, u32[]{:S(2)}) copy-start(f32[2048]{0:T(1024)} %param.34) | copy-start | bytes 24580
  6.3 4.3 %collective-permute-start = (bf16[8,64,128]{2,1,0:T(8,128)(2,1)S(1)}, bf16[8,64,128]{2,1,0:T(8,128)(2,1)S(1)}, u32[]{:S(2)}, u32[]{:S(2)}) collective-permute-start(bf16[8,64,128]{2,1,0:T(8,128)(2,1)S(1)} %get-tuple-element.32), channel_id=1, source_target_pairs={{0,1},{1,0},{2,3},{3,2},{4,5},{5,4},{6,7},{7,6},{8,9},{9,8},{10,11... | collective-permute-start | bytes 393224 | tf_op jit(solution)/shard_map/ppermute | solution.py:491
  50.0 4.8 %collective-permute-start.1 = (bf16[8,192,128]{2,1,0:T(8,128)(2,1)S(1)}, bf16[8,192,128]{2,1,0:T(8,128)(2,1)S(1)}, u32[]{:S(2)}, u32[]{:S(2)}) collective-permute-start(bf16[8,192,128]{2,1,0:T(8,128)(2,1)S(1)} %bitcast.30), channel_id=1, source_target_pairs={{0,1},{1,0},{2,3},{3,2},{4,5},{5,4},{6,7},{7,6},{8,9},{9,8},{10,11... | collective-permute-start | bytes 1179656 | tf_op jit(solution)/shard_map/ppermute | solution.py:491
  53.4 1.5 %copy-start.3 = (bf16[1,448,2048]{2,1,0:T(8,128)(2,1)S(1)}, bf16[1,448,2048]{2,1,0:T(8,128)(2,1)}, u32[]{:S(2)}) copy-start(bf16[1,448,2048]{2,1,0:T(8,128)(2,1)} %param.37) | copy-start | bytes 5505028
  56.2 1.8 %collective-permute-start.2 = (bf16[8,192,128]{2,1,0:T(8,128)(2,1)S(1)}, bf16[8,192,128]{2,1,0:T(8,128)(2,1)S(1)}, u32[]{:S(2)}, u32[]{:S(2)}) collective-permute-start(bf16[8,192,128]{2,1,0:T(8,128)(2,1)S(1)} %get-tuple-element.44), channel_id=1, source_target_pairs={{0,1},{1,0},{2,3},{3,2},{4,5},{5,4},{6,7},{7,6},{8,9},{9,8},{10,11... | collective-permute-start | bytes 1179656 | tf_op jit(solution)/shard_map/ppermute | solution.py:491
  58.8 22.7 %all-to-all-start.2 = ((bf16[128,3,4,128]{3,2,1,0:T(4,128)(2,1)}), bf16[128,3,4,128]{3,2,1,0:T(4,128)(2,1)S(1)}, u32[]{:S(2)}, u32[]{:S(2)}) async-start(bf16[128,3,4,128]{3,2,1,0:T(4,128)(2,1)} %bitcast.16), calls=%async_computation.2 | async-start | bytes 786432 | tf_op jit(solution)/shard_map/all_to_all | solution.py:495

commit v6 on v5

--- a/solution.py
+++ b/solution.py
@@ -17,6 +17,16 @@
 VMEM = pltpu.VMEM
 HEAD = 64
 LANES = 128
+FIRST_Z = 5
+FIRST_EP = 10
+
+
+def z_order(count):
+    return [(FIRST_Z + step) % count for step in range(count)]
+
+
+def ep_order(count):
+    return [(FIRST_EP + step) % count for step in range(count)]
 
 
 def in_hbm(array):
@@ -51,7 +61,8 @@
     shares = jnp.zeros((slots, seqs), F32)
     for k, choice in enumerate((first, second)):
         placed = jnp.sum(named[k] * counts, axis=0, keepdims=True).astype(jnp.int32)
-        here = slot == choice * (slots // experts) + placed
+        chunk = lax.rem(choice + (experts - FIRST_EP), experts)
+        here = slot == chunk * (slots // experts) + placed
         picked = jnp.where(here, 1.0, picked)
         shares = jnp.where(here, exps[k : k + 1, :] / total, shares)
     pick_ref[...] = picked.astype(BF16)
@@ -232,11 +243,11 @@
     spread = head_sums(centred * centred) * (1.0 / HEAD)
     mixed = (centred * lax.rsqrt(spread + GROUP_EPS) * group_gain_ref[...]).astype(BF16)
     core = lax.axis_index("tp_1")
-    for z in range(keep_ref.shape[0]):
+    for place, z in enumerate(z_order(keep_ref.shape[0])):
         own = w_output_ref[:, pl.ds(pl.multiple_of((2 * z + core) * LANES, LANES), LANES)]
-        keep_ref[z] = jnp.dot(mixed, own, preferred_element_type=F32)
+        keep_ref[place] = jnp.dot(mixed, own, preferred_element_type=F32)
         other = w_output_ref[:, pl.ds(pl.multiple_of((2 * z + 1 - core) * LANES, LANES), LANES)]
-        send_ref[z] = jnp.dot(mixed, other, preferred_element_type=F32).astype(BF16)
+        send_ref[place] = jnp.dot(mixed, other, preferred_element_type=F32).astype(BF16)
 
 
 def mix(state_rows, vectors, recept, unit_rate, key, value, w_output, group_gain, z_count):
@@ -354,7 +365,7 @@
     return jnp.concatenate(
         [
             ref[:, pl.ds(pl.multiple_of((2 * z + core) * LANES, LANES), LANES)]
-            for z in range(blocks)
+            for z in z_order(blocks)
         ],
         axis=1,
     )
@@ -491,14 +502,17 @@
     return lax.ppermute(shard, "tp_1", [(0, 1), (1, 0)])
 
 
-def exchange(shard, axis):
-    return lax.all_to_all(shard, axis, split_axis=0, concat_axis=0, tiled=True)
+def exchange(shard, axis, order):
+    return lax.all_to_all(
+        shard, axis, split_axis=0, concat_axis=0, axis_index_groups=[order], tiled=True
+    )
 
 
 def exchange_rows(shard):
-    groups = lax.axis_size("ep") * lax.axis_size("tp_0")
-    chunks = shard.reshape(groups, -1, 4, LANES)
-    return exchange(chunks, ("tp_0", "ep")).reshape(shard.shape)
+    ep_count, z_count = lax.axis_size("ep"), lax.axis_size("tp_0")
+    order = [z * ep_count + e for z in z_order(z_count) for e in ep_order(ep_count)]
+    chunks = shard.reshape(len(order), -1, 4, LANES)
+    return exchange(chunks, ("tp_0", "ep"), order).reshape(shard.shape)
 
 
 def local(
@@ -550,7 +564,7 @@
         z_count,
     )
     pair_sum = (keep + swap(send).astype(F32)).astype(BF16)
-    parts = exchange(pair_sum, "tp_0")
+    parts = exchange(pair_sum, "tp_0", z_order(z_count))
     new_state = update_state(state_rows, removed, unit_rate, decay, key, value)
 
     resid_own, outgoing = dispatch_rows(parts, own_tokens, pick)

time: 82.9 us -> 76.1 us (0.918)
  waiting for transfers between devices: 11.7 us -> 4.47 us
  starting transfers between devices: 13.2 us -> 19 us
  blocking collectives: 39.2 us -> 33.8 us
    all_to_all x1, waiting for transfers between devices: 9.1 us -> 1.88 us  [exchange(): lax.all_to_all(shard, axis, split_axis=0, concat_axis=0, axis_index_group...]
    all_to_all x1, starting transfers between devices: 6.16 us -> 13.1 us  [exchange(): lax.all_to_all(shard, axis, split_axis=0, concat_axis=0, axis_index_group...]
    all_to_all x2, blocking collectives: 39.2 us -> 33.8 us  [exchange(): lax.all_to_all(shard, axis, split_axis=0, concat_axis=0, axis_index_group...]
    ppermute x3, starting transfers between devices: 7.04 us -> 5.9 us  [swap(): return lax.ppermute(shard, 'tp_1', [(0, 1), (1, 0)])]
where the time goes in v6:
time: 76.1 us; the launch traced here: 75.7 us
  blocking collectives  33.8 us (44%)
  starting transfers between devices  19 us (25%)
  Pallas kernels  16.5 us (22%)
  waiting for transfers between devices  4.47 us (6%)
  other arithmetic  0.89 us (1%)
  between operations  0.77 us (1%)
    all_to_all x2, blocking collectives, exchange(): lax.all_to_all(shard, axis, split_axis=0, concat_axis=0, axis_index_group...  33.8 us
    all_to_all x1, starting transfers between devices, exchange(): lax.all_to_all(shard, axis, split_axis=0, concat_axis=0, axis_index_group...  13.1 us
    pallas_call x1, Pallas kernels, update_state(): pl.pallas_call(update_kernel, grid=(steps,), out_shape=jax.ShapeDtypeStru...  7.46 us
    ppermute x3, starting transfers between devices, swap(): return lax.ppermute(shard, 'tp_1', [(0, 1), (1, 0)])  5.9 us
    pallas_call x1, Pallas kernels, project_heads(): pl.pallas_call(project_kernel, out_shape=(jax.ShapeDtypeStruct((seqs * 8,...  3.57 us
    ppermute x3, waiting for transfers between devices, swap(): return lax.ppermute(shard, 'tp_1', [(0, 1), (1, 0)])  2.59 us
    pallas_call x3, Pallas kernels, call(): pl.pallas_call(body, out_shape=out_shape, in_specs=[vmem] * len(operands)...  2.46 us
    pallas_call x1, Pallas kernels, mix(): pl.pallas_call(mix_kernel, out_shape=(jax.ShapeDtypeStruct((z_count, seqs...  2 us
  transfers between devices with their start and end apart: 4, of which 4 were waited for; matrix products, arithmetic and copies ran while one was open for 0% of the time, Pallas kernels for 11%

profile of v6, /device:TPU:1, one launch (start us, length us, event | category | flops | bytes accessed | tf_op | source)
XLA Modules:
  0.0 75.7 jit_solution(9783906492646215248)
XLA Ops:
  0.6 0.0 copy-start
  0.6 0.0 copy-start.4
  0.7 0.0 copy-start.6
  0.7 3.6 %project_heads.1 = (f32[512,128]{1,0:T(8,128)S(1)}, f32[64,128]{1,0:T(8,128)S(1)}, f32[64,128]{1,0:T(8,128)S(1)}, f32[64,128]{1,0:T(8,128)S(1)}, f32[64,128]{1,0...) custom-call(bf16[64,2048]{1,0:T(8,128)(2,1)} %tokens_hbm.1, ...), custom_call_target="tpu_custom_call" | custom-call | flops 3000000000 | bytes 6291456 | tf_op jit(solution)/shard_map/project_heads/pallas_call | solution.py:172
  4.2 0.0 copy-done
  4.3 0.0 copy-done.4
  4.3 0.0 copy-done.6
  4.3 0.0 copy-start.1
  4.3 0.0 copy-start.2
  4.3 0.0 copy-start.5
  4.3 2.0 %mix.1 = (f32[8,64,128]{2,1,0:T(8,128)S(1)}, bf16[8,64,128]{2,1,0:T(8,128)(2,1)S(1)}, f32[64,128]{1,0:T(8,128)S(1)}) custom-call(f32[8192,64]{1,0:T(8,128)S(1)} %bitcast.22, f32[512,128]{1,0:T(8,128)S(1)} %get-tuple-element.26.vectors_ref, f32[64,128]{1,0:T(8,128)S(1)} %get-tuple-element.27.recept_ref, f32[64,128]{1,0:T(8,128)S(1)} %get-tuple-element.28.unit_rate_ref, ...), custom_call_target="tpu_custom_call" | custom-call | tf_op jit(solution)/shard_map/mix/pallas_call | solution.py:256
  6.3 3.3 %collective-permute-start = (bf16[8,64,128]{2,1,0:T(8,128)(2,1)S(1)}, bf16[8,64,128]{2,1,0:T(8,128)(2,1)S(1)}, u32[]{:S(2)}, u32[]{:S(2)}) collective-permute-start(bf16[8,64,128]{2,1,0:T(8,128)(2,1)S(1)} %get-tuple-element.32), channel_id=1, source_target_pairs={{0,1},{1,0},{2,3},{3,2},{4,5},{5,4},{6,7},{7,6},{8,9},{9,8},{10,11... | collective-permute-start | bytes 393224 | tf_op jit(solution)/shard_map/ppermute | solution.py:502
  9.6 1.0 %collective-permute-done = bf16[8,64,128]{2,1,0:T(8,128)(2,1)S(1)} collective-permute-done((bf16[8,64,128]{2,1,0:T(8,128)(2,1)S(1)}, bf16[8,64,128]{2,1,0:T(8,128)(2,1)S(1)}, u32[]{:S(2)}, u32[]{:S(2)}) %collective-permute-start) | collective-permute-done | bytes 131104 | tf_op jit(solution)/shard_map/ppermute | solution.py:502
  10.6 11.2 %all_to_all.15.parts_ref = bf16[8,64,128]{2,1,0:T(8,128)(2,1)S(1)} all-to-all(bf16[8,64,128]{2,1,0:T(8,128)(2,1)S(1)} %add_convert_fusion.1), channel_id=1, replica_groups={{10,12,14,0,2,4,6,8},{11,13,15,1,3,5,7,9},{26,28,30,16,18,20,22,24},{27..., dimensions={0} | all-to-all | bytes 262144 | tf_op jit(solution)/shard_map/all_to_all | solution.py:506
  21.8 0.2 dispatch_rows.1
  22.0 22.6 %all_to_all.16 = bf16[128,3,4,128]{3,2,1,0:T(4,128)(2,1)S(1)} all-to-all(bf16[128,3,4,128]{3,2,1,0:T(4,128)(2,1)S(1)} %bitcast.32), channel_id=1, replica_groups={{170,186,202,218,234,250,10,26,42,58,74,90,106,122,138,154,172,188,204,..., dimensions={0} | all-to-all | bytes 786432 | tf_op jit(solution)/shard_map/all_to_all | solution.py:506
  44.6 2.3 %collective-permute-start.1 = (bf16[8,192,128]{2,1,0:T(8,128)(2,1)S(1)}, bf16[8,192,128]{2,1,0:T(8,128)(2,1)S(1)}, u32[]{:S(2)}, u32[]{:S(2)}) collective-permute-start(bf16[8,192,128]{2,1,0:T(8,128)(2,1)S(1)} %bitcast.30), channel_id=1, source_target_pairs={{0,1},{1,0},{2,3},{3,2},{4,5},{5,4},{6,7},{7,6},{8,9},{9,8},{10,11... | collective-permute-start | bytes 1179656 | tf_op jit(solution)/shard_map/ppermute | solution.py:502
  46.9 0.0 copy-done.1
  46.9 0.0 copy-done.2
  46.9 0.0 copy-done.5
  46.9 0.8 %own_half.1 = (f32[192,128]{1,0:T(8,128)S(1)}, f32[192,448]{1,0:T(8,128)S(1)}, f32[192,448]{1,0:T(8,128)S(1)}) custom-call(bf16[8,192,128]{2,1,0:T(8,128)(2,1)S(1)} %bitcast.31, f32[1,2048]{1,0:T(1,128)S(1)} %bitcast.33, bf16[448,2048]{1,0:T(8,128)(2,1)S(1)} %bitcast.23, bf16[448,2048]{1,0:T(8,128)(2,1)S(1)} %bitcast.25), custom_call_target="tpu_custom_call" | custom-call | tf_op jit(solution)/shard_map/own_half/pallas_call | solution.py:437
  47.7 0.6 collective-permute-done.1.rows_ref
  48.3 0.2 copy-done.3
  48.4 1.2 %other_half.1 = (bf16[192,448]{1,0:T(8,128)(2,1)S(1)}, bf16[8,192,128]{2,1,0:T(8,128)(2,1)S(1)}) custom-call(bf16[8,192,128]{2,1,0:T(8,128)(2,1)S(1)} %collective-permute-done.1.rows_ref, f32[1,2048]{1,0:T(1,128)S(1)} %bitcast.34, bf16[448,2048]{1,0:T(8,128)(2,1)S(1)} %bitcast.24, bf16[448,2048]{1,0:T(8,128)(2,1)S(1)} %bitcast.26, ...), custom_call_target="tpu_custom_call" | custom-call | tf_op jit(solution)/shard_map/other_half/pallas_call | solution.py:437
  49.7 0.3 collective-permute-start.2
  50.0 0.5 keep_half.1
  50.4 1.0 %collective-permute-done.2 = bf16[8,192,128]{2,1,0:T(8,128)(2,1)S(1)} collective-permute-done((bf16[8,192,128]{2,1,0:T(8,128)(2,1)S(1)}, bf16[8,192,128]{2,1,0:T(8,128)(2,1)S(1)}, u32[]{:S(2)}, u32[]{:S(2)}) %collective-permute-start.2) | collective-permute-done | bytes 393248 | tf_op jit(solution)/shard_map/ppermute | solution.py:502
  51.5 0.9 %add_convert_fusion = bf16[8,192,128]{2,1,0:T(8,128)(2,1)} fusion(f32[8,192,128]{2,1,0:T(8,128)S(1)} %keep_half.1, bf16[8,192,128]{2,1,0:T(8,128)(2,1)S(1)} %collective-permute-done.2), kind=kLoop, calls=%fused_computation | loop fusion | flops 589824 | bytes 1572864 | tf_op jit(solution)/shard_map/convert_element_type | solution.py:475
  52.3 13.1 %all-to-all-start.2 = ((bf16[128,3,4,128]{3,2,1,0:T(4,128)(2,1)}), bf16[128,3,4,128]{3,2,1,0:T(4,128)(2,1)S(1)}, u32[]{:S(2)}, u32[]{:S(2)}) async-start(bf16[128,3,4,128]{3,2,1,0:T(4,128)(2,1)} %bitcast.16), calls=%async_computation.2 | async-start | bytes 786432 | tf_op jit(solution)/shard_map/all_to_all | solution.py:506
  65.5 7.5 %update_state.1 = f32[8192,64]{1,0:T(8,128)} custom-call(f32[8192,64]{1,0:T(8,128)} %bitcast.21, f32[64,128]{1,0:T(8,128)S(1)} %get-tuple-element.46.removed_ref, f32[64,128]{1,0:T(8,128)S(1)} %get-tuple-element.28.unit_rate_ref, f32[64,128]{1,0:T(8,128)S(1)} %get-tuple-element.47.decay_ref, f32[64,128]{1,0:T(8,128)S(1)} %get-tuple-element.29.key_ref, ...), custom_call_target="tpu_custom_call" | custom-call | flops 2000000000 | bytes 8388608 | tf_op jit(solution)/shard_map/update_state/pallas_call | solution.py:321
  72.9 1.9 %all-to-all-done.2 = bf16[128,3,4,128]{3,2,1,0:T(4,128)(2,1)S(1)} async-done(((bf16[128,3,4,128]{3,2,1,0:T(4,128)(2,1)}), bf16[128,3,4,128]{3,2,1,0:T(4,128)(2,1)S(1)}, u32[]{:S(2)}, u32[]{:S(2)}) %all-to-all-start.2) | async-done | bytes 393248 | tf_op jit(solution)/shard_map/all_to_all | solution.py:506
  74.8 0.9 %combine.1 = bf16[64,128]{1,0:T(8,128)(2,1)} custom-call(f32[192,64]{1,0:T(8,128)S(1)} %get-tuple-element.25.share_ref, bf16[8,192,128]{2,1,0:T(8,128)(2,1)S(1)} %bitcast.29, bf16[64,128]{1,0:T(8,128)(2,1)S(1)} %get-tuple-element.45.resid_ref), custom_call_target="tpu_custom_call" | custom-call | tf_op jit(solution)/shard_map/combine/pallas_call | solution.py:493
  (2 shorter events, 0.0 us)
Async XLA Ops:
  0.6 3.6 %copy-start = (f32[64,2,64,64]{3,2,1,0:T(8,128)S(1)}, f32[64,2,64,64]{3,2,1,0:T(8,128)}, u32[]{:S(2)}) copy-start(f32[64,2,64,64]{3,2,1,0:T(8,128)} %param.20) | copy-start | bytes 6291460
  0.6 3.6 %copy-start.4 = (bf16[128,2048]{1,0:T(8,128)(2,1)S(1)}, bf16[128,2048]{1,0:T(8,128)(2,1)}, u32[]{:S(2)}) copy-start(bf16[128,2048]{1,0:T(8,128)(2,1)} %w_output_ref.1) | copy-start | bytes 1572868
  0.7 3.6 %copy-start.6 = (f32[128]{0:T(128)S(1)}, f32[128]{0:T(128)}, u32[]{:S(2)}) copy-start(f32[128]{0:T(128)} %param.32) | copy-start | bytes 1540
  4.3 42.6 %copy-start.1 = (bf16[1,2048,448]{1,2,0:T(8,128)(2,1)S(1)}, bf16[1,2048,448]{1,2,0:T(8,128)(2,1)}, u32[]{:S(2)}) copy-start(bf16[1,2048,448]{1,2,0:T(8,128)(2,1)} %param.35) | copy-start | bytes 5505028
  4.3 42.6 %copy-start.2 = (bf16[1,2048,448]{1,2,0:T(8,128)(2,1)S(1)}, bf16[1,2048,448]{1,2,0:T(8,128)(2,1)}, u32[]{:S(2)}) copy-start(bf16[1,2048,448]{1,2,0:T(8,128)(2,1)} %param.36) | copy-start | bytes 5505028
  4.3 42.6 %copy-start.5 = (f32[2048]{0:T(1024)S(1)}, f32[2048]{0:T(1024)}, u32[]{:S(2)}) copy-start(f32[2048]{0:T(1024)} %param.34) | copy-start | bytes 24580
  6.3 4.3 %collective-permute-start = (bf16[8,64,128]{2,1,0:T(8,128)(2,1)S(1)}, bf16[8,64,128]{2,1,0:T(8,128)(2,1)S(1)}, u32[]{:S(2)}, u32[]{:S(2)}) collective-permute-start(bf16[8,64,128]{2,1,0:T(8,128)(2,1)S(1)} %get-tuple-element.32), channel_id=1, source_target_pairs={{0,1},{1,0},{2,3},{3,2},{4,5},{5,4},{6,7},{7,6},{8,9},{9,8},{10,11... | collective-permute-start | bytes 393224 | tf_op jit(solution)/shard_map/ppermute | solution.py:502
  44.6 3.7 %collective-permute-start.1 = (bf16[8,192,128]{2,1,0:T(8,128)(2,1)S(1)}, bf16[8,192,128]{2,1,0:T(8,128)(2,1)S(1)}, u32[]{:S(2)}, u32[]{:S(2)}) collective-permute-start(bf16[8,192,128]{2,1,0:T(8,128)(2,1)S(1)} %bitcast.30), channel_id=1, source_target_pairs={{0,1},{1,0},{2,3},{3,2},{4,5},{5,4},{6,7},{7,6},{8,9},{9,8},{10,11... | collective-permute-start | bytes 1179656 | tf_op jit(solution)/shard_map/ppermute | solution.py:502
  46.9 1.5 %copy-start.3 = (bf16[1,448,2048]{2,1,0:T(8,128)(2,1)S(1)}, bf16[1,448,2048]{2,1,0:T(8,128)(2,1)}, u32[]{:S(2)}) copy-start(bf16[1,448,2048]{2,1,0:T(8,128)(2,1)} %param.37) | copy-start | bytes 5505028
  49.7 1.8 %collective-permute-start.2 = (bf16[8,192,128]{2,1,0:T(8,128)(2,1)S(1)}, bf16[8,192,128]{2,1,0:T(8,128)(2,1)S(1)}, u32[]{:S(2)}, u32[]{:S(2)}) collective-permute-start(bf16[8,192,128]{2,1,0:T(8,128)(2,1)S(1)} %get-tuple-element.44), channel_id=1, source_target_pairs={{0,1},{1,0},{2,3},{3,2},{4,5},{5,4},{6,7},{7,6},{8,9},{9,8},{10,11... | collective-permute-start | bytes 1179656 | tf_op jit(solution)/shard_map/ppermute | solution.py:502
  52.3 22.5 %all-to-all-start.2 = ((bf16[128,3,4,128]{3,2,1,0:T(4,128)(2,1)}), bf16[128,3,4,128]{3,2,1,0:T(4,128)(2,1)S(1)}, u32[]{:S(2)}, u32[]{:S(2)}) async-start(bf16[128,3,4,128]{3,2,1,0:T(4,128)(2,1)} %bitcast.16), calls=%async_computation.2 | async-start | bytes 786432 | tf_op jit(solution)/shard_map/all_to_all | solution.py:506

commit v7 on v6

--- a/solution.py
+++ b/solution.py
@@ -207,20 +207,27 @@
     unit_rate_ref,
     key_ref,
     value_ref,
-    w_output_ref,
+    w_output_hbm,
     group_gain_ref,
-    keep_ref,
     send_ref,
     removed_ref,
+    mixed_ref,
+    w_output_ref,
     products_ref,
+    sem,
 ):
+    w_output_copy = pltpu.make_async_copy(w_output_hbm, w_output_ref, sem)
+    w_output_copy.start()
     seqs = recept_ref.shape[0]
-    for seq in range(seqs):
-        left = vectors_ref[seq * 8 : seq * 8 + 8, :HEAD].astype(BF16)
-        right = state_ref[seq * LANES : (seq + 1) * LANES, :].astype(BF16)
-        products_ref[seq * 8 : seq * 8 + 8, :] = lax.dot_general(
-            left, right, (((1,), (1,)), ((), ())), preferred_element_type=F32
-        )
+    group = 2
+    for seq in range(0, seqs, group):
+        left = vectors_ref[seq * 8 : (seq + group) * 8, :HEAD].astype(BF16)
+        right = state_ref[seq * LANES : (seq + group) * LANES, :].astype(BF16)
+        out = lax.dot_general(left, right, ACROSS, preferred_element_type=F32)
+        for one in range(group):
+            products_ref[(seq + one) * 8 : (seq + one + 1) * 8, :] = out[
+                one * 8 : (one + 1) * 8, one * LANES : (one + 1) * LANES
+            ]
     first_head = lax.broadcasted_iota(jnp.int32, (seqs, LANES), 1) < HEAD
     removed = jnp.where(
         first_head,
@@ -242,12 +249,17 @@
     centred = readout - head_sums(readout) * (1.0 / HEAD)
     spread = head_sums(centred * centred) * (1.0 / HEAD)
     mixed = (centred * lax.rsqrt(spread + GROUP_EPS) * group_gain_ref[...]).astype(BF16)
-    core = lax.axis_index("tp_1")
-    for place, z in enumerate(z_order(keep_ref.shape[0])):
-        own = w_output_ref[:, pl.ds(pl.multiple_of((2 * z + core) * LANES, LANES), LANES)]
-        keep_ref[place] = jnp.dot(mixed, own, preferred_element_type=F32)
-        other = w_output_ref[:, pl.ds(pl.multiple_of((2 * z + 1 - core) * LANES, LANES), LANES)]
-        send_ref[place] = jnp.dot(mixed, other, preferred_element_type=F32).astype(BF16)
+    mixed_ref[...] = mixed
+    w_output_copy.wait()
+    out_columns(mixed, w_output_ref, send_ref, 1 - lax.axis_index("tp_1"))
+
+
+def out_columns(mixed, w_output_ref, out_ref, core):
+    for place, z in enumerate(z_order(out_ref.shape[0])):
+        cols = pl.ds(pl.multiple_of((2 * z + core) * LANES, LANES), LANES)
+        out_ref[place] = jnp.dot(
+            mixed, w_output_ref[:, cols], preferred_element_type=F32
+        ).astype(out_ref.dtype)
 
 
 def mix(state_rows, vectors, recept, unit_rate, key, value, w_output, group_gain, z_count):
@@ -256,16 +268,30 @@
     return pl.pallas_call(
         mix_kernel,
         out_shape=(
-            jax.ShapeDtypeStruct((z_count, seqs, LANES), F32),
             jax.ShapeDtypeStruct((z_count, seqs, LANES), BF16),
             jax.ShapeDtypeStruct((seqs, LANES), F32),
+            jax.ShapeDtypeStruct((seqs, LANES), BF16),
+            jax.ShapeDtypeStruct(w_output.shape, BF16),
         ),
-        in_specs=[vmem] * 8,
-        out_specs=(vmem,) * 3,
-        scratch_shapes=[VMEM((seqs * 8, LANES), F32)],
+        in_specs=[vmem] * 6 + [pl.BlockSpec(memory_space=pl.ANY), vmem],
+        out_specs=(vmem,) * 4,
+        scratch_shapes=[VMEM((seqs * 8, LANES), F32), pltpu.SemaphoreType.DMA(())],
         compiler_params=pltpu.CompilerParams(vmem_limit_bytes=12 << 20),
         name="mix",
-    )(state_rows, vectors, recept, unit_rate, key, value, w_output, group_gain)
+    )(state_rows, vectors, recept, unit_rate, key, value, in_hbm(w_output), group_gain)
+
+
+def keep_out_kernel(mixed_ref, w_output_ref, keep_ref):
+    out_columns(mixed_ref[...], w_output_ref, keep_ref, lax.axis_index("tp_1"))
+
+
+def keep_out(mixed, w_output, z_count):
+    return pl.pallas_call(
+        keep_out_kernel,
+        out_shape=jax.ShapeDtypeStruct((z_count, *mixed.shape), F32),
+        compiler_params=pltpu.CompilerParams(vmem_limit_bytes=2 << 20),
+        name="keep_out",
+    )(mixed, w_output)
 
 
 def update_kernel(
@@ -552,7 +578,7 @@
         route_logits.T,
         slot_count,
     )
-    keep, send, removed = mix(
+    send, removed, mixed, w_output_near = mix(
         state_rows,
         vectors,
         recept,
@@ -563,6 +589,7 @@
         group_gain.reshape(1, -1),
         z_count,
     )
+    keep = keep_out(mixed, w_output_near, z_count)
     pair_sum = (keep + swap(send).astype(F32)).astype(BF16)
     parts = exchange(pair_sum, "tp_0", z_order(z_count))
     new_state = update_state(state_rows, removed, unit_rate, decay, key, value)

time: 76.1 us -> 75.5 us (level)
  transfers between devices with their start and end apart: 4 -> 4, of which waited for: 4 -> 4; matrix products, arithmetic and copies ran while one was open for 0% -> 0% of each run, Pallas kernels for 11% -> 12%
where the time goes in v7:
time: 75.5 us; the launch traced here: 75.1 us
  blocking collectives  33.8 us (45%)
  starting transfers between devices  19 us (25%)
  Pallas kernels  16.2 us (21%)
  waiting for transfers between devices  4.24 us (6%)
  other arithmetic  0.89 us (1%)
  between operations  0.76 us (1%)
    all_to_all x2, blocking collectives, exchange(): lax.all_to_all(shard, axis, split_axis=0, concat_axis=0, axis_index_group...  33.8 us
    all_to_all x1, starting transfers between devices, exchange(): lax.all_to_all(shard, axis, split_axis=0, concat_axis=0, axis_index_group...  13.1 us
    pallas_call x1, Pallas kernels, update_state(): pl.pallas_call(update_kernel, grid=(steps,), out_shape=jax.ShapeDtypeStru...  7.47 us
    ppermute x3, starting transfers between devices, swap(): return lax.ppermute(shard, 'tp_1', [(0, 1), (1, 0)])  5.9 us
    pallas_call x1, Pallas kernels, project_heads(): pl.pallas_call(project_kernel, out_shape=(jax.ShapeDtypeStruct((seqs * 8,...  3.57 us
    pallas_call x3, Pallas kernels, call(): pl.pallas_call(body, out_shape=out_shape, in_specs=[vmem] * len(operands)...  2.47 us
    ppermute x3, waiting for transfers between devices, swap(): return lax.ppermute(shard, 'tp_1', [(0, 1), (1, 0)])  2.38 us
    all_to_all x1, waiting for transfers between devices, exchange(): lax.all_to_all(shard, axis, split_axis=0, concat_axis=0, axis_index_group...  1.86 us
  transfers between devices with their start and end apart: 4, of which 4 were waited for; matrix products, arithmetic and copies ran while one was open for 0% of the time, Pallas kernels for 12%

profile of v7, /device:TPU:1, one launch (start us, length us, event | category | flops | bytes accessed | tf_op | source)
XLA Modules:
  0.0 75.1 jit_solution(10819536227821242298)
XLA Ops:
  0.6 0.0 copy-start
  0.6 0.0 copy-start.5
  0.7 3.6 %project_heads.1 = (f32[512,128]{1,0:T(8,128)S(1)}, f32[64,128]{1,0:T(8,128)S(1)}, f32[64,128]{1,0:T(8,128)S(1)}, f32[64,128]{1,0:T(8,128)S(1)}, f32[64,128]{1,0...) custom-call(bf16[64,2048]{1,0:T(8,128)(2,1)} %tokens_hbm.1, ...), custom_call_target="tpu_custom_call" | custom-call | flops 3000000000 | bytes 6291456 | tf_op jit(solution)/shard_map/project_heads/pallas_call | solution.py:172
  4.2 0.0 copy-done
  4.2 0.0 copy-done.5
  4.3 0.0 copy-start.2
  4.3 1.4 %mix.1 = (bf16[8,64,128]{2,1,0:T(8,128)(2,1)S(1)}, f32[64,128]{1,0:T(8,128)S(1)}, bf16[64,128]{1,0:T(8,128)(2,1)S(1)}, bf16[128,2048]{1,0:T(8,128)(2,1)S(1)}) custom-call(f32[8192,64]{1,0:T(8,128)S(1)} %bitcast.22, f32[512,128]{1,0:T(8,128)S(1)} %get-tuple-element.27.vectors_ref, f32[64,128]{1,0:T(8,128)S(1)} %get-tuple-element.28.recept_ref, ...), custom_call_target="tpu_custom_call" | custom-call | tf_op jit(solution)/shard_map/mix/pallas_call | solution.py:268
  5.7 0.0 copy-start.1
  5.7 0.0 copy-start.4
  5.7 3.3 %collective-permute-start = (bf16[8,64,128]{2,1,0:T(8,128)(2,1)S(1)}, bf16[8,64,128]{2,1,0:T(8,128)(2,1)S(1)}, u32[]{:S(2)}, u32[]{:S(2)}) collective-permute-start(bf16[8,64,128]{2,1,0:T(8,128)(2,1)S(1)} %get-tuple-element.34), channel_id=1, source_target_pairs={{0,1},{1,0},{2,3},{3,2},{4,5},{5,4},{6,7},{7,6},{8,9},{9,8},{10,11... | collective-permute-start | bytes 393224 | tf_op jit(solution)/shard_map/ppermute | solution.py:528
  9.0 0.2 keep_out.1
  9.2 0.8 %collective-permute-done = bf16[8,64,128]{2,1,0:T(8,128)(2,1)S(1)} collective-permute-done((bf16[8,64,128]{2,1,0:T(8,128)(2,1)S(1)}, bf16[8,64,128]{2,1,0:T(8,128)(2,1)S(1)}, u32[]{:S(2)}, u32[]{:S(2)}) %collective-permute-start) | collective-permute-done | bytes 131104 | tf_op jit(solution)/shard_map/ppermute | solution.py:528
  10.0 11.2 %all_to_all.15.parts_ref = bf16[8,64,128]{2,1,0:T(8,128)(2,1)S(1)} all-to-all(bf16[8,64,128]{2,1,0:T(8,128)(2,1)S(1)} %add_convert_fusion.1), channel_id=1, replica_groups={{10,12,14,0,2,4,6,8},{11,13,15,1,3,5,7,9},{26,28,30,16,18,20,22,24},{27..., dimensions={0} | all-to-all | bytes 262144 | tf_op jit(solution)/shard_map/all_to_all | solution.py:532
  21.2 0.2 dispatch_rows.1
  21.4 22.6 %all_to_all.16 = bf16[128,3,4,128]{3,2,1,0:T(4,128)(2,1)S(1)} all-to-all(bf16[128,3,4,128]{3,2,1,0:T(4,128)(2,1)S(1)} %bitcast.32), channel_id=1, replica_groups={{170,186,202,218,234,250,10,26,42,58,74,90,106,122,138,154,172,188,204,..., dimensions={0} | all-to-all | bytes 786432 | tf_op jit(solution)/shard_map/all_to_all | solution.py:532
  44.0 2.3 %collective-permute-start.1 = (bf16[8,192,128]{2,1,0:T(8,128)(2,1)S(1)}, bf16[8,192,128]{2,1,0:T(8,128)(2,1)S(1)}, u32[]{:S(2)}, u32[]{:S(2)}) collective-permute-start(bf16[8,192,128]{2,1,0:T(8,128)(2,1)S(1)} %bitcast.30), channel_id=1, source_target_pairs={{0,1},{1,0},{2,3},{3,2},{4,5},{5,4},{6,7},{7,6},{8,9},{9,8},{10,11... | collective-permute-start | bytes 1179656 | tf_op jit(solution)/shard_map/ppermute | solution.py:528
  46.3 0.0 copy-done.2
  46.3 0.0 copy-done.1
  46.3 0.0 copy-done.4
  46.4 0.0 copy-start.3
  46.4 0.8 %own_half.1 = (f32[192,128]{1,0:T(8,128)S(1)}, f32[192,448]{1,0:T(8,128)S(1)}, f32[192,448]{1,0:T(8,128)S(1)}) custom-call(bf16[8,192,128]{2,1,0:T(8,128)(2,1)S(1)} %bitcast.31, f32[1,2048]{1,0:T(1,128)S(1)} %bitcast.33, bf16[448,2048]{1,0:T(8,128)(2,1)S(1)} %bitcast.23, bf16[448,2048]{1,0:T(8,128)(2,1)S(1)} %bitcast.25), custom_call_target="tpu_custom_call" | custom-call | tf_op jit(solution)/shard_map/own_half/pallas_call | solution.py:463
  47.1 0.6 collective-permute-done.1.rows_ref
  47.7 0.2 copy-done.3
  47.9 1.2 %other_half.1 = (bf16[192,448]{1,0:T(8,128)(2,1)S(1)}, bf16[8,192,128]{2,1,0:T(8,128)(2,1)S(1)}) custom-call(bf16[8,192,128]{2,1,0:T(8,128)(2,1)S(1)} %collective-permute-done.1.rows_ref, f32[1,2048]{1,0:T(1,128)S(1)} %bitcast.34, bf16[448,2048]{1,0:T(8,128)(2,1)S(1)} %bitcast.24, bf16[448,2048]{1,0:T(8,128)(2,1)S(1)} %bitcast.26, ...), custom_call_target="tpu_custom_call" | custom-call | tf_op jit(solution)/shard_map/other_half/pallas_call | solution.py:463
  49.1 0.3 collective-permute-start.2
  49.4 0.5 keep_half.1
  49.9 1.0 %collective-permute-done.2 = bf16[8,192,128]{2,1,0:T(8,128)(2,1)S(1)} collective-permute-done((bf16[8,192,128]{2,1,0:T(8,128)(2,1)S(1)}, bf16[8,192,128]{2,1,0:T(8,128)(2,1)S(1)}, u32[]{:S(2)}, u32[]{:S(2)}) %collective-permute-start.2) | collective-permute-done | bytes 393248 | tf_op jit(solution)/shard_map/ppermute | solution.py:528
  50.9 0.8 %add_convert_fusion = bf16[8,192,128]{2,1,0:T(8,128)(2,1)} fusion(f32[8,192,128]{2,1,0:T(8,128)S(1)} %keep_half.1, bf16[8,192,128]{2,1,0:T(8,128)(2,1)S(1)} %collective-permute-done.2), kind=kLoop, calls=%fused_computation | loop fusion | flops 589824 | bytes 1572864 | tf_op jit(solution)/shard_map/convert_element_type | solution.py:501
  51.8 13.1 %all-to-all-start.2 = ((bf16[128,3,4,128]{3,2,1,0:T(4,128)(2,1)}), bf16[128,3,4,128]{3,2,1,0:T(4,128)(2,1)S(1)}, u32[]{:S(2)}, u32[]{:S(2)}) async-start(bf16[128,3,4,128]{3,2,1,0:T(4,128)(2,1)} %bitcast.16), calls=%async_computation.2 | async-start | bytes 786432 | tf_op jit(solution)/shard_map/all_to_all | solution.py:532
  64.9 7.5 %update_state.1 = f32[8192,64]{1,0:T(8,128)} custom-call(f32[8192,64]{1,0:T(8,128)} %bitcast.21, f32[64,128]{1,0:T(8,128)S(1)} %get-tuple-element.48.removed_ref, f32[64,128]{1,0:T(8,128)S(1)} %get-tuple-element.29.unit_rate_ref, f32[64,128]{1,0:T(8,128)S(1)} %get-tuple-element.49.decay_ref, f32[64,128]{1,0:T(8,128)S(1)} %get-tuple-element.30.key_ref, ...), custom_call_target="tpu_custom_call" | custom-call | flops 2000000000 | bytes 8388608 | tf_op jit(solution)/shard_map/update_state/pallas_call | solution.py:347
  72.3 1.9 %all-to-all-done.2 = bf16[128,3,4,128]{3,2,1,0:T(4,128)(2,1)S(1)} async-done(((bf16[128,3,4,128]{3,2,1,0:T(4,128)(2,1)}), bf16[128,3,4,128]{3,2,1,0:T(4,128)(2,1)S(1)}, u32[]{:S(2)}, u32[]{:S(2)}) %all-to-all-start.2) | async-done | bytes 393248 | tf_op jit(solution)/shard_map/all_to_all | solution.py:532
  74.2 0.9 %combine.1 = bf16[64,128]{1,0:T(8,128)(2,1)} custom-call(f32[192,64]{1,0:T(8,128)S(1)} %get-tuple-element.26.share_ref, bf16[8,192,128]{2,1,0:T(8,128)(2,1)S(1)} %bitcast.29, bf16[64,128]{1,0:T(8,128)(2,1)S(1)} %get-tuple-element.47.resid_ref), custom_call_target="tpu_custom_call" | custom-call | tf_op jit(solution)/shard_map/combine/pallas_call | solution.py:519
  (1 shorter events, 0.0 us)
Async XLA Ops:
  0.6 3.6 %copy-start = (f32[64,2,64,64]{3,2,1,0:T(8,128)S(1)}, f32[64,2,64,64]{3,2,1,0:T(8,128)}, u32[]{:S(2)}) copy-start(f32[64,2,64,64]{3,2,1,0:T(8,128)} %param.20) | copy-start | bytes 6291460
  0.6 3.6 %copy-start.5 = (f32[128]{0:T(128)S(1)}, f32[128]{0:T(128)}, u32[]{:S(2)}) copy-start(f32[128]{0:T(128)} %param.32) | copy-start | bytes 1540
  4.3 42.1 %copy-start.2 = (bf16[1,2048,448]{1,2,0:T(8,128)(2,1)S(1)}, bf16[1,2048,448]{1,2,0:T(8,128)(2,1)}, u32[]{:S(2)}) copy-start(bf16[1,2048,448]{1,2,0:T(8,128)(2,1)} %param.36) | copy-start | bytes 5505028
  5.7 40.6 %copy-start.1 = (bf16[1,2048,448]{1,2,0:T(8,128)(2,1)S(1)}, bf16[1,2048,448]{1,2,0:T(8,128)(2,1)}, u32[]{:S(2)}) copy-start(bf16[1,2048,448]{1,2,0:T(8,128)(2,1)} %param.35) | copy-start | bytes 5505028
  5.7 40.6 %copy-start.4 = (f32[2048]{0:T(1024)S(1)}, f32[2048]{0:T(1024)}, u32[]{:S(2)}) copy-start(f32[2048]{0:T(1024)} %param.34) | copy-start | bytes 24580
  5.7 4.3 %collective-permute-start = (bf16[8,64,128]{2,1,0:T(8,128)(2,1)S(1)}, bf16[8,64,128]{2,1,0:T(8,128)(2,1)S(1)}, u32[]{:S(2)}, u32[]{:S(2)}) collective-permute-start(bf16[8,64,128]{2,1,0:T(8,128)(2,1)S(1)} %get-tuple-element.34), channel_id=1, source_target_pairs={{0,1},{1,0},{2,3},{3,2},{4,5},{5,4},{6,7},{7,6},{8,9},{9,8},{10,11... | collective-permute-start | bytes 393224 | tf_op jit(solution)/shard_map/ppermute | solution.py:528
  44.0 3.7 %collective-permute-start.1 = (bf16[8,192,128]{2,1,0:T(8,128)(2,1)S(1)}, bf16[8,192,128]{2,1,0:T(8,128)(2,1)S(1)}, u32[]{:S(2)}, u32[]{:S(2)}) collective-permute-start(bf16[8,192,128]{2,1,0:T(8,128)(2,1)S(1)} %bitcast.30), channel_id=1, source_target_pairs={{0,1},{1,0},{2,3},{3,2},{4,5},{5,4},{6,7},{7,6},{8,9},{9,8},{10,11... | collective-permute-start | bytes 1179656 | tf_op jit(solution)/shard_map/ppermute | solution.py:528
  46.4 1.5 %copy-start.3 = (bf16[1,448,2048]{2,1,0:T(8,128)(2,1)S(1)}, bf16[1,448,2048]{2,1,0:T(8,128)(2,1)}, u32[]{:S(2)}) copy-start(bf16[1,448,2048]{2,1,0:T(8,128)(2,1)} %param.37) | copy-start | bytes 5505028
  49.1 1.8 %collective-permute-start.2 = (bf16[8,192,128]{2,1,0:T(8,128)(2,1)S(1)}, bf16[8,192,128]{2,1,0:T(8,128)(2,1)S(1)}, u32[]{:S(2)}, u32[]{:S(2)}) collective-permute-start(bf16[8,192,128]{2,1,0:T(8,128)(2,1)S(1)} %get-tuple-element.46), channel_id=1, source_target_pairs={{0,1},{1,0},{2,3},{3,2},{4,5},{5,4},{6,7},{7,6},{8,9},{9,8},{10,11... | collective-permute-start | bytes 1179656 | tf_op jit(solution)/shard_map/ppermute | solution.py:528
  51.8 22.4 %all-to-all-start.2 = ((bf16[128,3,4,128]{3,2,1,0:T(4,128)(2,1)}), bf16[128,3,4,128]{3,2,1,0:T(4,128)(2,1)S(1)}, u32[]{:S(2)}, u32[]{:S(2)}) async-start(bf16[128,3,4,128]{3,2,1,0:T(4,128)(2,1)} %bitcast.16), calls=%async_computation.2 | async-start | bytes 786432 | tf_op jit(solution)/shard_map/all_to_all | solution.py:532

commit v8 on v7

--- a/solution.py
+++ b/solution.py
@@ -386,19 +386,21 @@
 ACROSS = (((1,), (1,)), ((), ()))
 
 
-def core_columns(ref, core):
-    blocks = ref.shape[1] // (2 * LANES)
+def core_columns(ref, core, first=0, count=None):
+    blocks = z_order(ref.shape[1] // (2 * LANES))
+    count = len(blocks) if count is None else count
     return jnp.concatenate(
         [
             ref[:, pl.ds(pl.multiple_of((2 * z + core) * LANES, LANES), LANES)]
-            for z in z_order(blocks)
+            for z in blocks[first : first + count]
         ],
         axis=1,
     )
 
 
-def half_products(rows_ref, gain_ref, gate_ref, up_ref, core):
-    gain = core_columns(gain_ref, core)
+def half_products(rows_ref, gain_ref, gate_ref, up_ref, core, first=0):
+    count = rows_ref.shape[0]
+    gain = core_columns(gain_ref, core, first, count)
     squares = jnp.zeros(rows_ref.shape[1:], F32)
     parts = []
     for z in range(rows_ref.shape[0]):
@@ -407,19 +409,40 @@
         parts.append((rows * gain[:, z * LANES : (z + 1) * LANES]).astype(BF16))
     x = jnp.concatenate(parts, axis=1)
     gate = lax.dot_general(
-        x, core_columns(gate_ref, core), ACROSS, preferred_element_type=F32
+        x, core_columns(gate_ref, core, first, count), ACROSS, preferred_element_type=F32
     )
     upward = lax.dot_general(
-        x, core_columns(up_ref, core), ACROSS, preferred_element_type=F32
+        x, core_columns(up_ref, core, first, count), ACROSS, preferred_element_type=F32
     )
     return squares, gate, upward
 
 
-def own_half_kernel(rows_ref, gain_ref, gate_ref, up_ref, squares_ref, gate_out, up_out):
+def own_half_kernel(
+    rows_ref, gain_ref, gate_ref, up_ref, down_ref, squares_ref, gate_out, up_out
+):
     core = lax.axis_index("tp_1")
     squares_ref[...], gate_out[...], up_out[...] = half_products(
         rows_ref, gain_ref, gate_ref, up_ref, core
     )
+
+
+def other_first_kernel(
+    rows_ref,
+    gain_ref,
+    gate_ref,
+    up_ref,
+    squares_part_ref,
+    gate_part_ref,
+    up_part_ref,
+    squares_ref,
+    gate_out,
+    up_out,
+):
+    other = 1 - lax.axis_index("tp_1")
+    squares, gate, upward = half_products(rows_ref, gain_ref, gate_ref, up_ref, other)
+    squares_ref[...] = squares + squares_part_ref[...]
+    gate_out[...] = gate + gate_part_ref[...]
+    up_out[...] = upward + up_part_ref[...]
 
 
 def other_half_kernel(
@@ -435,7 +458,9 @@
     send_ref,
 ):
     other = 1 - lax.axis_index("tp_1")
-    squares, gate, upward = half_products(rows_ref, gain_ref, gate_ref, up_ref, other)
+    squares, gate, upward = half_products(
+        rows_ref, gain_ref, gate_ref, up_ref, other, send_ref.shape[0] - rows_ref.shape[0]
+    )
     square_sum = jnp.sum(squares + squares_ref[...], axis=1, keepdims=True)
     scale = lax.rsqrt(square_sum / gate_ref.shape[1] + RMS_EPS)
     gate = (gate + gate_part_ref[...]) * scale
@@ -469,17 +494,15 @@
             name=name,
         )(*operands)
 
-    other = swap(own)
+    middle = own.shape[0] // 2
+    other_first, other_last = swap(own[:middle]), swap(own[middle:])
+    sums = (jax.ShapeDtypeStruct((rows, LANES), F32), part, part)
+    partial = call(own_half_kernel, "own_half", own, gain, gate, up, down, out_shape=sums)
+    other_first, partial = lax.optimization_barrier((other_first, partial))
     partial = call(
-        own_half_kernel,
-        "own_half",
-        own,
-        gain,
-        gate,
-        up,
-        out_shape=(jax.ShapeDtypeStruct((rows, LANES), F32), part, part),
-    )
-    other, partial = lax.optimization_barrier((other, partial))
+        other_first_kernel, "other_first", other_first, gain, gate, up, *partial, out_shape=sums
+    )
+    other, partial = lax.optimization_barrier((other_last, partial))
     hidden, send = call(
         other_half_kernel,
         "other_half",

time: 75.5 us -> 75.3 us (level)
    ppermute x3 -> x4, waiting for transfers between devices: 2.38 us -> 1.84 us  [swap(): return lax.ppermute(shard, 'tp_1', [(0, 1), (1, 0)])]
    ppermute x3 -> x4, starting transfers between devices: 5.9 us -> 6.25 us  [swap(): return lax.ppermute(shard, 'tp_1', [(0, 1), (1, 0)])]
    pallas_call x3 -> x4, Pallas kernels: 2.47 us -> 2.6 us  [call(): pl.pallas_call(body, out_shape=out_shape, in_specs=[vmem] * len(operands)...]
  transfers between devices with their start and end apart: 4 -> 5, of which waited for: 4 -> 4; matrix products, arithmetic and copies ran while one was open for 0% -> 0% of each run, Pallas kernels for 12% -> 13%
where the time goes in v8:
time: 75.3 us; the launch traced here: 74.9 us
  blocking collectives  33.8 us (45%)
  starting transfers between devices  19.4 us (26%)
  Pallas kernels  16.3 us (22%)
  waiting for transfers between devices  3.57 us (5%)
  other arithmetic  0.87 us (1%)
  between operations  0.78 us (1%)
    all_to_all x2, blocking collectives, exchange(): lax.all_to_all(shard, axis, split_axis=0, concat_axis=0, axis_index_group...  33.8 us
    all_to_all x1, starting transfers between devices, exchange(): lax.all_to_all(shard, axis, split_axis=0, concat_axis=0, axis_index_group...  13.1 us
    pallas_call x1, Pallas kernels, update_state(): pl.pallas_call(update_kernel, grid=(steps,), out_shape=jax.ShapeDtypeStru...  7.47 us
    ppermute x4, starting transfers between devices, swap(): return lax.ppermute(shard, 'tp_1', [(0, 1), (1, 0)])  6.25 us
    pallas_call x1, Pallas kernels, project_heads(): pl.pallas_call(project_kernel, out_shape=(jax.ShapeDtypeStruct((seqs * 8,...  3.57 us
    pallas_call x4, Pallas kernels, call(): pl.pallas_call(body, out_shape=out_shape, in_specs=[vmem] * len(operands)...  2.6 us
    ppermute x4, waiting for transfers between devices, swap(): return lax.ppermute(shard, 'tp_1', [(0, 1), (1, 0)])  1.84 us
    all_to_all x1, waiting for transfers between devices, exchange(): lax.all_to_all(shard, axis, split_axis=0, concat_axis=0, axis_index_group...  1.72 us
  transfers between devices with their start and end apart: 5, of which 4 were waited for; matrix products, arithmetic and copies ran while one was open for 0% of the time, Pallas kernels for 13%

profile of v8, /device:TPU:1, one launch (start us, length us, event | category | flops | bytes accessed | tf_op | source)
XLA Modules:
  0.0 74.9 jit_solution(12884341038091314034)
XLA Ops:
  0.6 0.0 copy-start
  0.6 0.0 copy-start.5
  0.7 3.6 %project_heads.1 = (f32[512,128]{1,0:T(8,128)S(1)}, f32[64,128]{1,0:T(8,128)S(1)}, f32[64,128]{1,0:T(8,128)S(1)}, f32[64,128]{1,0:T(8,128)S(1)}, f32[64,128]{1,0...) custom-call(bf16[64,2048]{1,0:T(8,128)(2,1)} %tokens_hbm.1, ...), custom_call_target="tpu_custom_call" | custom-call | flops 3000000000 | bytes 6291456 | tf_op jit(solution)/shard_map/project_heads/pallas_call | solution.py:172
  4.3 0.0 copy-start.2
  4.3 0.0 copy-start.3
  4.3 1.4 %mix.1 = (bf16[8,64,128]{2,1,0:T(8,128)(2,1)S(1)}, f32[64,128]{1,0:T(8,128)S(1)}, bf16[64,128]{1,0:T(8,128)(2,1)S(1)}, bf16[128,2048]{1,0:T(8,128)(2,1)S(1)}) custom-call(f32[8192,64]{1,0:T(8,128)S(1)} %bitcast.24, f32[512,128]{1,0:T(8,128)S(1)} %get-tuple-element.34.vectors_ref, f32[64,128]{1,0:T(8,128)S(1)} %get-tuple-element.35.recept_ref, ...), custom_call_target="tpu_custom_call" | custom-call | tf_op jit(solution)/shard_map/mix/pallas_call | solution.py:268
  5.7 0.0 copy-start.1
  5.7 0.0 copy-start.4
  5.7 3.3 %collective-permute-start = (bf16[8,64,128]{2,1,0:T(8,128)(2,1)S(1)}, bf16[8,64,128]{2,1,0:T(8,128)(2,1)S(1)}, u32[]{:S(2)}, u32[]{:S(2)}) collective-permute-start(bf16[8,64,128]{2,1,0:T(8,128)(2,1)S(1)} %get-tuple-element.41), channel_id=1, source_target_pairs={{0,1},{1,0},{2,3},{3,2},{4,5},{5,4},{6,7},{7,6},{8,9},{9,8},{10,11... | collective-permute-start | bytes 393224 | tf_op jit(solution)/shard_map/ppermute | solution.py:551
  9.0 0.2 keep_out.1
  9.2 0.8 %collective-permute-done = bf16[8,64,128]{2,1,0:T(8,128)(2,1)S(1)} collective-permute-done((bf16[8,64,128]{2,1,0:T(8,128)(2,1)S(1)}, bf16[8,64,128]{2,1,0:T(8,128)(2,1)S(1)}, u32[]{:S(2)}, u32[]{:S(2)}) %collective-permute-start) | collective-permute-done | bytes 131104 | tf_op jit(solution)/shard_map/ppermute | solution.py:551
  10.1 11.2 %all_to_all.15.parts_ref = bf16[8,64,128]{2,1,0:T(8,128)(2,1)S(1)} all-to-all(bf16[8,64,128]{2,1,0:T(8,128)(2,1)S(1)} %add_convert_fusion.1), channel_id=1, replica_groups={{10,12,14,0,2,4,6,8},{11,13,15,1,3,5,7,9},{26,28,30,16,18,20,22,24},{27..., dimensions={0} | all-to-all | bytes 262144 | tf_op jit(solution)/shard_map/all_to_all | solution.py:555
  21.2 0.2 dispatch_rows.1
  21.4 22.6 %all_to_all.16 = bf16[128,3,4,128]{3,2,1,0:T(4,128)(2,1)S(1)} all-to-all(bf16[128,3,4,128]{3,2,1,0:T(4,128)(2,1)S(1)} %bitcast.36), channel_id=1, replica_groups={{170,186,202,218,234,250,10,26,42,58,74,90,106,122,138,154,172,188,204,..., dimensions={0} | all-to-all | bytes 786432 | tf_op jit(solution)/shard_map/all_to_all | solution.py:555
  44.0 0.1 fusion
  44.2 2.4 %collective-permute-start.2 = (bf16[4,192,128]{2,1,0:T(8,128)(2,1)S(1)}, bf16[4,192,128]{2,1,0:T(8,128)(2,1)S(1)}, u32[]{:S(2)}, u32[]{:S(2)}) collective-permute-start(bf16[4,192,128]{2,1,0:T(8,128)(2,1)S(1)} %bitcast.43), channel_id=1, source_target_pairs={{0,1},{1,0},{2,3},{3,2},{4,5},{5,4},{6,7},{7,6},{8,9},{9,8},{10,11... | collective-permute-start | bytes 589832 | tf_op jit(solution)/shard_map/ppermute | solution.py:551
  46.6 0.1 collective-permute-start.1
  46.7 0.0 copy-done.3
  46.7 0.0 copy-done.4
  46.7 0.8 %own_half.1 = (f32[192,128]{1,0:T(8,128)S(1)}, f32[192,448]{1,0:T(8,128)S(1)}, f32[192,448]{1,0:T(8,128)S(1)}) custom-call(bf16[8,192,128]{2,1,0:T(8,128)(2,1)S(1)} %bitcast.34, f32[1,2048]{1,0:T(1,128)S(1)} %bitcast.37, bf16[448,2048]{1,0:T(8,128)(2,1)S(1)} %bitcast.25, bf16[448,2048]{1,0:T(8,128)(2,1)S(1)} %bitcast.28, bf16[448,2048]{1,0:T(8,128)(2,1)S(1)} %bitcast.31), custom_call_target="tpu_custom_call" | custom-call | tf_op jit(solution)/shard_map/own_half/pallas_call | solution.py:488
  47.5 0.2 collective-permute-done.2.rows_ref
  47.7 0.5 other_first.1
  48.1 0.0 collective-permute-done.1.rows_ref
  48.1 0.9 %other_half.1 = (bf16[192,448]{1,0:T(8,128)(2,1)S(1)}, bf16[8,192,128]{2,1,0:T(8,128)(2,1)S(1)}) custom-call(bf16[4,192,128]{2,1,0:T(8,128)(2,1)S(1)} %collective-permute-done.1.rows_ref, f32[1,2048]{1,0:T(1,128)S(1)} %bitcast.39, bf16[448,2048]{1,0:T(8,128)(2,1)S(1)} %bitcast.27, bf16[448,2048]{1,0:T(8,128)(2,1)S(1)} %bitcast.30, ...), custom_call_target="tpu_custom_call" | custom-call | tf_op jit(solution)/shard_map/other_half/pallas_call | solution.py:488
  49.0 0.5 collective-permute-start.3
  49.5 0.5 keep_half.1
  50.0 0.9 %collective-permute-done.3 = bf16[8,192,128]{2,1,0:T(8,128)(2,1)S(1)} collective-permute-done((bf16[8,192,128]{2,1,0:T(8,128)(2,1)S(1)}, bf16[8,192,128]{2,1,0:T(8,128)(2,1)S(1)}, u32[]{:S(2)}, u32[]{:S(2)}) %collective-permute-start.3) | collective-permute-done | bytes 393248 | tf_op jit(solution)/shard_map/ppermute | solution.py:551
  50.9 0.8 %add_convert_fusion = bf16[8,192,128]{2,1,0:T(8,128)(2,1)} fusion(f32[8,192,128]{2,1,0:T(8,128)S(1)} %keep_half.1, bf16[8,192,128]{2,1,0:T(8,128)(2,1)S(1)} %collective-permute-done.3), kind=kLoop, calls=%fused_computation | loop fusion | flops 589824 | bytes 1572864 | tf_op jit(solution)/shard_map/convert_element_type | solution.py:524
  51.7 13.1 %all-to-all-start.2 = ((bf16[128,3,4,128]{3,2,1,0:T(4,128)(2,1)}), bf16[128,3,4,128]{3,2,1,0:T(4,128)(2,1)S(1)}, u32[]{:S(2)}, u32[]{:S(2)}) async-start(bf16[128,3,4,128]{3,2,1,0:T(4,128)(2,1)} %bitcast.18), calls=%async_computation.2 | async-start | bytes 786432 | tf_op jit(solution)/shard_map/all_to_all | solution.py:555
  64.8 7.5 %update_state.1 = f32[8192,64]{1,0:T(8,128)} custom-call(f32[8192,64]{1,0:T(8,128)} %bitcast.23, f32[64,128]{1,0:T(8,128)S(1)} %get-tuple-element.62.removed_ref, f32[64,128]{1,0:T(8,128)S(1)} %get-tuple-element.36.unit_rate_ref, f32[64,128]{1,0:T(8,128)S(1)} %get-tuple-element.63.decay_ref, f32[64,128]{1,0:T(8,128)S(1)} %get-tuple-element.37.key_ref, ...), custom_call_target="tpu_custom_call" | custom-call | flops 2000000000 | bytes 8388608 | tf_op jit(solution)/shard_map/update_state/pallas_call | solution.py:347
  72.3 1.7 %all-to-all-done.2 = bf16[128,3,4,128]{3,2,1,0:T(4,128)(2,1)S(1)} async-done(((bf16[128,3,4,128]{3,2,1,0:T(4,128)(2,1)}), bf16[128,3,4,128]{3,2,1,0:T(4,128)(2,1)S(1)}, u32[]{:S(2)}, u32[]{:S(2)}) %all-to-all-start.2) | async-done | bytes 393248 | tf_op jit(solution)/shard_map/all_to_all | solution.py:555
  74.0 0.9 %combine.1 = bf16[64,128]{1,0:T(8,128)(2,1)} custom-call(f32[192,64]{1,0:T(8,128)S(1)} %get-tuple-element.33.share_ref, bf16[8,192,128]{2,1,0:T(8,128)(2,1)S(1)} %bitcast.35, bf16[64,128]{1,0:T(8,128)(2,1)S(1)} %get-tuple-element.61.resid_ref), custom_call_target="tpu_custom_call" | custom-call | tf_op jit(solution)/shard_map/combine/pallas_call | solution.py:542
  (5 shorter events, 0.0 us)
Async XLA Ops:
  0.6 3.6 %copy-start = (f32[64,2,64,64]{3,2,1,0:T(8,128)S(1)}, f32[64,2,64,64]{3,2,1,0:T(8,128)}, u32[]{:S(2)}) copy-start(f32[64,2,64,64]{3,2,1,0:T(8,128)} %param.20) | copy-start | bytes 6291460
  0.6 3.6 %copy-start.5 = (f32[128]{0:T(128)S(1)}, f32[128]{0:T(128)}, u32[]{:S(2)}) copy-start(f32[128]{0:T(128)} %param.32) | copy-start | bytes 1540
  4.3 42.4 %copy-start.2 = (bf16[1,2048,448]{1,2,0:T(8,128)(2,1)S(1)}, bf16[1,2048,448]{1,2,0:T(8,128)(2,1)}, u32[]{:S(2)}) copy-start(bf16[1,2048,448]{1,2,0:T(8,128)(2,1)} %param.36) | copy-start | bytes 5505028
  4.3 42.4 %copy-start.3 = (bf16[1,448,2048]{2,1,0:T(8,128)(2,1)S(1)}, bf16[1,448,2048]{2,1,0:T(8,128)(2,1)}, u32[]{:S(2)}) copy-start(bf16[1,448,2048]{2,1,0:T(8,128)(2,1)} %param.37) | copy-start | bytes 5505028
  5.7 41.0 %copy-start.1 = (bf16[1,2048,448]{1,2,0:T(8,128)(2,1)S(1)}, bf16[1,2048,448]{1,2,0:T(8,128)(2,1)}, u32[]{:S(2)}) copy-start(bf16[1,2048,448]{1,2,0:T(8,128)(2,1)} %param.35) | copy-start | bytes 5505028
  5.7 41.0 %copy-start.4 = (f32[2048]{0:T(1024)S(1)}, f32[2048]{0:T(1024)}, u32[]{:S(2)}) copy-start(f32[2048]{0:T(1024)} %param.34) | copy-start | bytes 24580
  5.7 4.3 %collective-permute-start = (bf16[8,64,128]{2,1,0:T(8,128)(2,1)S(1)}, bf16[8,64,128]{2,1,0:T(8,128)(2,1)S(1)}, u32[]{:S(2)}, u32[]{:S(2)}) collective-permute-start(bf16[8,64,128]{2,1,0:T(8,128)(2,1)S(1)} %get-tuple-element.41), channel_id=1, source_target_pairs={{0,1},{1,0},{2,3},{3,2},{4,5},{5,4},{6,7},{7,6},{8,9},{9,8},{10,11... | collective-permute-start | bytes 393224 | tf_op jit(solution)/shard_map/ppermute | solution.py:551
  44.2 3.5 %collective-permute-start.2 = (bf16[4,192,128]{2,1,0:T(8,128)(2,1)S(1)}, bf16[4,192,128]{2,1,0:T(8,128)(2,1)S(1)}, u32[]{:S(2)}, u32[]{:S(2)}) collective-permute-start(bf16[4,192,128]{2,1,0:T(8,128)(2,1)S(1)} %bitcast.43), channel_id=1, source_target_pairs={{0,1},{1,0},{2,3},{3,2},{4,5},{5,4},{6,7},{7,6},{8,9},{9,8},{10,11... | collective-permute-start | bytes 589832 | tf_op jit(solution)/shard_map/ppermute | solution.py:551
  46.6 1.6 %collective-permute-start.1 = (bf16[4,192,128]{2,1,0:T(8,128)(2,1)S(1)}, bf16[4,192,128]{2,1,0:T(8,128)(2,1)S(1)}, u32[]{:S(2)}, u32[]{:S(2)}) collective-permute-start(bf16[4,192,128]{2,1,0:T(8,128)(2,1)S(1)} %bitcast.42), channel_id=1, source_target_pairs={{0,1},{1,0},{2,3},{3,2},{4,5},{5,4},{6,7},{7,6},{8,9},{9,8},{10,11... | collective-permute-start | bytes 589832 | tf_op jit(solution)/shard_map/ppermute | solution.py:551
  49.0 1.8 %collective-permute-start.3 = (bf16[8,192,128]{2,1,0:T(8,128)(2,1)S(1)}, bf16[8,192,128]{2,1,0:T(8,128)(2,1)S(1)}, u32[]{:S(2)}, u32[]{:S(2)}) collective-permute-start(bf16[8,192,128]{2,1,0:T(8,128)(2,1)S(1)} %get-tuple-element.60), channel_id=1, source_target_pairs={{0,1},{1,0},{2,3},{3,2},{4,5},{5,4},{6,7},{7,6},{8,9},{9,8},{10,11... | collective-permute-start | bytes 1179656 | tf_op jit(solution)/shard_map/ppermute | solution.py:551
  51.7 22.3 %all-to-all-start.2 = ((bf16[128,3,4,128]{3,2,1,0:T(4,128)(2,1)}), bf16[128,3,4,128]{3,2,1,0:T(4,128)(2,1)S(1)}, u32[]{:S(2)}, u32[]{:S(2)}) async-start(bf16[128,3,4,128]{3,2,1,0:T(4,128)(2,1)} %bitcast.18), calls=%async_computation.2 | async-start | bytes 786432 | tf_op jit(solution)/shard_map/all_to_all | solution.py:555

commit v9 on v8

--- a/solution.py
+++ b/solution.py
@@ -22,7 +22,7 @@
 
 
 def z_order(count):
-    return [(FIRST_Z + step) % count for step in range(count)]
+    return [(FIRST_Z + 3 * step) % count for step in range(count)]
 
 
 def ep_order(count):

time: 75.3 us -> 75.2 us (level)
  transfers between devices with their start and end apart: 5 -> 5, of which waited for: 4 -> 4; matrix products, arithmetic and copies ran while one was open for 0% -> 0% of each run, Pallas kernels for 13% -> 12%
where the time goes in v9:
time: 75.2 us; the launch traced here: 74.9 us
  blocking collectives  33.4 us (44%)
  starting transfers between devices  19.6 us (26%)
  Pallas kernels  16.3 us (22%)
  waiting for transfers between devices  3.75 us (5%)
  other arithmetic  0.87 us (1%)
  between operations  0.78 us (1%)
    all_to_all x2, blocking collectives, exchange(): lax.all_to_all(shard, axis, split_axis=0, concat_axis=0, axis_index_group...  33.4 us
    all_to_all x1, starting transfers between devices, exchange(): lax.all_to_all(shard, axis, split_axis=0, concat_axis=0, axis_index_group...  13.1 us
    pallas_call x1, Pallas kernels, update_state(): pl.pallas_call(update_kernel, grid=(steps,), out_shape=jax.ShapeDtypeStru...  7.47 us
    ppermute x4, starting transfers between devices, swap(): return lax.ppermute(shard, 'tp_1', [(0, 1), (1, 0)])  6.47 us
    pallas_call x1, Pallas kernels, project_heads(): pl.pallas_call(project_kernel, out_shape=(jax.ShapeDtypeStruct((seqs * 8,...  3.57 us
    pallas_call x4, Pallas kernels, call(): pl.pallas_call(body, out_shape=out_shape, in_specs=[vmem] * len(operands)...  2.57 us
    all_to_all x1, waiting for transfers between devices, exchange(): lax.all_to_all(shard, axis, split_axis=0, concat_axis=0, axis_index_group...  1.88 us
    ppermute x4, waiting for transfers between devices, swap(): return lax.ppermute(shard, 'tp_1', [(0, 1), (1, 0)])  1.87 us
  transfers between devices with their start and end apart: 5, of which 4 were waited for; matrix products, arithmetic and copies ran while one was open for 0% of the time, Pallas kernels for 12%

profile of v9, /device:TPU:1, one launch (start us, length us, event | category | flops | bytes accessed | tf_op | source)
XLA Modules:
  0.0 74.9 jit_solution(13109426960640902498)
XLA Ops:
  0.6 0.0 copy-start
  0.7 3.6 %project_heads.1 = (f32[512,128]{1,0:T(8,128)S(1)}, f32[64,128]{1,0:T(8,128)S(1)}, f32[64,128]{1,0:T(8,128)S(1)}, f32[64,128]{1,0:T(8,128)S(1)}, f32[64,128]{1,0...) custom-call(bf16[64,2048]{1,0:T(8,128)(2,1)} %tokens_hbm.1, ...), custom_call_target="tpu_custom_call" | custom-call | flops 3000000000 | bytes 6291456 | tf_op jit(solution)/shard_map/project_heads/pallas_call | solution.py:172
  4.2 0.0 copy-done
  4.2 0.0 copy-done.5
  4.3 0.0 copy-start.2
  4.3 0.0 copy-start.3
  4.3 1.4 %mix.1 = (bf16[8,64,128]{2,1,0:T(8,128)(2,1)S(1)}, f32[64,128]{1,0:T(8,128)S(1)}, bf16[64,128]{1,0:T(8,128)(2,1)S(1)}, bf16[128,2048]{1,0:T(8,128)(2,1)S(1)}) custom-call(f32[8192,64]{1,0:T(8,128)S(1)} %bitcast.24, f32[512,128]{1,0:T(8,128)S(1)} %get-tuple-element.34.vectors_ref, f32[64,128]{1,0:T(8,128)S(1)} %get-tuple-element.35.recept_ref, ...), custom_call_target="tpu_custom_call" | custom-call | tf_op jit(solution)/shard_map/mix/pallas_call | solution.py:268
  5.7 0.0 copy-start.1
  5.7 0.0 copy-start.4
  5.7 3.3 %collective-permute-start = (bf16[8,64,128]{2,1,0:T(8,128)(2,1)S(1)}, bf16[8,64,128]{2,1,0:T(8,128)(2,1)S(1)}, u32[]{:S(2)}, u32[]{:S(2)}) collective-permute-start(bf16[8,64,128]{2,1,0:T(8,128)(2,1)S(1)} %get-tuple-element.41), channel_id=1, source_target_pairs={{0,1},{1,0},{2,3},{3,2},{4,5},{5,4},{6,7},{7,6},{8,9},{9,8},{10,11... | collective-permute-start | bytes 393224 | tf_op jit(solution)/shard_map/ppermute | solution.py:551
  9.0 0.2 keep_out.1
  9.2 0.8 %collective-permute-done = bf16[8,64,128]{2,1,0:T(8,128)(2,1)S(1)} collective-permute-done((bf16[8,64,128]{2,1,0:T(8,128)(2,1)S(1)}, bf16[8,64,128]{2,1,0:T(8,128)(2,1)S(1)}, u32[]{:S(2)}, u32[]{:S(2)}) %collective-permute-start) | collective-permute-done | bytes 131104 | tf_op jit(solution)/shard_map/ppermute | solution.py:551
  10.1 11.0 %all_to_all.15.parts_ref = bf16[8,64,128]{2,1,0:T(8,128)(2,1)S(1)} all-to-all(bf16[8,64,128]{2,1,0:T(8,128)(2,1)S(1)} %add_convert_fusion.1), channel_id=1, replica_groups={{10,0,6,12,2,8,14,4},{11,1,7,13,3,9,15,5},{26,16,22,28,18,24,30,20},{27..., dimensions={0} | all-to-all | bytes 262144 | tf_op jit(solution)/shard_map/all_to_all | solution.py:555
  21.0 0.2 dispatch_rows.1
  21.2 22.4 %all_to_all.16 = bf16[128,3,4,128]{3,2,1,0:T(4,128)(2,1)S(1)} all-to-all(bf16[128,3,4,128]{3,2,1,0:T(4,128)(2,1)S(1)} %bitcast.36), channel_id=1, replica_groups={{170,186,202,218,234,250,10,26,42,58,74,90,106,122,138,154,160,176,192,..., dimensions={0} | all-to-all | bytes 786432 | tf_op jit(solution)/shard_map/all_to_all | solution.py:555
  43.6 0.1 fusion
  43.8 2.6 %collective-permute-start.2 = (bf16[4,192,128]{2,1,0:T(8,128)(2,1)S(1)}, bf16[4,192,128]{2,1,0:T(8,128)(2,1)S(1)}, u32[]{:S(2)}, u32[]{:S(2)}) collective-permute-start(bf16[4,192,128]{2,1,0:T(8,128)(2,1)S(1)} %bitcast.43), channel_id=1, source_target_pairs={{0,1},{1,0},{2,3},{3,2},{4,5},{5,4},{6,7},{7,6},{8,9},{9,8},{10,11... | collective-permute-start | bytes 589832 | tf_op jit(solution)/shard_map/ppermute | solution.py:551
  46.4 0.1 collective-permute-start.1
  46.5 0.0 copy-done.2
  46.5 0.8 %own_half.1 = (f32[192,128]{1,0:T(8,128)S(1)}, f32[192,448]{1,0:T(8,128)S(1)}, f32[192,448]{1,0:T(8,128)S(1)}) custom-call(bf16[8,192,128]{2,1,0:T(8,128)(2,1)S(1)} %bitcast.34, f32[1,2048]{1,0:T(1,128)S(1)} %bitcast.37, bf16[448,2048]{1,0:T(8,128)(2,1)S(1)} %bitcast.25, bf16[448,2048]{1,0:T(8,128)(2,1)S(1)} %bitcast.28, bf16[448,2048]{1,0:T(8,128)(2,1)S(1)} %bitcast.31), custom_call_target="tpu_custom_call" | custom-call | tf_op jit(solution)/shard_map/own_half/pallas_call | solution.py:488
  47.3 0.2 collective-permute-done.2.rows_ref
  47.5 0.5 other_first.1
  47.9 0.0 collective-permute-done.1.rows_ref
  48.0 0.9 %other_half.1 = (bf16[192,448]{1,0:T(8,128)(2,1)S(1)}, bf16[8,192,128]{2,1,0:T(8,128)(2,1)S(1)}) custom-call(bf16[4,192,128]{2,1,0:T(8,128)(2,1)S(1)} %collective-permute-done.1.rows_ref, f32[1,2048]{1,0:T(1,128)S(1)} %bitcast.39, bf16[448,2048]{1,0:T(8,128)(2,1)S(1)} %bitcast.27, bf16[448,2048]{1,0:T(8,128)(2,1)S(1)} %bitcast.30, ...), custom_call_target="tpu_custom_call" | custom-call | tf_op jit(solution)/shard_map/other_half/pallas_call | solution.py:488
  48.8 0.5 collective-permute-start.3
  49.3 0.5 keep_half.1
  49.8 0.9 %collective-permute-done.3 = bf16[8,192,128]{2,1,0:T(8,128)(2,1)S(1)} collective-permute-done((bf16[8,192,128]{2,1,0:T(8,128)(2,1)S(1)}, bf16[8,192,128]{2,1,0:T(8,128)(2,1)S(1)}, u32[]{:S(2)}, u32[]{:S(2)}) %collective-permute-start.3) | collective-permute-done | bytes 393248 | tf_op jit(solution)/shard_map/ppermute | solution.py:551
  50.7 0.8 %add_convert_fusion = bf16[8,192,128]{2,1,0:T(8,128)(2,1)} fusion(f32[8,192,128]{2,1,0:T(8,128)S(1)} %keep_half.1, bf16[8,192,128]{2,1,0:T(8,128)(2,1)S(1)} %collective-permute-done.3), kind=kLoop, calls=%fused_computation | loop fusion | flops 589824 | bytes 1572864 | tf_op jit(solution)/shard_map/convert_element_type | solution.py:524
  51.5 13.1 %all-to-all-start.2 = ((bf16[128,3,4,128]{3,2,1,0:T(4,128)(2,1)}), bf16[128,3,4,128]{3,2,1,0:T(4,128)(2,1)S(1)}, u32[]{:S(2)}, u32[]{:S(2)}) async-start(bf16[128,3,4,128]{3,2,1,0:T(4,128)(2,1)} %bitcast.18), calls=%async_computation.2 | async-start | bytes 786432 | tf_op jit(solution)/shard_map/all_to_all | solution.py:555
  64.6 7.5 %update_state.1 = f32[8192,64]{1,0:T(8,128)} custom-call(f32[8192,64]{1,0:T(8,128)} %bitcast.23, f32[64,128]{1,0:T(8,128)S(1)} %get-tuple-element.62.removed_ref, f32[64,128]{1,0:T(8,128)S(1)} %get-tuple-element.36.unit_rate_ref, f32[64,128]{1,0:T(8,128)S(1)} %get-tuple-element.63.decay_ref, f32[64,128]{1,0:T(8,128)S(1)} %get-tuple-element.37.key_ref, ...), custom_call_target="tpu_custom_call" | custom-call | flops 2000000000 | bytes 8388608 | tf_op jit(solution)/shard_map/update_state/pallas_call | solution.py:347
  72.1 1.9 %all-to-all-done.2 = bf16[128,3,4,128]{3,2,1,0:T(4,128)(2,1)S(1)} async-done(((bf16[128,3,4,128]{3,2,1,0:T(4,128)(2,1)}), bf16[128,3,4,128]{3,2,1,0:T(4,128)(2,1)S(1)}, u32[]{:S(2)}, u32[]{:S(2)}) %all-to-all-start.2) | async-done | bytes 393248 | tf_op jit(solution)/shard_map/all_to_all | solution.py:555
  74.0 0.9 %combine.1 = bf16[64,128]{1,0:T(8,128)(2,1)} custom-call(f32[192,64]{1,0:T(8,128)S(1)} %get-tuple-element.33.share_ref, bf16[8,192,128]{2,1,0:T(8,128)(2,1)S(1)} %bitcast.35, bf16[64,128]{1,0:T(8,128)(2,1)S(1)} %get-tuple-element.61.resid_ref), custom_call_target="tpu_custom_call" | custom-call | tf_op jit(solution)/shard_map/combine/pallas_call | solution.py:542
  (5 shorter events, 0.0 us)
Async XLA Ops:
  0.6 3.6 %copy-start = (f32[64,2,64,64]{3,2,1,0:T(8,128)S(1)}, f32[64,2,64,64]{3,2,1,0:T(8,128)}, u32[]{:S(2)}) copy-start(f32[64,2,64,64]{3,2,1,0:T(8,128)} %param.20) | copy-start | bytes 6291460
  0.6 3.6 %copy-start.5 = (f32[128]{0:T(128)S(1)}, f32[128]{0:T(128)}, u32[]{:S(2)}) copy-start(f32[128]{0:T(128)} %param.32) | copy-start | bytes 1540
  4.3 42.2 %copy-start.2 = (bf16[1,2048,448]{1,2,0:T(8,128)(2,1)S(1)}, bf16[1,2048,448]{1,2,0:T(8,128)(2,1)}, u32[]{:S(2)}) copy-start(bf16[1,2048,448]{1,2,0:T(8,128)(2,1)} %param.36) | copy-start | bytes 5505028
  4.3 42.2 %copy-start.3 = (bf16[1,448,2048]{2,1,0:T(8,128)(2,1)S(1)}, bf16[1,448,2048]{2,1,0:T(8,128)(2,1)}, u32[]{:S(2)}) copy-start(bf16[1,448,2048]{2,1,0:T(8,128)(2,1)} %param.37) | copy-start | bytes 5505028
  5.7 40.8 %copy-start.1 = (bf16[1,2048,448]{1,2,0:T(8,128)(2,1)S(1)}, bf16[1,2048,448]{1,2,0:T(8,128)(2,1)}, u32[]{:S(2)}) copy-start(bf16[1,2048,448]{1,2,0:T(8,128)(2,1)} %param.35) | copy-start | bytes 5505028
  5.7 40.8 %copy-start.4 = (f32[2048]{0:T(1024)S(1)}, f32[2048]{0:T(1024)}, u32[]{:S(2)}) copy-start(f32[2048]{0:T(1024)} %param.34) | copy-start | bytes 24580
  5.7 4.3 %collective-permute-start = (bf16[8,64,128]{2,1,0:T(8,128)(2,1)S(1)}, bf16[8,64,128]{2,1,0:T(8,128)(2,1)S(1)}, u32[]{:S(2)}, u32[]{:S(2)}) collective-permute-start(bf16[8,64,128]{2,1,0:T(8,128)(2,1)S(1)} %get-tuple-element.41), channel_id=1, source_target_pairs={{0,1},{1,0},{2,3},{3,2},{4,5},{5,4},{6,7},{7,6},{8,9},{9,8},{10,11... | collective-permute-start | bytes 393224 | tf_op jit(solution)/shard_map/ppermute | solution.py:551
  43.8 3.7 %collective-permute-start.2 = (bf16[4,192,128]{2,1,0:T(8,128)(2,1)S(1)}, bf16[4,192,128]{2,1,0:T(8,128)(2,1)S(1)}, u32[]{:S(2)}, u32[]{:S(2)}) collective-permute-start(bf16[4,192,128]{2,1,0:T(8,128)(2,1)S(1)} %bitcast.43), channel_id=1, source_target_pairs={{0,1},{1,0},{2,3},{3,2},{4,5},{5,4},{6,7},{7,6},{8,9},{9,8},{10,11... | collective-permute-start | bytes 589832 | tf_op jit(solution)/shard_map/ppermute | solution.py:551
  46.4 1.6 %collective-permute-start.1 = (bf16[4,192,128]{2,1,0:T(8,128)(2,1)S(1)}, bf16[4,192,128]{2,1,0:T(8,128)(2,1)S(1)}, u32[]{:S(2)}, u32[]{:S(2)}) collective-permute-start(bf16[4,192,128]{2,1,0:T(8,128)(2,1)S(1)} %bitcast.42), channel_id=1, source_target_pairs={{0,1},{1,0},{2,3},{3,2},{4,5},{5,4},{6,7},{7,6},{8,9},{9,8},{10,11... | collective-permute-start | bytes 589832 | tf_op jit(solution)/shard_map/ppermute | solution.py:551
  48.8 1.8 %collective-permute-start.3 = (bf16[8,192,128]{2,1,0:T(8,128)(2,1)S(1)}, bf16[8,192,128]{2,1,0:T(8,128)(2,1)S(1)}, u32[]{:S(2)}, u32[]{:S(2)}) collective-permute-start(bf16[8,192,128]{2,1,0:T(8,128)(2,1)S(1)} %get-tuple-element.60), channel_id=1, source_target_pairs={{0,1},{1,0},{2,3},{3,2},{4,5},{5,4},{6,7},{7,6},{8,9},{9,8},{10,11... | collective-permute-start | bytes 1179656 | tf_op jit(solution)/shard_map/ppermute | solution.py:551
  51.5 22.5 %all-to-all-start.2 = ((bf16[128,3,4,128]{3,2,1,0:T(4,128)(2,1)}), bf16[128,3,4,128]{3,2,1,0:T(4,128)(2,1)S(1)}, u32[]{:S(2)}, u32[]{:S(2)}) async-start(bf16[128,3,4,128]{3,2,1,0:T(4,128)(2,1)} %bitcast.18), calls=%async_computation.2 | async-start | bytes 786432 | tf_op jit(solution)/shard_map/all_to_all | solution.py:555
